TPU v7x, 32 devices: a whole 2x2x4 slice. The times are simulated.
32 devices in a mesh: sp: 8 (over z, x), tp: 4 (over y, core).
Axes of the slice: x: 2, y: 2, z: 4, core: 2. Of those that a mesh axis runs over, the one named last changes fastest.
Arguments:
- stream: bfloat16 [4096, 2048], P(('sp', 'tp')), may hold values from -6 to 6
- projected: bfloat16 [4096, 2048], P('sp', 'tp'), may hold values from -6 to 6
- segments: int32 [4096], P('sp'), may hold values from 0 to 3, never falling along the last dimension, each value on 1 to 1536 neighbouring positions
- group_weight: bfloat16 [4, 512, 512], replicated, may hold values from -0.25 to 0.25
- group_scale: float32 [2048], replicated, may hold values from 0.1 to 1.9
- out_weight: bfloat16 [2048, 2048], replicated, may hold values from -0.125 to 0.125
- ffn_gain: float32 [2048], replicated, may hold values from 0.1 to 1.9
- routes: int32 [4096, 4], P(('sp', 'tp')), may hold values from 0 to 31, all different within a row; in each aligned block of 128 rows (0 to 127, 128 to 255, ...) at most 24 rows name the same one
- route_weights: float32 [4096, 4], P(('sp', 'tp')), may hold values from 0.05 to 0.5
- expert_gate: bfloat16 [32, 2048, 1024], P(('sp', 'tp')), may hold values from -0.25 to 0.25
- expert_up: bfloat16 [32, 2048, 1024], P(('sp', 'tp')), may hold values from -0.25 to 0.25
- expert_down: bfloat16 [32, 1024, 2048], P(('sp', 'tp')), may hold values from -0.1875 to 0.1875
Outputs:
- combined: bfloat16 [4096, 2048], P(('sp', 'tp'))
Inputs may be any that keep to these rules, and one draw needn't show every extreme that they name: `segments`: document numbers never fall along the positions; a document has 1 to 1536 positions, and one has exactly 1536. `routes`: each row names 4 different experts. Among the 128 rows of one device (aligned blocks), no expert is named more than 24 times, and in some blocks one is named exactly 24 times.
All inputs are finite; a program needn't handle non-finite values.
Results may differ from a plain program's by a relative error of at most 0.015.
Values may be sent and summed in bfloat16 or wider, within the bound.
No kernel may reach another device: no remote copies, remote signals or barrier semaphores. Data moves between devices by JAX's collectives and lax.ppermute only.
A program may use at most 128 MiB of HBM per device.

v0:
```python
import jax
import jax.numpy as jnp
from jax import lax
from jax.sharding import PartitionSpec as P

GROUPS = 4


norm_eps = 1e-05
clamp_limit = 7.0
sigmoid_alpha = 1.702
longest_window = 16


def carried_in(value, axis, join, neutral):
    count, mine = (lax.axis_size(axis), lax.axis_index(axis))
    pieces = jax.tree.map(lambda part: lax.all_gather(part, axis), value)
    so_far = jax.tree.map(
        lambda part, zero: jnp.full_like(part, 0) + jnp.asarray(zero, part.dtype), value, neutral
    )

    def hop(position, so_far):
        longer = join(so_far, jax.tree.map(lambda part: part[position], pieces))
        return jax.tree.map(lambda new, old: jnp.where(position < mine, new, old), longer, so_far)

    return lax.fori_loop(0, count - 1, hop, so_far)


def rms_scale(resid, gain):
    values = resid.astype(jnp.float32)
    inverse = lax.rsqrt(jnp.mean(values * values, -1, keepdims=True) + norm_eps)
    return (values * inverse * gain).astype(jnp.bfloat16)


def run_expert(block, gate_matrix, up_matrix, down_matrix):
    leading = block.shape[:-1]
    flat_rows = block.reshape(-1, block.shape[-1])
    gate_value = jnp.dot(flat_rows, gate_matrix, preferred_element_type=jnp.float32)
    up_value = jnp.dot(flat_rows, up_matrix, preferred_element_type=jnp.float32)
    gated = jnp.minimum(gate_value, clamp_limit)
    linear = jnp.clip(up_value, -clamp_limit, clamp_limit)
    activated = (gated * jax.nn.sigmoid(sigmoid_alpha * gated) * (linear + 1.0)).astype(
        jnp.bfloat16
    )
    result = jnp.dot(activated, down_matrix, preferred_element_type=jnp.float32).astype(
        jnp.bfloat16
    )
    return result.reshape(leading + (down_matrix.shape[1],))


def keep_latter(earlier, latter):
    present = latter[1] >= 0
    return (
        jnp.where(present[..., None], latter[0], earlier[0]),
        jnp.where(present, latter[1], earlier[1]),
    )


def body(
    stream,
    projected,
    segments,
    group_weight,
    group_scale,
    out_weight,
    ffn_gain,
    routes,
    route_weights,
    expert_gate,
    expert_up,
    expert_down,
):
    row_count, channels = projected.shape
    tp_count = lax.axis_size("tp")
    sp_count = lax.axis_size("sp")
    model_width = channels * tp_count
    group_width = model_width // GROUPS
    rim_rows = longest_window - 1
    channel = lax.axis_index("tp") * channels + jnp.arange(channels, dtype=jnp.int32)
    window = jnp.left_shift(jnp.full((channels,), 2, jnp.int32), channel // group_width)
    identity = (jnp.zeros((rim_rows, channels), jnp.bfloat16), jnp.full((rim_rows,), -1, jnp.int32))
    before_rows, before_docs = carried_in(
        (projected[row_count - rim_rows :], segments[row_count - rim_rows :]),
        "sp",
        keep_latter,
        identity,
    )
    extended = jnp.concatenate([before_rows, projected], 0)
    extended_docs = jnp.concatenate([before_docs, segments], 0)
    window_sum = jnp.zeros((row_count, channels), jnp.float32)
    window_count = jnp.zeros((row_count, channels), jnp.float32)
    for offset in range(longest_window):
        earlier_rows = extended[rim_rows - offset : rim_rows - offset + row_count].astype(
            jnp.float32
        )
        earlier_docs = extended_docs[rim_rows - offset : rim_rows - offset + row_count]
        included = (earlier_docs == segments)[:, None] & (offset < window)[None, :]
        window_sum = window_sum + jnp.where(included, earlier_rows, jnp.float32(0.0))
        window_count = window_count + included.astype(jnp.float32)
    mixed = (window_sum / window_count - projected.astype(jnp.float32)).astype(jnp.bfloat16)
    tokens_here = lax.all_to_all(mixed, "tp", split_axis=0, concat_axis=1, tiled=True)
    tok_count = tokens_here.shape[0]
    grouped = jnp.einsum(
        "rgc,gcd->rgd",
        tokens_here.reshape(tok_count, GROUPS, group_width),
        group_weight,
        preferred_element_type=jnp.float32,
    ).reshape(tok_count, model_width)
    scaled = (grouped * group_scale).astype(jnp.bfloat16)
    mixer_out = jnp.dot(scaled, out_weight, preferred_element_type=jnp.float32)
    resid = (stream.astype(jnp.float32) + mixer_out).astype(jnp.bfloat16)
    normed = rms_scale(resid, ffn_gain)
    top_count = routes.shape[1]
    expert_count = sp_count * tp_count
    capacity = 3 * tok_count * top_count // (2 * expert_count)
    flat_routes = routes.reshape(-1)
    onehot = (flat_routes[:, None] == jnp.arange(expert_count, dtype=jnp.int32)[None, :]).astype(
        jnp.int32
    )
    ranking = jnp.sum((jnp.cumsum(onehot, 0) - onehot) * onehot, 1)
    slot_index = flat_routes * capacity + ranking
    token_of = jnp.arange(flat_routes.shape[0], dtype=jnp.int32) // top_count
    slot_token = jnp.zeros((expert_count * capacity,), jnp.int32).at[slot_index].set(token_of)
    slot_live = jnp.zeros((expert_count * capacity,), jnp.bool_).at[slot_index].set(True)
    outgoing = jnp.where(slot_live[:, None], normed[slot_token], jnp.zeros((), jnp.bfloat16))
    results = run_expert(
        lax.all_to_all(
            outgoing.reshape(expert_count, capacity, model_width),
            ("sp", "tp"),
            split_axis=0,
            concat_axis=0,
            tiled=True,
        ),
        expert_gate[0],
        expert_up[0],
        expert_down[0],
    )
    returned = lax.all_to_all(results, ("sp", "tp"), split_axis=0, concat_axis=0, tiled=True)
    picked = returned.reshape(expert_count * capacity, model_width)[slot_index]
    weighted = picked.astype(jnp.float32) * route_weights.reshape(-1)[:, None]
    moe_sum = jnp.sum(weighted.reshape(tok_count, top_count, model_width), 1)
    return (resid.astype(jnp.float32) + moe_sum).astype(jnp.bfloat16)


def solution(mesh):
    in_specs = (
        P(("sp", "tp"), None),
        P("sp", "tp"),
        P("sp"),
        P(),
        P(),
        P(),
        P(),
        P(("sp", "tp"), None),
        P(("sp", "tp"), None),
        P(("sp", "tp"), None, None),
        P(("sp", "tp"), None, None),
        P(("sp", "tp"), None, None),
    )
    out_specs = P(("sp", "tp"), None)
    return jax.shard_map(body, mesh=mesh, in_specs=in_specs, out_specs=out_specs, check_vma=False)
```

profile of v0, /device:TPU:0, one launch (start us, length us, event | category | flops | bytes accessed | tf_op | source)
XLA Modules:
  0.0 276.2 jit_solution(8071681615724556386)
XLA Ops:
  0.2 1.4 dynamic-slice
  2.3 0.8 slice_dynamic-update-slice_fusion
  3.2 13.1 %all-reduce = s32[120]{0:T(128)S(1)} all-reduce(s32[120]{0:T(128)S(1)} %slice_dynamic-update-slice_fusion), channel_id=2, replica_groups=mesh['sp'=8,'tp'=4] {'sp'}, use_global_device_ids=true, to_apply=%add | all-reduce | flops 120 | bytes 960
  16.2 0.1 reshape.217
  16.3 0.7 slice_bitcast_fusion
  17.1 30.5 %all-gather.2 = bf16[8,15,512]{2,1,0:T(8,128)(2,1)S(1)} all-gather(bf16[1,15,512]{2,1,0:T(8,128)(2,1)S(1)} %slice_bitcast_fusion), channel_id=3, replica_groups=mesh['sp'=8,'tp'=4] {'sp'}, dimensions={0}, use_global_device_ids=true | all-gather | bytes 138240 | tf_op jit(solution)/shard_map/all_gather | solution.py:17
  47.6 0.9 while.16
  47.7 0.1 select_select_fusion.2
  47.8 0.1 select_select_fusion.2
  48.0 0.1 select_select_fusion.2
  48.1 0.1 select_select_fusion.2
  48.4 0.1 select_select_fusion.2
  48.5 0.8 pad_add_fusion
  49.2 0.8 slice_compare_fusion.14
  50.0 15.9 %fusion.45 = bf16[512,512]{1,0:T(8,128)(2,1)} fusion(bf16[512,512]{1,0:T(8,128)(2,1)} %param.15, bf16[15,512]{1,0:T(8,128)(2,1)S(1)} %get-tuple-element.116, f32[512]{0:T(512)S(1)} %get-tuple-element.183, pred[512]{0:T(512)(128)(4,1)S(1)} %get-tuple-element.167, pred[512]{0:T(512)(128)(4,1)S(1)} %get-tuple-element.168, ...), kind=kLoop, calls=%fused_computation.105 | loop fusion | flops 36700160 | bytes 1081856 | tf_op jit(solution)/shard_map/convert_element_type | solution.py:100
  65.9 4.1 %all-to-all-start = ((bf16[4,128,512]{2,1,0:T(8,128)(2,1)}), bf16[4,128,512]{2,1,0:T(8,128)(2,1)}, u32[]{:S(2)}, u32[]{:S(2)}) async-start(bf16[4,128,512]{2,1,0:T(8,128)(2,1)} %bitcast.2), calls=%async_computation | async-start | bytes 1048576 | tf_op jit(solution)/shard_map/all_to_all | solution.py:101
  70.0 0.8 copy.22
  70.8 0.1 eq.89
  70.9 0.1 eq.85
  71.0 0.7 broadcast_multiply_fusion
  71.7 1.2 reduce-window.6
  72.9 0.2 slice_reduce_fusion
  73.2 0.1 copy.21
  73.3 0.1 mul.75
  73.4 0.1 fusion.63
  73.5 2.4 scatter_custom_fusion.1
  76.0 2.4 scatter_custom_fusion
  78.4 0.1 broadcast_in_dim.109
  78.6 0.3 all-to-all-done
  78.9 1.5 convolution_bitcast_fusion
  80.4 1.3 copy.20
  81.7 1.6 fusion.44
  83.3 4.8 %multiply_reduce_fusion.1 = (f32[128]{0:T(128)S(1)}, f32[128,2048]{1,0:T(8,128)S(1)}) fusion(bf16[128,2048]{0,1:T(8,128)(2,1)S(1)} %fusion.44, bf16[2048,2048]{1,0:T(8,128)(2,1)} %param.19, bf16[128,2048]{1,0:T(8,128)(2,1)} %param.14), kind=kOutput, calls=%fused_computation.104 | convolution fusion | flops 1075314560 | bytes 10486272 | tf_op jit(solution)/shard_map/dot_general | solution.py:110
  88.1 1.0 copy-done.1
  89.1 0.2 multiply_convert_fusion.1
  89.3 4.3 %gather_fusion = bf16[768,2048]{1,0:T(8,128)(2,1)} fusion(bf16[128,2048]{1,0:T(8,128)(2,1)S(1)} %multiply_convert_fusion.1, s32[1024]{0:T(1024)S(1)} %pad_clamp_fusion.1), kind=kCustom, calls=%fused_computation | custom fusion | bytes 6294528 | tf_op jit(solution)/shard_map/gather | solution.py:125
  93.5 2.2 broadcast_select_fusion.2
  95.7 73.9 %all_to_all.26 = bf16[32,24,2048]{2,1,0:T(8,128)(2,1)S(1)} all-to-all(bf16[32,24,2048]{2,1,0:T(8,128)(2,1)S(1)} %broadcast_select_fusion.2), channel_id=1, replica_groups=mesh['sp'=8,'tp'=4] {'sp','tp'}, dimensions={0} | all-to-all | bytes 6291456 | tf_op jit(solution)/shard_map/all_to_all | solution.py:127
  169.6 3.4 %fusion.2 = f32[768,1024]{1,0:T(8,128)S(1)} fusion(bf16[768,2048]{1,0:T(8,128)(2,1)S(1)} %bitcast.72, bf16[1,2048,1024]{2,1,0:T(8,128)(2,1)S(1)} %copy-done.6), kind=kOutput, calls=%fused_computation.11 | convolution fusion | flops 3221225472 | bytes 10485760 | tf_op jit(solution)/shard_map/dot_general | solution.py:39
  173.1 4.1 %multiply_convert_fusion = bf16[768,1024]{1,0:T(8,128)(2,1)S(1)} fusion(f32[768,1024]{1,0:T(8,128)S(1)} %fusion.2, bf16[768,2048]{1,0:T(8,128)(2,1)S(1)} %bitcast.73, bf16[1,2048,1024]{2,1,0:T(8,128)(2,1)S(1)} %copy-done.7), kind=kOutput, calls=%fused_computation.17 | convolution fusion | flops 3229089792 | bytes 12058624 | tf_op jit(solution)/shard_map/dot_general | solution.py:38
  177.3 4.8 %fusion.6 = bf16[768,2048]{1,0:T(8,128)(2,1)} fusion(bf16[768,1024]{1,0:T(8,128)(2,1)S(1)} %multiply_convert_fusion, bf16[1,1024,2048]{2,1,0:T(8,128)(2,1)S(1)} %copy-done.8), kind=kOutput, calls=%fused_computation.16 | convolution fusion | flops 3222798336 | bytes 8912896 | tf_op jit(solution)/shard_map/dot_general | solution.py:45
  182.1 4.0 %all-to-all-start.2 = ((bf16[32,24,2048]{2,1,0:T(8,128)(2,1)}), bf16[32,24,2048]{2,1,0:T(8,128)(2,1)}, u32[]{:S(2)}, u32[]{:S(2)}) async-start(bf16[32,24,2048]{2,1,0:T(8,128)(2,1)} %bitcast.71), calls=%async_computation.2 | async-start | bytes 6291456 | tf_op jit(solution)/shard_map/all_to_all | solution.py:138
  186.1 0.1 copy.25
  186.2 71.2 %all-to-all-done.2 = bf16[32,24,2048]{2,1,0:T(8,128)(2,1)} async-done(((bf16[32,24,2048]{2,1,0:T(8,128)(2,1)}), bf16[32,24,2048]{2,1,0:T(8,128)(2,1)}, u32[]{:S(2)}, u32[]{:S(2)}) %all-to-all-start.2) | async-done | bytes 3145760 | tf_op jit(solution)/shard_map/all_to_all | solution.py:138
  257.5 7.6 %gather_fusion.1 = bf16[512,2048]{1,0:T(8,128)(2,1)} fusion(bf16[768,2048]{1,0:T(8,128)(2,1)} %bitcast.15, s32[1024]{0:T(1024)S(1)} %pad_clamp_fusion), kind=kCustom, calls=%fused_computation.1 | custom fusion | bytes 4196352 | tf_op jit(solution)/shard_map/gather | solution.py:139
  265.1 4.8 %reshape.184 = f32[128,4,2048]{2,1,0:T(4,128)} reshape(bf16[512,2048]{1,0:T(8,128)(2,1)} %gather_fusion.1) | data formatting | bytes 6291456 | tf_op jit(solution)/shard_map/convert_element_type | solution.py:140
  269.8 5.5 %multiply_reduce_fusion = f32[128,2048]{1,0:T(8,128)S(1)} fusion(f32[128,4,2048]{2,1,0:T(4,128)} %reshape.184, f32[128,4]{1,0:T(8,128)S(1)} %copy.25), kind=kLoop, calls=%fused_computation.15 | loop fusion | flops 1835008 | bytes 5244928 | tf_op jit(solution)/shard_map/reduce_sum | solution.py:141
  275.3 0.9 add_convert_fusion
  (54 shorter events, 0.6 us)
Async XLA Ops:
  0.0 78.9 %copy-start = (bf16[4,512,512]{2,1,0:T(8,128)(2,1)S(1)}, bf16[4,512,512]{2,1,0:T(8,128)(2,1)}, u32[]{:S(2)}) copy-start(bf16[4,512,512]{2,1,0:T(8,128)(2,1)} %param.17) | copy-start | bytes 6291460
  65.9 13.0 %all-to-all-start = ((bf16[4,128,512]{2,1,0:T(8,128)(2,1)}), bf16[4,128,512]{2,1,0:T(8,128)(2,1)}, u32[]{:S(2)}, u32[]{:S(2)}) async-start(bf16[4,128,512]{2,1,0:T(8,128)(2,1)} %bitcast.2), calls=%async_computation | async-start | bytes 1048576 | tf_op jit(solution)/shard_map/all_to_all | solution.py:101
  71.7 10.0 %copy-start.3 = (f32[2048]{0:T(1024)S(1)}, f32[2048]{0:T(1024)}, u32[]{:S(2)}) copy-start(f32[2048]{0:T(1024)} %param.18) | copy-start | bytes 24580
  83.3 5.8 %copy-start.4 = (f32[2048]{0:T(1024)S(1)}, f32[2048]{0:T(1024)}, u32[]{:S(2)}) copy-start(f32[2048]{0:T(1024)} %param.20) | copy-start | bytes 24580
  88.1 1.0 copy-start.1
  95.7 73.9 %copy-start.6 = (bf16[1,2048,1024]{2,1,0:T(8,128)(2,1)S(1)}, bf16[1,2048,1024]{2,1,0:T(8,128)(2,1)}, u32[]{:S(2)}) copy-start(bf16[1,2048,1024]{2,1,0:T(8,128)(2,1)} %param.24) | copy-start | bytes 12582916
  169.6 3.5 %copy-start.7 = (bf16[1,2048,1024]{2,1,0:T(8,128)(2,1)S(1)}, bf16[1,2048,1024]{2,1,0:T(8,128)(2,1)}, u32[]{:S(2)}) copy-start(bf16[1,2048,1024]{2,1,0:T(8,128)(2,1)} %param.23) | copy-start | bytes 12582916
  173.1 4.2 %copy-start.8 = (bf16[1,1024,2048]{2,1,0:T(8,128)(2,1)S(1)}, bf16[1,1024,2048]{2,1,0:T(8,128)(2,1)}, u32[]{:S(2)}) copy-start(bf16[1,1024,2048]{2,1,0:T(8,128)(2,1)} %param.25) | copy-start | bytes 12582916
  182.1 4.0 %copy-start.5 = (f32[128,4]{0,1:T(4,128)S(1)}, f32[128,4]{0,1:T(4,128)}, u32[]{:S(2)}) copy-start(f32[128,4]{0,1:T(4,128)} %param.22) | copy-start | bytes 6148
  182.1 75.4 %all-to-all-start.2 = ((bf16[32,24,2048]{2,1,0:T(8,128)(2,1)}), bf16[32,24,2048]{2,1,0:T(8,128)(2,1)}, u32[]{:S(2)}, u32[]{:S(2)}) async-start(bf16[32,24,2048]{2,1,0:T(8,128)(2,1)} %bitcast.71), calls=%async_computation.2 | async-start | bytes 6291456 | tf_op jit(solution)/shard_map/all_to_all | solution.py:138
  269.8 5.5 %copy-start.2 = (f32[128,2048]{1,0:T(8,128)S(1)}, f32[128,2048]{1,0:T(8,128)}, u32[]{:S(2)}) copy-start(f32[128,2048]{1,0:T(8,128)} %copy-done.1) | copy-start | bytes 3145732
where the time goes:
time: 278 us; the launch traced here: 276 us
  blocking collectives  117 us (42%)
  waiting for transfers between devices  71.6 us (26%)
  other arithmetic  30.6 us (11%)
  local copies, waits for them, and re-layouts  28.6 us (10%)
  matrix products  18.7 us (7%)
  starting transfers between devices  8.13 us (3%)
    all_to_all x1, blocking collectives, body(): lax.all_to_all(outgoing.reshape(expert_count, capacity, model_width), ('s...  73.9 us
    all_to_all x1, waiting for transfers between devices, body(): lax.all_to_all(results, ('sp', 'tp'), split_axis=0, concat_axis=0, tiled=...  71.2 us
    all_gather x1, blocking collectives, carried_in(): pieces = jax.tree.map(lambda part: lax.all_gather(part, axis), value)  30.5 us
    convert_element_type x1, other arithmetic, body(): (window_sum / window_count - projected.astype(jnp.float32)).astype(jnp.bf...  15.9 us
    unnamed x1, blocking collectives  13.1 us
    gather x1, local copies, waits for them, and re-layouts, body(): picked = returned.reshape(expert_count * capacity, model_width)[slot_index]  7.56 us
  transfers between devices with their start and end apart: 2, of which 2 were waited for; matrix products, arithmetic and copies ran while one was open for 3% of the time, Pallas kernels for 0%

commit v1 on v0

v1 whole, which is shorter than its diff:
```python
import functools

import jax
import jax.numpy as jnp
from jax import lax
from jax.experimental import pallas as pl
from jax.experimental.pallas import tpu as pltpu
from jax.sharding import PartitionSpec as P

GROUPS = 4

norm_eps = 1e-05
clamp_limit = 7.0
sigmoid_alpha = 1.702
longest_window = 16
VMEM_BYTES = 56 * 1024 * 1024


def dot32(a, b):
    return jnp.dot(a, b, preferred_element_type=jnp.float32)


def pool_kernel(first_ref, rim_ref, rows_ref, docs_ref, out_ref, *, group_width, span):
    row_count, channels = rows_ref.shape
    rim = rim_ref.shape[0]
    block = min(row_count, 128)
    first_group = first_ref[0] // group_width
    groups_here = max(1, channels // group_width)
    width = channels // groups_here
    wide = block + rim
    docs = docs_ref[...]
    rim_docs = (rim_ref[0:1, 0:rim].astype(jnp.float32) - 1.0).astype(jnp.int32)
    at_row = lax.broadcasted_iota(jnp.int32, (block, wide), 0)
    at_col = lax.broadcasted_iota(jnp.int32, (block, wide), 1)
    for start in range(0, row_count, block):
        here = docs[:, start : start + block]
        if start == 0:
            before, before_rows = rim_docs, rim_ref[...]
        else:
            before = docs[:, start - rim : start]
            before_rows = rows_ref[start - rim : start, :]
        col_docs = jnp.concatenate([before, here], 1)
        row_docs = jnp.sum(
            jnp.where(at_col == at_row + rim, jnp.broadcast_to(col_docs, (block, wide)), 0),
            1,
            keepdims=True,
        )
        back = at_row + rim - at_col
        alike = (col_docs == row_docs) & (back >= 0)
        own = rows_ref[start : start + block, :]
        values = jnp.concatenate([before_rows, own], 0)
        for part in range(groups_here):
            window = jnp.left_shift(2, first_group + part)
            band = jnp.where(alike & (back < window), 1.0, 0.0)
            count = jnp.sum(band, 1, keepdims=True)
            lanes = slice(part * width, (part + 1) * width)
            total = dot32(band.astype(jnp.bfloat16), values[:, lanes])
            out_ref[start : start + block, lanes] = (
                total / count - own[:, lanes].astype(jnp.float32)
            ).astype(jnp.bfloat16)


def pool(first, rim, rows, docs, group_width):
    return pl.pallas_call(
        functools.partial(pool_kernel, group_width=group_width, span=longest_window),
        out_shape=jax.ShapeDtypeStruct(rows.shape, jnp.bfloat16),
        in_specs=[
            pl.BlockSpec(memory_space=pltpu.SMEM),
            pl.BlockSpec(memory_space=pltpu.VMEM),
            pl.BlockSpec(memory_space=pltpu.VMEM),
            pl.BlockSpec(memory_space=pltpu.VMEM),
        ],
        out_specs=pl.BlockSpec(memory_space=pltpu.VMEM),
        name="pool",
    )(first, rim, rows, docs)


def slot_table(routes_t, experts, capacity):
    top, tokens = routes_t.shape
    expert = lax.broadcasted_iota(jnp.int32, (experts, tokens), 0)
    named = jnp.zeros((experts, tokens), jnp.bool_)
    for j in range(top):
        named = named | (routes_t[j : j + 1, :] == expert)
    earlier = (
        lax.broadcasted_iota(jnp.int32, (tokens, tokens), 0)
        < lax.broadcasted_iota(jnp.int32, (tokens, tokens), 1)
    )
    ones = jnp.where(named, 1.0, 0.0)
    rank = dot32(ones.astype(jnp.bfloat16), jnp.where(earlier, 1.0, 0.0).astype(jnp.bfloat16))
    held = jnp.where(named, rank, -1.0).astype(jnp.bfloat16)
    slots = experts * capacity
    low = lax.broadcasted_iota(jnp.int32, (slots, experts), 1) * capacity
    slot = lax.broadcasted_iota(jnp.int32, (slots, experts), 0)
    spread = jnp.where((slot >= low) & (slot < low + capacity), 1.0, 0.0).astype(jnp.bfloat16)
    within = slot - jnp.where((slot >= low) & (slot < low + capacity), low, 0)
    place = jnp.sum(
        jnp.where((slot >= low) & (slot < low + capacity), slot - low, 0), 1, keepdims=True
    ).astype(jnp.float32)
    del within
    return dot32(spread, held) == place, spread


def mixer_kernel(
    mixed_ref, gw_ref, gs_ref, ow_ref, stream_ref, gain_ref, routes_ref, resid_ref, send_ref,
    *, capacity, experts,
):
    groups, width, _ = gw_ref.shape
    parts = []
    for g in range(groups):
        lanes = slice(g * width, (g + 1) * width)
        grouped = dot32(mixed_ref[:, lanes], gw_ref[g])
        parts.append((grouped * gs_ref[:, lanes]).astype(jnp.bfloat16))
    scaled = jnp.concatenate(parts, 1)
    mixer_out = dot32(scaled, ow_ref[...])
    resid = (stream_ref[...].astype(jnp.float32) + mixer_out).astype(jnp.bfloat16)
    resid_ref[...] = resid
    values = resid.astype(jnp.float32)
    inverse = lax.rsqrt(jnp.mean(values * values, -1, keepdims=True) + norm_eps)
    normed = (values * inverse * gain_ref[...]).astype(jnp.bfloat16)
    taken, _ = slot_table(routes_ref[...], experts, capacity)
    pick = jnp.where(taken, 1.0, 0.0).astype(jnp.bfloat16)
    send_ref[...] = dot32(pick, normed).astype(jnp.bfloat16)


def mixer(mixed, gw, gs, ow, stream, gain, routes_t, experts, capacity):
    tokens, width = mixed.shape
    return pl.pallas_call(
        functools.partial(mixer_kernel, capacity=capacity, experts=experts),
        out_shape=(
            jax.ShapeDtypeStruct((tokens, width), jnp.bfloat16),
            jax.ShapeDtypeStruct((experts * capacity, width), jnp.bfloat16),
        ),
        in_specs=[pl.BlockSpec(memory_space=pltpu.VMEM)] * 7,
        out_specs=(pl.BlockSpec(memory_space=pltpu.VMEM),) * 2,
        compiler_params=pltpu.CompilerParams(vmem_limit_bytes=VMEM_BYTES),
        name="mixer",
    )(mixed, gw, gs.reshape(1, -1), ow, stream, gain.reshape(1, -1), routes_t)


def combine_kernel(resid_ref, back_ref, routes_ref, weights_ref, out_ref, *, capacity, experts):
    routes_t, weights_t = routes_ref[...], weights_ref[...]
    top, tokens = routes_t.shape
    taken, spread = slot_table(routes_t, experts, capacity)
    expert = lax.broadcasted_iota(jnp.int32, (experts, tokens), 0)
    weight = jnp.zeros((experts, tokens), jnp.float32)
    for j in range(top):
        weight = weight + jnp.where(routes_t[j : j + 1, :] == expert, weights_t[j : j + 1, :], 0.0)
    high = weight.astype(jnp.bfloat16)
    low = (weight - high.astype(jnp.float32)).astype(jnp.bfloat16)
    back = back_ref[...]
    total = resid_ref[...].astype(jnp.float32)
    for piece in (high, low):
        factor = jnp.where(taken, dot32(spread, piece), 0.0).astype(jnp.bfloat16)
        total = total + lax.dot_general(
            factor, back, (((0,), (0,)), ((), ())), preferred_element_type=jnp.float32
        )
    out_ref[...] = total.astype(jnp.bfloat16)


def combine(resid, back, routes_t, weights_t, experts, capacity):
    return pl.pallas_call(
        functools.partial(combine_kernel, capacity=capacity, experts=experts),
        out_shape=jax.ShapeDtypeStruct(resid.shape, jnp.bfloat16),
        in_specs=[pl.BlockSpec(memory_space=pltpu.VMEM)] * 4,
        out_specs=pl.BlockSpec(memory_space=pltpu.VMEM),
        compiler_params=pltpu.CompilerParams(vmem_limit_bytes=VMEM_BYTES),
        name="combine",
    )(resid, back, routes_t, weights_t)


def run_expert(rows, gate_matrix, up_matrix, down_matrix):
    gate_value = dot32(rows, gate_matrix)
    up_value = dot32(rows, up_matrix)
    gated = jnp.minimum(gate_value, clamp_limit)
    linear = jnp.clip(up_value, -clamp_limit, clamp_limit)
    activated = (gated * jax.nn.sigmoid(sigmoid_alpha * gated) * (linear + 1.0)).astype(
        jnp.bfloat16
    )
    return dot32(activated, down_matrix).astype(jnp.bfloat16)


def body(
    stream,
    projected,
    segments,
    group_weight,
    group_scale,
    out_weight,
    ffn_gain,
    routes,
    route_weights,
    expert_gate,
    expert_up,
    expert_down,
):
    row_count, channels = projected.shape
    tp_count = lax.axis_size("tp")
    sp_count = lax.axis_size("sp")
    model_width = channels * tp_count
    group_width = model_width // GROUPS
    rim = longest_window
    tail_docs = (segments[row_count - rim :] + 1).astype(jnp.bfloat16)
    payload = jnp.concatenate(
        [
            jnp.pad(tail_docs, (0, channels - rim))[None, :],
            projected[row_count - rim + 1 :],
        ],
        0,
    )
    before = lax.ppermute(payload, "sp", [(i, i + 1) for i in range(sp_count - 1)])
    first = (lax.axis_index("tp") * channels).reshape(1)
    mixed = pool(first, before, projected, segments[None, :], group_width)
    tokens_here = lax.all_to_all(mixed, "tp", split_axis=0, concat_axis=1, tiled=True)
    tok_count, top_count = routes.shape
    expert_count = sp_count * tp_count
    capacity = 3 * tok_count * top_count // (2 * expert_count)
    routes_t = routes.T
    resid, outgoing = mixer(
        tokens_here, group_weight, group_scale, out_weight, stream, ffn_gain, routes_t,
        expert_count, capacity,
    )
    arrived = lax.all_to_all(
        outgoing.reshape(expert_count, capacity, model_width),
        ("sp", "tp"), split_axis=0, concat_axis=0, tiled=True,
    ).reshape(expert_count * capacity, model_width)
    results = run_expert(arrived, expert_gate[0], expert_up[0], expert_down[0])
    returned = lax.all_to_all(
        results.reshape(expert_count, capacity, model_width),
        ("sp", "tp"), split_axis=0, concat_axis=0, tiled=True,
    ).reshape(expert_count * capacity, model_width)
    return combine(resid, returned, routes_t, route_weights.T, expert_count, capacity)


def solution(mesh):
    in_specs = (
        P(("sp", "tp"), None),
        P("sp", "tp"),
        P("sp"),
        P(),
        P(),
        P(),
        P(),
        P(("sp", "tp"), None),
        P(("sp", "tp"), None),
        P(("sp", "tp"), None, None),
        P(("sp", "tp"), None, None),
        P(("sp", "tp"), None, None),
    )
    out_specs = P(("sp", "tp"), None)
    return jax.shard_map(body, mesh=mesh, in_specs=in_specs, out_specs=out_specs, check_vma=False)
```

time: 278 us -> 200 us (0.72)
  waiting for transfers between devices: 71.6 us -> 1.42 us
  blocking collectives: 117 us -> 164 us
  other arithmetic: 30.6 us -> 0.77 us
  local copies, waits for them, and re-layouts: 28.6 us -> 2.19 us
  Pallas kernels: 0 us -> 15.5 us
  matrix products: 18.7 us -> 11.2 us
  starting transfers between devices: 8.13 us -> 4.87 us
    all_to_all x0 -> x2, blocking collectives: none -> 87 us  [the longest x1 74.7 us: body(): lax.all_to_all(results.reshape(expert_count, capacity, model_width), ('sp...]
    all_to_all x2 -> x0, waiting for transfers between devices: 71.6 us -> none  [the longest x1 71.2 us: body(): lax.all_to_all(results, ('sp', 'tp'), split_axis=0, concat_axis=0, tiled=...]
    all_gather x1 -> x0, blocking collectives: 30.5 us -> none  [carried_in(): pieces = jax.tree.map(lambda part: lax.all_gather(part, axis), value)]
    convert_element_type x5 -> x1, other arithmetic: 18.5 us -> 0.76 us  [body(): tail_docs = (segments[row_count - rim:] + 1).astype(jnp.bfloat16)]
    pallas_call x0 -> x3, Pallas kernels: none -> 15.5 us  [the longest x1 8.76 us: mixer(): pl.pallas_call(functools.partial(mixer_kernel, capacity=capacity, experts...]
    unnamed x1 -> x0, blocking collectives: 13.1 us -> none
    gather x2 -> x0, local copies, waits for them, and re-layouts: 11.8 us -> none  [the longest x1 7.56 us: body(): picked = returned.reshape(expert_count * capacity, model_width)[slot_index]]
    all_to_all x2 -> x0, starting transfers between devices: 8.13 us -> none  [the longest x1 4.14 us: body(): lax.all_to_all(mixed, 'tp', split_axis=0, concat_axis=1, tiled=True)]
  transfers between devices with their start and end apart: 2 -> 1, of which waited for: 2 -> 1; matrix products, arithmetic and copies ran while one was open for 3% -> 0% of each run, Pallas kernels for 0% -> 0%
where the time goes in v1:
time: 200 us
  blocking collectives  164 us (82%)
  Pallas kernels  15.5 us (8%)
  matrix products  11.2 us (6%)
  starting transfers between devices  4.87 us (2%)
  local copies, waits for them, and re-layouts  2.19 us (1%)
    all_to_all x1, blocking collectives, body(): lax.all_to_all(outgoing.reshape(expert_count, capacity, model_width), ('s...  76.9 us
    all_to_all x1, blocking collectives, body(): lax.all_to_all(results.reshape(expert_count, capacity, model_width), ('sp...  74.7 us
    all_to_all x1, blocking collectives, body(): lax.all_to_all(mixed, 'tp', split_axis=0, concat_axis=1, tiled=True)  12.3 us
    dot_general x3, matrix products, dot32(): return jnp.dot(a, b, preferred_element_type=jnp.float32)  11.2 us
    pallas_call x1, Pallas kernels, mixer(): pl.pallas_call(functools.partial(mixer_kernel, capacity=capacity, experts...  8.76 us
    ppermute x1, starting transfers between devices, body(): lax.ppermute(payload, 'sp', [(i, i + 1) for i in range(sp_count - 1)])  4.87 us
    pallas_call x1, Pallas kernels, combine(): pl.pallas_call(functools.partial(combine_kernel, capacity=capacity, exper...  4.41 us
  transfers between devices with their start and end apart: 1, of which 1 were waited for; matrix products, arithmetic and copies ran while one was open for 0% of the time, Pallas kernels for 0%

profile of v1, /device:TPU:0, one launch (start us, length us, event | category | flops | bytes accessed | tf_op | source)
XLA Modules:
  0.0 199.9 jit_solution(11055199929855051807)
XLA Ops:
  0.0 0.8 add_convert_fusion
  0.8 0.7 slice.7
  1.5 4.9 %collective-permute-start = (bf16[16,512]{1,0:T(8,128)(2,1)S(1)}, bf16[16,512]{1,0:T(8,128)(2,1)S(1)}, u32[]{:S(2)}, u32[]{:S(2)}) collective-permute-start(bf16[16,512]{1,0:T(8,128)(2,1)S(1)} %pad_maximum_fusion), channel_id=1, source_target_pairs={{0,4},{4,8},{8,12},{12,16},{16,20},{20,24},{24,28},{1,5},{5,9},{9,... | collective-permute-start | bytes 49160 | tf_op jit(solution)/shard_map/ppermute | solution.py:210
  6.4 1.4 collective-permute-done.rim_ref
  7.8 0.0 copy-start
  7.8 0.6 copy-done
  8.4 2.3 %pool.1 = bf16[512,512]{1,0:T(8,128)(2,1)} custom-call(s32[1]{0:T(128)} %bitcast.first_ref, bf16[16,512]{1,0:T(8,128)(2,1)} %copy-done, bf16[512,512]{1,0:T(8,128)(2,1)} %rows_ref.1, s32[1,512]{1,0:T(1,128)} %bitcast.43), custom_call_target="tpu_custom_call" | custom-call | tf_op jit(solution)/shard_map/pool/pallas_call | solution.py:64
  10.8 12.3 %all_to_all.29 = bf16[4,128,512]{2,1,0:T(8,128)(2,1)S(1)} all-to-all(bf16[4,128,512]{2,1,0:T(8,128)(2,1)} %bitcast.36), channel_id=1, replica_groups=mesh['sp'=8,'tp'=4] {'tp'}, dimensions={0} | all-to-all | bytes 1048576 | tf_op jit(solution)/shard_map/all_to_all | solution.py:213
  23.0 0.8 copy.15
  23.9 8.8 %mixer.1 = (bf16[128,2048]{1,0:T(8,128)(2,1)}, bf16[768,2048]{1,0:T(8,128)(2,1)}) custom-call(bf16[128,2048]{1,0:T(8,128)(2,1)} %bitcast.35, bf16[4,512,512]{2,1,0:T(8,128)(2,1)} %gw_ref.1, f32[1,2048]{1,0:T(1,128)} %bitcast.40, bf16[2048,2048]{1,0:T(8,128)(2,1)} %ow_ref.1, bf16[128,2048]{1,0:T(8,128)(2,1)} %stream_ref.1, f32[1,2048]{1,0:T(1,128)} %bitcast.41, ...), custom_call_target="tpu_custom_call" | custom-call | tf_op jit(solution)/shard_map/mixer/pallas_call | solution.py:127
  32.6 0.0 copy-start.1
  32.6 76.9 %all_to_all.30 = bf16[32,24,2048]{2,1,0:T(8,128)(2,1)S(1)} all-to-all(bf16[32,24,2048]{2,1,0:T(8,128)(2,1)} %bitcast.31), channel_id=1, replica_groups=mesh['sp'=8,'tp'=4] {'sp','tp'}, dimensions={0} | all-to-all | bytes 6291456 | tf_op jit(solution)/shard_map/all_to_all | solution.py:222
  109.5 0.0 copy-done.1
  109.5 0.0 copy-start.2
  109.5 3.4 %fusion.2 = f32[768,1024]{1,0:T(8,128)S(1)} fusion(bf16[768,2048]{1,0:T(8,128)(2,1)S(1)} %bitcast.32, bf16[1,2048,1024]{2,1,0:T(8,128)(2,1)S(1)} %copy-done.1), kind=kOutput, calls=%fused_computation.2 | convolution fusion | flops 3221225472 | bytes 10485760 | tf_op jit(solution)/shard_map/dot_general | solution.py:20
  112.9 0.0 copy-done.2
  112.9 0.0 copy-start.3
  112.9 4.1 %multiply_convert_fusion = bf16[768,1024]{1,0:T(8,128)(2,1)S(1)} fusion(f32[768,1024]{1,0:T(8,128)S(1)} %fusion.2, bf16[768,2048]{1,0:T(8,128)(2,1)S(1)} %bitcast.33, bf16[1,2048,1024]{2,1,0:T(8,128)(2,1)S(1)} %copy-done.2), kind=kOutput, calls=%fused_computation.7 | convolution fusion | flops 3229089792 | bytes 12058624 | tf_op jit(solution)/shard_map/dot_general | solution.py:20
  117.1 0.0 copy-done.3
  117.1 3.6 %fusion.6 = bf16[768,2048]{1,0:T(8,128)(2,1)S(1)} fusion(bf16[768,1024]{1,0:T(8,128)(2,1)S(1)} %multiply_convert_fusion, bf16[1,1024,2048]{2,1,0:T(8,128)(2,1)S(1)} %copy-done.3), kind=kOutput, calls=%fused_computation.6 | convolution fusion | flops 3222798336 | bytes 8912896 | tf_op jit(solution)/shard_map/dot_general | solution.py:20
  120.7 74.7 %all_to_all.31 = bf16[32,24,2048]{2,1,0:T(8,128)(2,1)} all-to-all(bf16[32,24,2048]{2,1,0:T(8,128)(2,1)S(1)} %bitcast.34), channel_id=1, replica_groups=mesh['sp'=8,'tp'=4] {'sp','tp'}, dimensions={0} | all-to-all | bytes 6291456 | tf_op jit(solution)/shard_map/all_to_all | solution.py:227
  195.5 4.4 %combine.1 = bf16[128,2048]{1,0:T(8,128)(2,1)} custom-call(bf16[128,2048]{1,0:T(8,128)(2,1)} %get-tuple-element.7.resid_ref, bf16[768,2048]{1,0:T(8,128)(2,1)} %bitcast.30, s32[4,128]{1,0:T(4,128)} %bitcast.39, f32[4,128]{1,0:T(4,128)} %bitcast.42), custom_call_target="tpu_custom_call" | custom-call | tf_op jit(solution)/shard_map/combine/pallas_call | solution.py:161
  (3 shorter events, 0.0 us)
Async XLA Ops:
  1.5 6.3 %collective-permute-start = (bf16[16,512]{1,0:T(8,128)(2,1)S(1)}, bf16[16,512]{1,0:T(8,128)(2,1)S(1)}, u32[]{:S(2)}, u32[]{:S(2)}) collective-permute-start(bf16[16,512]{1,0:T(8,128)(2,1)S(1)} %pad_maximum_fusion), channel_id=1, source_target_pairs={{0,4},{4,8},{8,12},{12,16},{16,20},{20,24},{24,28},{1,5},{5,9},{9,... | collective-permute-start | bytes 49160 | tf_op jit(solution)/shard_map/ppermute | solution.py:210
  7.8 0.6 copy-start
  32.6 76.9 %copy-start.1 = (bf16[1,2048,1024]{2,1,0:T(8,128)(2,1)S(1)}, bf16[1,2048,1024]{2,1,0:T(8,128)(2,1)}, u32[]{:S(2)}) copy-start(bf16[1,2048,1024]{2,1,0:T(8,128)(2,1)} %param.22) | copy-start | bytes 12582916
  109.5 3.5 %copy-start.2 = (bf16[1,2048,1024]{2,1,0:T(8,128)(2,1)S(1)}, bf16[1,2048,1024]{2,1,0:T(8,128)(2,1)}, u32[]{:S(2)}) copy-start(bf16[1,2048,1024]{2,1,0:T(8,128)(2,1)} %param.21) | copy-start | bytes 12582916
  112.9 4.2 %copy-start.3 = (bf16[1,1024,2048]{2,1,0:T(8,128)(2,1)S(1)}, bf16[1,1024,2048]{2,1,0:T(8,128)(2,1)}, u32[]{:S(2)}) copy-start(bf16[1,1024,2048]{2,1,0:T(8,128)(2,1)} %param.23) | copy-start | bytes 12582916

commit v2 on v1

v2 whole, which is shorter than its diff:
```python
import functools

import jax
import jax.numpy as jnp
from jax import lax
from jax.experimental import pallas as pl
from jax.experimental.pallas import tpu as pltpu
from jax.sharding import PartitionSpec as P


GROUPS = 4

norm_eps = 1e-05
clamp_limit = 7.0
sigmoid_alpha = 1.702
longest_window = 16
VMEM_BYTES = 12 * 1024 * 1024
EXPERT_BYTES = 30 * 1024 * 1024


def dot32(a, b):
    return jnp.dot(a, b, preferred_element_type=jnp.float32)


def pool_kernel(
    place_ref, rim_ref, rows_ref, docs_ref, *refs, group_width,
):
    out_refs, ext_ref = refs[:-1], refs[-1]
    _, channels = rows_ref.shape
    rim = rim_ref.shape[0]
    block = out_refs[0].shape[0]
    group, mine, edge = place_ref[0], place_ref[1], place_ref[2]
    groups_here = max(1, channels // group_width)
    width = channels // groups_here
    wide = block + rim
    ext_ref[0:rim, :] = rim_ref[...]
    ext_ref[rim:, :] = rows_ref[...]
    rim_docs = (rim_ref[0:1, 0:rim].astype(jnp.float32) - 1.0).astype(jnp.int32)
    rim_docs = jnp.where(edge == 0, -1, rim_docs)
    at_row = lax.broadcasted_iota(jnp.int32, (block, wide), 0)
    at_col = lax.broadcasted_iota(jnp.int32, (block, wide), 1)
    back = at_row + rim - at_col
    for d in range(len(out_refs)):
        index = mine ^ d
        here = docs_ref[pl.ds(index, 1), :]
        previous = docs_ref[pl.ds(jnp.maximum(index - 1, 0), 1), :][:, block - rim :]
        before = jnp.where(index == 0, rim_docs, previous)
        col_docs = jnp.concatenate([before, here], 1)
        row_docs = jnp.sum(
            jnp.where(back == 0, jnp.broadcast_to(col_docs, (block, wide)), 0), 1, keepdims=True
        )
        alike = (col_docs == row_docs) & (back >= 0)
        start = pl.multiple_of(index * block, block)
        values = ext_ref[pl.ds(start, wide), :]
        own = values[rim:, :].astype(jnp.float32)
        for part in range(groups_here):
            window = jnp.left_shift(2, group + part)
            band = jnp.where(alike & (back < window), 1.0, 0.0)
            count = jnp.sum(band, 1, keepdims=True)
            lanes = slice(part * width, (part + 1) * width)
            total = dot32(band.astype(jnp.bfloat16), values[:, lanes])
            out_refs[d][:, lanes] = (total / count - own[:, lanes]).astype(jnp.bfloat16)


def named_experts(routes_t, plane, count):
    experts = lax.broadcasted_iota(jnp.int32, (count, routes_t.shape[1]), 0)
    here = experts + plane * count
    return [routes_t[j : j + 1, :] == here for j in range(routes_t.shape[0])]


def slot_table(matches, capacity):
    count, tokens = matches[0].shape
    named = matches[0]
    for match in matches[1:]:
        named = named | match
    earlier = (
        lax.broadcasted_iota(jnp.int32, (tokens, tokens), 0)
        < lax.broadcasted_iota(jnp.int32, (tokens, tokens), 1)
    )
    ones = jnp.where(named, 1.0, 0.0)
    rank = dot32(ones.astype(jnp.bfloat16), jnp.where(earlier, 1.0, 0.0).astype(jnp.bfloat16))
    held = jnp.where(named, rank, -1.0).astype(jnp.bfloat16)
    slots = count * capacity
    low = lax.broadcasted_iota(jnp.int32, (slots, count), 1) * capacity
    slot = lax.broadcasted_iota(jnp.int32, (slots, count), 0)
    inside = (slot >= low) & (slot < low + capacity)
    spread = jnp.where(inside, 1.0, 0.0).astype(jnp.bfloat16)
    place = jnp.sum(jnp.where(inside, slot - low, 0), 1, keepdims=True).astype(jnp.float32)
    return dot32(spread, held) == place, spread


def pick_rows(where_ref, routes_t, rows, send_ref, capacity):
    count = send_ref.shape[0] // capacity
    taken, _ = slot_table(named_experts(routes_t, where_ref[0], count), capacity)
    send_ref[...] = dot32(jnp.where(taken, 1.0, 0.0).astype(jnp.bfloat16), rows).astype(
        jnp.bfloat16
    )


def mixer_kernel(
    where_ref, table_ref, gs_ref, stream_ref, gain_ref, *refs, capacity,
):
    block_refs = refs[:-9]
    gw_src, ow_src, resid_ref, chunk_ref, send_ref, mixed_ref, gw_ref, ow_ref, sems = refs[-9:]
    groups, width, _ = gw_ref.shape

    def piece(g):
        rows = pl.ds(g * width, width)
        return (
            pltpu.make_async_copy(gw_src.at[g], gw_ref.at[g], sems.at[0, g]),
            pltpu.make_async_copy(ow_src.at[rows, :], ow_ref.at[rows, :], sems.at[1, g]),
        )

    for k in range(2):
        for g in range(groups):
            piece(g)[k].start()
    tokens, _ = block_refs[0].shape
    for d in range(len(block_refs)):
        mixed_ref[where_ref[1] ^ d] = block_refs[d][...]
    mixed = jnp.concatenate([mixed_ref[d] for d in range(len(block_refs))], 1)
    parts = []
    for g in range(groups):
        lanes = slice(g * width, (g + 1) * width)
        piece(g)[0].wait()
        grouped = dot32(mixed[:, lanes], gw_ref[g])
        parts.append((grouped * gs_ref[:, lanes]).astype(jnp.bfloat16))
    mixer_out = jnp.zeros((tokens, stream_ref.shape[1]), jnp.float32)
    for g in range(groups):
        piece(g)[1].wait()
        mixer_out = mixer_out + dot32(parts[g], ow_ref[g * width : (g + 1) * width, :])
    resid = (stream_ref[...].astype(jnp.float32) + mixer_out).astype(jnp.bfloat16)
    resid_ref[...] = resid
    values = resid.astype(jnp.float32)
    inverse = lax.rsqrt(jnp.mean(values * values, -1, keepdims=True) + norm_eps)
    normed = (values * inverse * gain_ref[...]).astype(jnp.bfloat16)
    chunk_ref[0:tokens, :] = normed
    top = table_ref.shape[0] // 2
    weights = table_ref[top:, :]
    high = weights.astype(jnp.bfloat16)
    low = (weights - high.astype(jnp.float32)).astype(jnp.bfloat16)
    routes_t = table_ref[0:top, :]
    lines = [piece.astype(jnp.float32)[j : j + 1, :] for piece in (routes_t, high, low)
             for j in range(top)]
    line = jnp.concatenate(lines, 1)
    line = jnp.pad(line, ((0, 0), (0, chunk_ref.shape[1] - line.shape[1])))
    rest = chunk_ref.shape[0] - tokens
    chunk_ref[tokens:, :] = jnp.broadcast_to(line, (rest, line.shape[1])).astype(jnp.bfloat16)
    pick_rows(where_ref, routes_t.astype(jnp.int32), normed, send_ref, capacity)


def read_table(chunk_ref, tokens, top):
    line = chunk_ref[tokens:, :].astype(jnp.float32)
    rows = [line[0:1, j * tokens : (j + 1) * tokens] for j in range(3 * top)]
    pieces = [jnp.concatenate(rows[k * top : (k + 1) * top], 0) for k in range(3)]
    return pieces[0].astype(jnp.int32), pieces[1], pieces[2]


def call(kernel, shapes, args, flops, scratch=(), limit=VMEM_BYTES, in_hbm=0):
    specs = [pl.BlockSpec(memory_space=pltpu.SMEM)]
    specs += [pl.BlockSpec(memory_space=pltpu.VMEM)] * (len(args) - 1 - in_hbm)
    specs += [pl.BlockSpec(memory_space=pltpu.HBM)] * in_hbm
    return pl.pallas_call(
        kernel,
        out_shape=tuple(shapes),
        in_specs=specs,
        out_specs=(pl.BlockSpec(memory_space=pltpu.VMEM),) * len(shapes),
        scratch_shapes=scratch,
        compiler_params=pltpu.CompilerParams(vmem_limit_bytes=limit),
        cost_estimate=pl.CostEstimate(
            flops=flops, transcendentals=0, bytes_accessed=sum(a.nbytes for a in args)
        ),
    )(*args)


def pick_kernel(where_ref, chunk_ref, send_ref, *, tokens, top, capacity):
    routes_t, _, _ = read_table(chunk_ref, tokens, top)
    pick_rows(where_ref, routes_t, chunk_ref[0:tokens, :], send_ref, capacity)


def weighted_sum(where_ref, routes_t, weights, back, capacity):
    count = back.shape[0] // capacity
    matches = named_experts(routes_t, where_ref[0], count)
    taken, spread = slot_table(matches, capacity)
    total = jnp.zeros((routes_t.shape[1], back.shape[1]), jnp.float32)
    for piece in weights:
        weight = jnp.zeros(matches[0].shape, jnp.float32)
        for j, match in enumerate(matches):
            weight = weight + jnp.where(match, piece[j : j + 1, :], 0.0)
        factor = jnp.where(taken, dot32(spread, weight.astype(jnp.bfloat16)), 0.0)
        total = total + lax.dot_general(
            factor.astype(jnp.bfloat16), back, (((0,), (0,)), ((), ())),
            preferred_element_type=jnp.float32,
        )
    return total


def partial_kernel(where_ref, chunk_ref, back_ref, *refs, tokens, top, capacity):
    routes_t, high, low = read_table(chunk_ref, tokens, top)
    total = weighted_sum(where_ref, routes_t, (high, low), back_ref[...], capacity)
    for ref in refs[:-1]:
        total = total + ref[...].astype(jnp.float32)
    refs[-1][...] = total.astype(jnp.bfloat16)


def final_kernel(where_ref, chunk_ref, resid_ref, back_ref, *refs, tokens, top, capacity):
    routes_t, high, low = read_table(chunk_ref, tokens, top)
    total = weighted_sum(where_ref, routes_t, (high, low), back_ref[...], capacity)
    total = total + resid_ref[...].astype(jnp.float32)
    for ref in refs[:-1]:
        total = total + ref[...].astype(jnp.float32)
    refs[-1][...] = total.astype(jnp.bfloat16)


WEIGHT_CUTS = 4
in_hbm = functools.partial(pltpu.with_memory_space_constraint, memory_space=pltpu.HBM)


def expert_kernel(where_ref, *refs, inputs):
    row_refs, sources = refs[:inputs], refs[inputs : inputs + 3]
    out_refs = refs[inputs + 3 : 2 * inputs + 3]
    stores, sems = refs[2 * inputs + 3 : -1], refs[-1]
    gate_ref, up_ref, down_ref = stores

    def piece(k, b):
        size = stores[k].shape[0] // WEIGHT_CUTS
        part = pl.ds(b * size, size)
        return pltpu.make_async_copy(
            sources[k].at[0, part, :], stores[k].at[part, :], sems.at[k, b]
        )

    for b in range(WEIGHT_CUTS):
        piece(0, b).start()
        piece(1, b).start()
    for b in range(WEIGHT_CUTS):
        piece(2, b).start()
    rows = jnp.concatenate([ref[...] for ref in row_refs], 0)
    size = rows.shape[1] // WEIGHT_CUTS
    gate_value = up_value = None
    for b in range(WEIGHT_CUTS):
        lanes = slice(b * size, (b + 1) * size)
        piece(0, b).wait()
        part = dot32(rows[:, lanes], gate_ref[lanes, :])
        gate_value = part if b == 0 else gate_value + part
        piece(1, b).wait()
        part = dot32(rows[:, lanes], up_ref[lanes, :])
        up_value = part if b == 0 else up_value + part
    gated = jnp.minimum(gate_value, clamp_limit)
    linear = jnp.clip(up_value, -clamp_limit, clamp_limit)
    activated = (gated * jax.nn.sigmoid(sigmoid_alpha * gated) * (linear + 1.0)).astype(
        jnp.bfloat16
    )
    size = activated.shape[1] // WEIGHT_CUTS
    total = None
    for b in range(WEIGHT_CUTS):
        lanes = slice(b * size, (b + 1) * size)
        piece(2, b).wait()
        part = dot32(activated[:, lanes], down_ref[lanes, :])
        total = part if b == 0 else total + part
    result = total.astype(jnp.bfloat16)
    length = row_refs[0].shape[0]
    for i in range(inputs):
        out_refs[i][...] = result[i * length : (i + 1) * length]


def body(
    stream,
    projected,
    segments,
    group_weight,
    group_scale,
    out_weight,
    ffn_gain,
    routes,
    route_weights,
    expert_gate,
    expert_up,
    expert_down,
    *,
    planes,
):
    row_count, channels = projected.shape
    tp_count = lax.axis_size("tp")
    sp_count = lax.axis_size("sp")
    width = channels * tp_count
    group_width = width // GROUPS
    tokens, top = routes.shape
    devices = sp_count * tp_count
    count = devices // planes
    capacity = 3 * tokens * top // (2 * devices)
    hidden = expert_gate.shape[2]
    every = ("sp", "tp")
    sp_index, tp_index = lax.axis_index("sp"), lax.axis_index("tp")
    plane = (sp_index * tp_count + tp_index) // count
    where = jnp.stack([plane, tp_index]).astype(jnp.int32)
    place = jnp.stack([tp_index * channels // group_width, tp_index, sp_index]).astype(jnp.int32)
    sizes = dict(tokens=tokens, top=top, capacity=capacity)

    def hop(value):
        pairs = [(i, (i + count) % devices) for i in range(devices)]
        return lax.ppermute(value, every, pairs)

    planes_of = [list(range(p * count, (p + 1) * count)) for p in range(planes)]

    def in_plane(rows):
        blocks = rows.reshape(count, capacity, width)
        moved = lax.all_to_all(
            blocks, every, split_axis=0, concat_axis=0, axis_index_groups=planes_of,
            tiled=True,
        )
        return moved.reshape(count * capacity, width)

    rim = longest_window
    tail_docs = (segments[row_count - rim :] + 1).astype(jnp.bfloat16)
    payload = jnp.concatenate(
        [
            jnp.pad(tail_docs, (0, channels - rim))[None, :],
            projected[row_count - rim + 1 :],
        ],
        0,
    )
    before = lax.ppermute(payload, "sp", [(i, (i + 1) % sp_count) for i in range(sp_count)])
    mixed = call(
        functools.partial(pool_kernel, group_width=group_width),
        [jax.ShapeDtypeStruct((tokens, channels), jnp.bfloat16)] * tp_count,
        [place, before, projected, segments.reshape(tp_count, tokens)],
        2 * row_count * channels * (tokens + rim),
        [pltpu.VMEM((row_count + rim, channels), jnp.bfloat16)],
    )
    blocks = [mixed[0]]
    for d in range(1, tp_count):
        pairs = [(i, i ^ d) for i in range(tp_count)]
        blocks.append(lax.ppermute(mixed[d], "tp", pairs))
    table = jnp.concatenate([routes.T.astype(jnp.float32), route_weights.T], 0)

    shape = jax.ShapeDtypeStruct((tokens, width), jnp.bfloat16)
    slots = jax.ShapeDtypeStruct((count * capacity, width), jnp.bfloat16)
    resid, chunk, rows = call(
        functools.partial(mixer_kernel, capacity=capacity),
        [shape, jax.ShapeDtypeStruct((tokens + 8, width), jnp.bfloat16), slots],
        [
            where, table, group_scale.reshape(1, -1), stream, ffn_gain.reshape(1, -1),
            *blocks, in_hbm(group_weight), in_hbm(out_weight),
        ],
        2 * tokens * width * (width + group_width),
        [
            pltpu.VMEM((tp_count, tokens, channels), jnp.bfloat16),
            pltpu.VMEM(group_weight.shape, jnp.bfloat16),
            pltpu.VMEM(out_weight.shape, jnp.bfloat16),
            pltpu.SemaphoreType.DMA((2, GROUPS)),
        ],
        EXPERT_BYTES,
        2,
    )
    small = 2 * tokens * count * capacity * width

    def run_experts(groups):
        matrices = [in_hbm(expert_gate), in_hbm(expert_up), in_hbm(expert_down)]
        return call(
            functools.partial(expert_kernel, inputs=len(groups)),
            [slots] * len(groups),
            [where, *groups, *matrices],
            6 * len(groups) * groups[0].size * hidden,
            [
                pltpu.VMEM((width, hidden), jnp.bfloat16),
                pltpu.VMEM((width, hidden), jnp.bfloat16),
                pltpu.VMEM((hidden, width), jnp.bfloat16),
                pltpu.SemaphoreType.DMA((3, WEIGHT_CUTS)),
            ],
            EXPERT_BYTES,
            3,
        )

    chunks = [chunk]
    arrived = [in_plane(rows)]
    for s in range(1, planes):
        chunks.append(hop(chunks[-1]))
        (rows,) = call(functools.partial(pick_kernel, **sizes), [slots], [where, chunks[s]], small)
        arrived.append(in_plane(rows))
    first = min(2, planes)
    results = list(run_experts(arrived[:first]))
    for s in range(first, planes):
        results += run_experts([arrived[s]])
    carried = []
    for s in range(1, planes):
        back = in_plane(results[s])
        (part,) = call(
            functools.partial(partial_kernel, **sizes),
            [shape], [where, chunks[s], back, *carried], 2 * small,
        )
        carried = [hop(part)]
    back = in_plane(results[0])
    (out,) = call(
        functools.partial(final_kernel, **sizes),
        [shape], [where, chunk, resid, back, *carried], 2 * small,
    )
    return out


def plane_count(mesh):
    sizes = mesh.shape
    heights = {getattr(d, "coords", (0, 0, -1))[2] for d in mesh.devices.flat}
    if -1 in heights:
        return max(1, sizes["sp"] // max(1, sizes["tp"] // 2))
    return len(heights)


def solution(mesh):
    in_specs = (
        P(("sp", "tp"), None),
        P("sp", "tp"),
        P("sp"),
        P(),
        P(),
        P(),
        P(),
        P(("sp", "tp"), None),
        P(("sp", "tp"), None),
        P(("sp", "tp"), None, None),
        P(("sp", "tp"), None, None),
        P(("sp", "tp"), None, None),
    )
    out_specs = P(("sp", "tp"), None)
    planes = plane_count(mesh)

    def layer(*args):
        return body(*args, planes=planes)

    return jax.shard_map(layer, mesh=mesh, in_specs=in_specs, out_specs=out_specs, check_vma=False)
```

time: 200 us -> 191 us (0.955)
  blocking collectives: 164 us -> 0 us
  waiting for transfers between devices: 1.42 us -> 97.5 us
  starting transfers between devices: 4.87 us -> 34.4 us
  Pallas kernels: 15.5 us -> 44.5 us
  matrix products: 11.2 us -> 0 us
  local copies, waits for them, and re-layouts: 2.19 us -> 11.4 us
    all_to_all x3 -> x0, blocking collectives: 164 us -> none  [the longest x1 76.9 us: body(): lax.all_to_all(outgoing.reshape(expert_count, capacity, model_width), ('s...]
    ppermute x1 -> x10, waiting for transfers between devices: 1.42 us -> 83.6 us  [the longest x6 74.1 us: hop(): return lax.ppermute(value, every, pairs)]
    all_to_all x0 -> x8, starting transfers between devices: none -> 29.3 us  [in_plane(): lax.all_to_all(blocks, every, split_axis=0, concat_axis=0, axis_index_gro...]
    pallas_call x3 -> x12, Pallas kernels: 15.5 us -> 44.5 us  [call(): pl.pallas_call(kernel, out_shape=tuple(shapes), in_specs=specs, out_specs...]
    all_to_all x0 -> x8, waiting for transfers between devices: none -> 13.8 us  [in_plane(): lax.all_to_all(blocks, every, split_axis=0, concat_axis=0, axis_index_gro...]
    dot_general x3 -> x0, matrix products: 11.2 us -> none  [dot32(): return jnp.dot(a, b, preferred_element_type=jnp.float32)]
    unnamed x8 -> x30, local copies, waits for them, and re-layouts: 0.61 us -> 10.7 us
    ppermute x1 -> x10, starting transfers between devices: 4.87 us -> 5.12 us  [the longest x1 3.02 us: body(): lax.ppermute(payload, 'sp', [(i, (i + 1) % sp_count) for i in range(sp_co...]
  transfers between devices with their start and end apart: 1 -> 18, of which waited for: 1 -> 14; matrix products, arithmetic and copies ran while one was open for 0% -> 1% of each run, Pallas kernels for 0% -> 18%
where the time goes in v2:
time: 191 us; the launch traced here: 190 us
  waiting for transfers between devices  97.5 us (51%)
  Pallas kernels  44.5 us (23%)
  starting transfers between devices  34.4 us (18%)
  local copies, waits for them, and re-layouts  11.4 us (6%)
  other arithmetic  2.29 us (1%)
    ppermute x6, waiting for transfers between devices, hop(): return lax.ppermute(value, every, pairs)  74.1 us
    pallas_call x12, Pallas kernels, call(): pl.pallas_call(kernel, out_shape=tuple(shapes), in_specs=specs, out_specs...  44.5 us
    all_to_all x8, starting transfers between devices, in_plane(): lax.all_to_all(blocks, every, split_axis=0, concat_axis=0, axis_index_gro...  29.3 us
    all_to_all x8, waiting for transfers between devices, in_plane(): lax.all_to_all(blocks, every, split_axis=0, concat_axis=0, axis_index_gro...  13.8 us
    unnamed x30, local copies, waits for them, and re-layouts  10.7 us
    ppermute x3, waiting for transfers between devices, body(): blocks.append(lax.ppermute(mixed[d], 'tp', pairs))  5.55 us
    ppermute x1, waiting for transfers between devices, body(): lax.ppermute(payload, 'sp', [(i, (i + 1) % sp_count) for i in range(sp_co...  4 us
  transfers between devices with their start and end apart: 18, of which 14 were waited for; matrix products, arithmetic and copies ran while one was open for 1% of the time, Pallas kernels for 18%

profile of v2, /device:TPU:0, one launch (start us, length us, event | category | flops | bytes accessed | tf_op | source)
XLA Modules:
  0.0 190.3 jit_solution(7837964790958991315)
XLA Ops:
  0.0 0.7 slice.7
  0.7 0.8 add_convert_fusion
  1.5 3.0 %collective-permute-start = (bf16[16,512]{1,0:T(8,128)(2,1)S(1)}, bf16[16,512]{1,0:T(8,128)(2,1)S(1)}, u32[]{:S(2)}, u32[]{:S(2)}) collective-permute-start(bf16[16,512]{1,0:T(8,128)(2,1)S(1)} %pad_maximum_fusion), channel_id=1, source_target_pairs={{0,4},{4,8},{8,12},{12,16},{16,20},{20,24},{24,28},{28,0},{1,5},{5... | collective-permute-start | bytes 49160 | tf_op jit(solution)/shard_map/ppermute | solution.py:321
  5.3 4.0 %collective-permute-done.rim_ref = bf16[16,512]{1,0:T(8,128)(2,1)S(1)} collective-permute-done((bf16[16,512]{1,0:T(8,128)(2,1)S(1)}, bf16[16,512]{1,0:T(8,128)(2,1)S(1)}, u32[]{:S(2)}, u32[]{:S(2)}) %collective-permute-start) | collective-permute-done | bytes 16416 | tf_op jit(solution)/shard_map/ppermute | solution.py:321
  9.3 1.0 copy-done.8
  11.0 1.1 shard_map.118
  12.2 1.8 collective-permute-start.2
  14.8 3.8 %collective-permute-done.2.refs_2_ = bf16[128,512]{1,0:T(8,128)(2,1)S(1)} collective-permute-done((bf16[128,512]{1,0:T(8,128)(2,1)S(1)}, bf16[128,512]{1,0:T(8,128)(2,1)S(1)}, u32[]{:S(2)}, u32[]{:S(2)}) %collective-permute-start.2) | collective-permute-done | bytes 131104 | tf_op jit(solution)/shard_map/ppermute | solution.py:332
  18.6 1.7 collective-permute-done.3.refs_3_
  20.3 1.0 copy-done.11
  21.4 0.7 copy-done.12
  22.8 6.6 %shard_map.119 = (bf16[128,2048]{1,0:T(8,128)(2,1)S(1)}, bf16[136,2048]{1,0:T(8,128)(2,1)S(1)}, bf16[192,2048]{1,0:T(8,128)(2,1)}) custom-call(s32[2]{0:T(128)S(1)} %pad_add_fusion.where_ref, f32[8,128]{1,0:T(8,128)S(1)} %pad_maximum_fusion.1.table_ref, f32[1,2048]{1,0:T(1,128)S(1)} %bitcast.36, bf16[128,2048]{1,0:T(8,128)(2,1)S(1)} %copy-done.11, ...), custom_call_target="tpu_custom_call" | custom-call | flops 1342177280 | bytes 11554824 | tf_op jit(solution)/shard_map/pallas_call | solution.py:162
  29.4 0.8 copy-done.9
  30.2 3.5 %all-to-all-start = ((bf16[8,24,2048]{2,1,0:T(8,128)(2,1)}), bf16[8,24,2048]{2,1,0:T(8,128)(2,1)S(1)}, u32[]{:S(2)}, u32[]{:S(2)}) async-start(bf16[8,24,2048]{2,1,0:T(8,128)(2,1)} %bitcast.9), calls=%async_computation | async-start | bytes 1572864 | tf_op jit(solution)/shard_map/all_to_all | solution.py:306
  33.8 16.7 %collective-permute-done.4.chunk_ref = bf16[136,2048]{1,0:T(8,128)(2,1)S(1)} collective-permute-done((bf16[136,2048]{1,0:T(8,128)(2,1)S(1)}, bf16[136,2048]{1,0:T(8,128)(2,1)S(1)}, u32[]{:S(2)}, u32[]{:S(2)}) %collective-permute-start.4) | collective-permute-done | bytes 557088 | tf_op jit(solution)/shard_map/ppermute | solution.py:300
  50.5 2.0 %shard_map.120 = bf16[192,2048]{1,0:T(8,128)(2,1)} custom-call(s32[2]{0:T(128)S(1)} %pad_add_fusion.where_ref, bf16[136,2048]{1,0:T(8,128)(2,1)S(1)} %collective-permute-done.4.chunk_ref), custom_call_target="tpu_custom_call" | custom-call | flops 100663296 | bytes 557064 | tf_op jit(solution)/shard_map/pallas_call | solution.py:162
  52.5 3.9 %all-to-all-start.1 = ((bf16[8,24,2048]{2,1,0:T(8,128)(2,1)}), bf16[8,24,2048]{2,1,0:T(8,128)(2,1)S(1)}, u32[]{:S(2)}, u32[]{:S(2)}) async-start(bf16[8,24,2048]{2,1,0:T(8,128)(2,1)} %bitcast.11), calls=%async_computation.1 | async-start | bytes 1572864 | tf_op jit(solution)/shard_map/all_to_all | solution.py:306
  56.4 16.8 %collective-permute-done.5.chunk_ref = bf16[136,2048]{1,0:T(8,128)(2,1)S(1)} collective-permute-done((bf16[136,2048]{1,0:T(8,128)(2,1)S(1)}, bf16[136,2048]{1,0:T(8,128)(2,1)S(1)}, u32[]{:S(2)}, u32[]{:S(2)}) %collective-permute-start.5) | collective-permute-done | bytes 557088 | tf_op jit(solution)/shard_map/ppermute | solution.py:300
  73.2 2.0 %shard_map.124 = bf16[192,2048]{1,0:T(8,128)(2,1)} custom-call(s32[2]{0:T(128)S(1)} %pad_add_fusion.where_ref, bf16[136,2048]{1,0:T(8,128)(2,1)S(1)} %collective-permute-done.5.chunk_ref), custom_call_target="tpu_custom_call" | custom-call | flops 100663296 | bytes 557064 | tf_op jit(solution)/shard_map/pallas_call | solution.py:162
  75.2 3.8 %all-to-all-start.5 = ((bf16[8,24,2048]{2,1,0:T(8,128)(2,1)}), bf16[8,24,2048]{2,1,0:T(8,128)(2,1)S(1)}, u32[]{:S(2)}, u32[]{:S(2)}) async-start(bf16[8,24,2048]{2,1,0:T(8,128)(2,1)} %bitcast.19), calls=%async_computation.5 | async-start | bytes 1572864 | tf_op jit(solution)/shard_map/all_to_all | solution.py:306
  79.0 9.0 %shard_map.121 = (bf16[192,2048]{1,0:T(8,128)(2,1)S(1)}, bf16[192,2048]{1,0:T(8,128)(2,1)S(1)}) custom-call(s32[2]{0:T(128)S(1)} %pad_add_fusion.where_ref, bf16[192,2048]{1,0:T(8,128)(2,1)S(1)} %bitcast.33, bf16[192,2048]{1,0:T(8,128)(2,1)S(1)} %bitcast.34, bf16[1,2048,1024]{2,1,0:T(8,128)(2,1)} %refs_1_.3, bf16[1,2048,1024]{2,1,0:T(8,128)(2,1)} %refs_2_.5, ...), custom_call_target="tpu_custom_call" | custom-call | flops 4831838208 | bytes 14155784 | tf_op jit(solution)/shard_map/pallas_call | solution.py:162
  88.0 0.9 copy-done.6
  88.9 0.9 copy-done.7
  89.8 0.9 all-to-all-done.5
  90.7 3.5 %all-to-all-start.7 = ((bf16[8,24,2048]{2,1,0:T(8,128)(2,1)}), bf16[8,24,2048]{2,1,0:T(8,128)(2,1)S(1)}, u32[]{:S(2)}, u32[]{:S(2)}) async-start(bf16[8,24,2048]{2,1,0:T(8,128)(2,1)} %bitcast.35), calls=%async_computation.7 | async-start | bytes 1572864 | tf_op jit(solution)/shard_map/all_to_all | solution.py:306
  94.3 16.7 %collective-permute-done.6.chunk_ref = bf16[136,2048]{1,0:T(8,128)(2,1)S(1)} collective-permute-done((bf16[136,2048]{1,0:T(8,128)(2,1)S(1)}, bf16[136,2048]{1,0:T(8,128)(2,1)S(1)}, u32[]{:S(2)}, u32[]{:S(2)}) %collective-permute-start.6) | collective-permute-done | bytes 557088 | tf_op jit(solution)/shard_map/ppermute | solution.py:300
  111.0 2.0 %shard_map.122 = bf16[192,2048]{1,0:T(8,128)(2,1)} custom-call(s32[2]{0:T(128)S(1)} %pad_add_fusion.where_ref, bf16[136,2048]{1,0:T(8,128)(2,1)S(1)} %collective-permute-done.6.chunk_ref), custom_call_target="tpu_custom_call" | custom-call | flops 100663296 | bytes 557064 | tf_op jit(solution)/shard_map/pallas_call | solution.py:162
  113.0 0.8 copy-done.4
  113.8 3.8 %all-to-all-start.3 = ((bf16[8,24,2048]{2,1,0:T(8,128)(2,1)}), bf16[8,24,2048]{2,1,0:T(8,128)(2,1)S(1)}, u32[]{:S(2)}, u32[]{:S(2)}) async-start(bf16[8,24,2048]{2,1,0:T(8,128)(2,1)} %bitcast.15), calls=%async_computation.3 | async-start | bytes 1572864 | tf_op jit(solution)/shard_map/all_to_all | solution.py:306
  117.6 6.8 %shard_map.125 = bf16[192,2048]{1,0:T(8,128)(2,1)} custom-call(s32[2]{0:T(128)S(1)} %pad_add_fusion.where_ref, bf16[192,2048]{1,0:T(8,128)(2,1)S(1)} %bitcast.26, bf16[1,2048,1024]{2,1,0:T(8,128)(2,1)} %refs_1_.3, bf16[1,2048,1024]{2,1,0:T(8,128)(2,1)} %refs_2_.5, bf16[1,1024,2048]{2,1,0:T(8,128)(2,1)} %refs_3_.5), custom_call_target="tpu_custom_call" | custom-call | flops 2415919104 | bytes 13369352 | tf_op jit(solution)/shard_map/pallas_call | solution.py:162
  124.5 4.8 %all-to-all-done.3 = bf16[8,24,2048]{2,1,0:T(8,128)(2,1)S(1)} async-done(((bf16[8,24,2048]{2,1,0:T(8,128)(2,1)}), bf16[8,24,2048]{2,1,0:T(8,128)(2,1)S(1)}, u32[]{:S(2)}, u32[]{:S(2)}) %all-to-all-start.3) | async-done | bytes 786464 | tf_op jit(solution)/shard_map/all_to_all | solution.py:306
  129.3 3.5 %all-to-all-start.6 = ((bf16[8,24,2048]{2,1,0:T(8,128)(2,1)}), bf16[8,24,2048]{2,1,0:T(8,128)(2,1)S(1)}, u32[]{:S(2)}, u32[]{:S(2)}) async-start(bf16[8,24,2048]{2,1,0:T(8,128)(2,1)} %bitcast.21), calls=%async_computation.6 | async-start | bytes 1572864 | tf_op jit(solution)/shard_map/all_to_all | solution.py:306
  132.9 1.0 copy-done.3
  133.9 2.1 %shard_map.126 = bf16[128,2048]{1,0:T(8,128)(2,1)} custom-call(s32[2]{0:T(128)S(1)} %pad_add_fusion.where_ref, bf16[136,2048]{1,0:T(8,128)(2,1)S(1)} %copy-done.3, bf16[192,2048]{1,0:T(8,128)(2,1)S(1)} %bitcast.28), custom_call_target="tpu_custom_call" | custom-call | flops 201326592 | bytes 1343496 | tf_op jit(solution)/shard_map/pallas_call | solution.py:162
  136.1 6.8 %shard_map.123 = bf16[192,2048]{1,0:T(8,128)(2,1)} custom-call(s32[2]{0:T(128)S(1)} %pad_add_fusion.where_ref, bf16[192,2048]{1,0:T(8,128)(2,1)S(1)} %bitcast.27, bf16[1,2048,1024]{2,1,0:T(8,128)(2,1)} %refs_1_.3, bf16[1,2048,1024]{2,1,0:T(8,128)(2,1)} %refs_2_.5, bf16[1,1024,2048]{2,1,0:T(8,128)(2,1)} %refs_3_.5), custom_call_target="tpu_custom_call" | custom-call | flops 2415919104 | bytes 13369352 | tf_op jit(solution)/shard_map/pallas_call | solution.py:162
  142.9 1.6 all-to-all-done.6
  144.5 3.5 %all-to-all-start.4 = ((bf16[8,24,2048]{2,1,0:T(8,128)(2,1)}), bf16[8,24,2048]{2,1,0:T(8,128)(2,1)S(1)}, u32[]{:S(2)}, u32[]{:S(2)}) async-start(bf16[8,24,2048]{2,1,0:T(8,128)(2,1)} %bitcast.17), calls=%async_computation.4 | async-start | bytes 1572864 | tf_op jit(solution)/shard_map/all_to_all | solution.py:306
  148.0 4.4 %collective-permute-done.7.refs_0_ = bf16[128,2048]{1,0:T(8,128)(2,1)} collective-permute-done((bf16[128,2048]{1,0:T(8,128)(2,1)}, bf16[128,2048]{1,0:T(8,128)(2,1)}, u32[]{:S(2)}, u32[]{:S(2)}) %collective-permute-start.7) | collective-permute-done | bytes 524320 | tf_op jit(solution)/shard_map/ppermute | solution.py:300
  152.4 2.6 %shard_map.127 = bf16[128,2048]{1,0:T(8,128)(2,1)} custom-call(s32[2]{0:T(128)S(1)} %pad_add_fusion.where_ref, bf16[136,2048]{1,0:T(8,128)(2,1)S(1)} %copy-done.1, bf16[192,2048]{1,0:T(8,128)(2,1)S(1)} %bitcast.31, bf16[128,2048]{1,0:T(8,128)(2,1)} %collective-permute-done.7.refs_0_), custom_call_target="tpu_custom_call" | custom-call | flops 201326592 | bytes 1867784 | tf_op jit(solution)/shard_map/pallas_call | solution.py:162
  155.0 4.6 %all-to-all-done.4 = bf16[8,24,2048]{2,1,0:T(8,128)(2,1)S(1)} async-done(((bf16[8,24,2048]{2,1,0:T(8,128)(2,1)}), bf16[8,24,2048]{2,1,0:T(8,128)(2,1)S(1)}, u32[]{:S(2)}, u32[]{:S(2)}) %all-to-all-start.4) | async-done | bytes 786464 | tf_op jit(solution)/shard_map/all_to_all | solution.py:306
  159.6 3.5 %all-to-all-start.2 = ((bf16[8,24,2048]{2,1,0:T(8,128)(2,1)}), bf16[8,24,2048]{2,1,0:T(8,128)(2,1)S(1)}, u32[]{:S(2)}, u32[]{:S(2)}) async-start(bf16[8,24,2048]{2,1,0:T(8,128)(2,1)} %bitcast.32), calls=%async_computation.2 | async-start | bytes 1572864 | tf_op jit(solution)/shard_map/all_to_all | solution.py:306
  163.2 7.2 %collective-permute-done.8.refs_0_ = bf16[128,2048]{1,0:T(8,128)(2,1)S(1)} collective-permute-done((bf16[128,2048]{1,0:T(8,128)(2,1)}, bf16[128,2048]{1,0:T(8,128)(2,1)S(1)}, u32[]{:S(2)}, u32[]{:S(2)}) %collective-permute-start.8) | collective-permute-done | bytes 524320 | tf_op jit(solution)/shard_map/ppermute | solution.py:300
  170.4 1.1 copy-done.5
  171.4 1.3 shard_map.128
  172.8 2.0 %all-to-all-done.2 = bf16[8,24,2048]{2,1,0:T(8,128)(2,1)S(1)} async-done(((bf16[8,24,2048]{2,1,0:T(8,128)(2,1)}), bf16[8,24,2048]{2,1,0:T(8,128)(2,1)S(1)}, u32[]{:S(2)}, u32[]{:S(2)}) %all-to-all-start.2) | async-done | bytes 786464 | tf_op jit(solution)/shard_map/all_to_all | solution.py:306
  174.8 12.3 %collective-permute-done.9.refs_0_ = bf16[128,2048]{1,0:T(8,128)(2,1)S(1)} collective-permute-done((bf16[128,2048]{1,0:T(8,128)(2,1)S(1)}, bf16[128,2048]{1,0:T(8,128)(2,1)S(1)}, u32[]{:S(2)}, u32[]{:S(2)}) %collective-permute-start.9) | collective-permute-done | bytes 524320 | tf_op jit(solution)/shard_map/ppermute | solution.py:300
  187.1 1.0 copy-done.10
  188.1 2.1 %shard_map.129 = bf16[128,2048]{1,0:T(8,128)(2,1)} custom-call(s32[2]{0:T(128)S(1)} %pad_add_fusion.where_ref, bf16[136,2048]{1,0:T(8,128)(2,1)S(1)} %get-tuple-element.18.chunk_ref, bf16[128,2048]{1,0:T(8,128)(2,1)S(1)} %copy-done.10, bf16[192,2048]{1,0:T(8,128)(2,1)S(1)} %bitcast.30, bf16[128,2048]{1,0:T(8,128)(2,1)S(1)} %collective-permute-done.9.refs_0_), custom_call_target="tpu_custom_call" | custom-call | flops 201326592 | bytes 2392072 | tf_op jit(solution)/shard_map/pallas_call | solution.py:162
  (39 shorter events, 3.3 us)
Async XLA Ops:
  1.5 7.8 %collective-permute-start = (bf16[16,512]{1,0:T(8,128)(2,1)S(1)}, bf16[16,512]{1,0:T(8,128)(2,1)S(1)}, u32[]{:S(2)}, u32[]{:S(2)}) collective-permute-start(bf16[16,512]{1,0:T(8,128)(2,1)S(1)} %pad_maximum_fusion), channel_id=1, source_target_pairs={{0,4},{4,8},{8,12},{12,16},{16,20},{20,24},{24,28},{28,0},{1,5},{5... | collective-permute-start | bytes 49160 | tf_op jit(solution)/shard_map/ppermute | solution.py:321
  9.3 1.0 copy-start.8
  10.3 0.7 copy-start.14
  12.1 2.7 %collective-permute-start.1 = (bf16[128,512]{1,0:T(8,128)(2,1)S(1)}, bf16[128,512]{1,0:T(8,128)(2,1)S(1)}, u32[]{:S(2)}, u32[]{:S(2)}) collective-permute-start(bf16[128,512]{1,0:T(8,128)(2,1)S(1)} %get-tuple-element.15), channel_id=1, source_target_pairs={{0,1},{1,0},{2,3},{3,2},{4,5},{5,4},{6,7},{7,6},{8,9},{9,8},{10,11... | collective-permute-start | bytes 393224 | tf_op jit(solution)/shard_map/ppermute | solution.py:332
  12.2 6.4 %collective-permute-start.2 = (bf16[128,512]{1,0:T(8,128)(2,1)S(1)}, bf16[128,512]{1,0:T(8,128)(2,1)S(1)}, u32[]{:S(2)}, u32[]{:S(2)}) collective-permute-start(bf16[128,512]{1,0:T(8,128)(2,1)S(1)} %get-tuple-element.16), channel_id=1, source_target_pairs={{0,2},{1,3},{2,0},{3,1},{4,6},{5,7},{6,4},{7,5},{8,10},{9,11},{10,... | collective-permute-start | bytes 393224 | tf_op jit(solution)/shard_map/ppermute | solution.py:332
  14.0 6.4 %collective-permute-start.3 = (bf16[128,512]{1,0:T(8,128)(2,1)S(1)}, bf16[128,512]{1,0:T(8,128)(2,1)S(1)}, u32[]{:S(2)}, u32[]{:S(2)}) collective-permute-start(bf16[128,512]{1,0:T(8,128)(2,1)S(1)} %get-tuple-element.17), channel_id=1, source_target_pairs={{0,3},{1,2},{2,1},{3,0},{4,7},{5,6},{6,5},{7,4},{8,11},{9,10},{10,... | collective-permute-start | bytes 393224 | tf_op jit(solution)/shard_map/ppermute | solution.py:332
  20.3 1.0 copy-start.11
  21.4 0.7 copy-start.12
  22.1 0.7 copy-start.13
  29.4 0.8 copy-start.9
  30.2 22.3 %all-to-all-start = ((bf16[8,24,2048]{2,1,0:T(8,128)(2,1)}), bf16[8,24,2048]{2,1,0:T(8,128)(2,1)S(1)}, u32[]{:S(2)}, u32[]{:S(2)}) async-start(bf16[8,24,2048]{2,1,0:T(8,128)(2,1)} %bitcast.9), calls=%async_computation | async-start | bytes 1572864 | tf_op jit(solution)/shard_map/all_to_all | solution.py:306
  33.7 16.7 %collective-permute-start.4 = (bf16[136,2048]{1,0:T(8,128)(2,1)S(1)}, bf16[136,2048]{1,0:T(8,128)(2,1)S(1)}, u32[]{:S(2)}, u32[]{:S(2)}) collective-permute-start(bf16[136,2048]{1,0:T(8,128)(2,1)S(1)} %get-tuple-element.18.chunk_ref), channel_id=1, source_target_pairs={{0,8},{1,9},{2,10},{3,11},{4,12},{5,13},{6,14},{7,15},{8,16},{9,17... | collective-permute-start | bytes 1671176 | tf_op jit(solution)/shard_map/ppermute | solution.py:300
  50.5 24.7 %copy-start.2 = (bf16[136,2048]{1,0:T(8,128)(2,1)}, bf16[136,2048]{1,0:T(8,128)(2,1)S(1)}, u32[]{:S(2)}) copy-start(bf16[136,2048]{1,0:T(8,128)(2,1)S(1)} %collective-permute-done.4.chunk_ref) | copy-start | bytes 1671172
  52.5 22.7 %all-to-all-start.1 = ((bf16[8,24,2048]{2,1,0:T(8,128)(2,1)}), bf16[8,24,2048]{2,1,0:T(8,128)(2,1)S(1)}, u32[]{:S(2)}, u32[]{:S(2)}) async-start(bf16[8,24,2048]{2,1,0:T(8,128)(2,1)} %bitcast.11), calls=%async_computation.1 | async-start | bytes 1572864 | tf_op jit(solution)/shard_map/all_to_all | solution.py:306
  56.3 16.8 %collective-permute-start.5 = (bf16[136,2048]{1,0:T(8,128)(2,1)S(1)}, bf16[136,2048]{1,0:T(8,128)(2,1)S(1)}, u32[]{:S(2)}, u32[]{:S(2)}) collective-permute-start(bf16[136,2048]{1,0:T(8,128)(2,1)S(1)} %collective-permute-done.4.chunk_ref), channel_id=1, source_target_pairs={{0,8},{1,9},{2,10},{3,11},{4,12},{5,13},{6,14},{7,15},{8,16},{9,17... | collective-permute-start | bytes 1671176 | tf_op jit(solution)/shard_map/ppermute | solution.py:300
  73.2 21.1 %copy-start = (bf16[136,2048]{1,0:T(8,128)(2,1)}, bf16[136,2048]{1,0:T(8,128)(2,1)S(1)}, u32[]{:S(2)}) copy-start(bf16[136,2048]{1,0:T(8,128)(2,1)S(1)} %collective-permute-done.5.chunk_ref) | copy-start | bytes 1671172
  75.2 15.5 %all-to-all-start.5 = ((bf16[8,24,2048]{2,1,0:T(8,128)(2,1)}), bf16[8,24,2048]{2,1,0:T(8,128)(2,1)S(1)}, u32[]{:S(2)}, u32[]{:S(2)}) async-start(bf16[8,24,2048]{2,1,0:T(8,128)(2,1)} %bitcast.19), calls=%async_computation.5 | async-start | bytes 1572864 | tf_op jit(solution)/shard_map/all_to_all | solution.py:306
  88.0 0.9 copy-start.6
  88.9 0.9 copy-start.7
  90.7 23.1 %all-to-all-start.7 = ((bf16[8,24,2048]{2,1,0:T(8,128)(2,1)}), bf16[8,24,2048]{2,1,0:T(8,128)(2,1)S(1)}, u32[]{:S(2)}, u32[]{:S(2)}) async-start(bf16[8,24,2048]{2,1,0:T(8,128)(2,1)} %bitcast.35), calls=%async_computation.7 | async-start | bytes 1572864 | tf_op jit(solution)/shard_map/all_to_all | solution.py:306
  94.2 16.7 %collective-permute-start.6 = (bf16[136,2048]{1,0:T(8,128)(2,1)S(1)}, bf16[136,2048]{1,0:T(8,128)(2,1)S(1)}, u32[]{:S(2)}, u32[]{:S(2)}) collective-permute-start(bf16[136,2048]{1,0:T(8,128)(2,1)S(1)} %collective-permute-done.5.chunk_ref), channel_id=1, source_target_pairs={{0,8},{1,9},{2,10},{3,11},{4,12},{5,13},{6,14},{7,15},{8,16},{9,17... | collective-permute-start | bytes 1671176 | tf_op jit(solution)/shard_map/ppermute | solution.py:300
  113.0 0.8 copy-start.4
  113.8 15.5 %all-to-all-start.3 = ((bf16[8,24,2048]{2,1,0:T(8,128)(2,1)}), bf16[8,24,2048]{2,1,0:T(8,128)(2,1)S(1)}, u32[]{:S(2)}, u32[]{:S(2)}) async-start(bf16[8,24,2048]{2,1,0:T(8,128)(2,1)} %bitcast.15), calls=%async_computation.3 | async-start | bytes 1572864 | tf_op jit(solution)/shard_map/all_to_all | solution.py:306
  129.3 15.1 %all-to-all-start.6 = ((bf16[8,24,2048]{2,1,0:T(8,128)(2,1)}), bf16[8,24,2048]{2,1,0:T(8,128)(2,1)S(1)}, u32[]{:S(2)}, u32[]{:S(2)}) async-start(bf16[8,24,2048]{2,1,0:T(8,128)(2,1)} %bitcast.21), calls=%async_computation.6 | async-start | bytes 1572864 | tf_op jit(solution)/shard_map/all_to_all | solution.py:306
  132.9 1.1 copy-start.3
  136.1 16.3 %collective-permute-start.7 = (bf16[128,2048]{1,0:T(8,128)(2,1)}, bf16[128,2048]{1,0:T(8,128)(2,1)}, u32[]{:S(2)}, u32[]{:S(2)}) collective-permute-start(bf16[128,2048]{1,0:T(8,128)(2,1)} %shard_map.126), channel_id=1, source_target_pairs={{0,8},{1,9},{2,10},{3,11},{4,12},{5,13},{6,14},{7,15},{8,16},{9,17... | collective-permute-start | bytes 1572872 | tf_op jit(solution)/shard_map/ppermute | solution.py:300
  136.1 16.3 %copy-start.1 = (bf16[136,2048]{1,0:T(8,128)(2,1)S(1)}, bf16[136,2048]{1,0:T(8,128)(2,1)}, u32[]{:S(2)}) copy-start(bf16[136,2048]{1,0:T(8,128)(2,1)} %copy-done) | copy-start | bytes 1671172
  144.5 15.1 %all-to-all-start.4 = ((bf16[8,24,2048]{2,1,0:T(8,128)(2,1)}), bf16[8,24,2048]{2,1,0:T(8,128)(2,1)S(1)}, u32[]{:S(2)}, u32[]{:S(2)}) async-start(bf16[8,24,2048]{2,1,0:T(8,128)(2,1)} %bitcast.17), calls=%async_computation.4 | async-start | bytes 1572864 | tf_op jit(solution)/shard_map/all_to_all | solution.py:306
  155.0 15.4 %collective-permute-start.8 = (bf16[128,2048]{1,0:T(8,128)(2,1)}, bf16[128,2048]{1,0:T(8,128)(2,1)S(1)}, u32[]{:S(2)}, u32[]{:S(2)}) collective-permute-start(bf16[128,2048]{1,0:T(8,128)(2,1)} %shard_map.127), channel_id=1, source_target_pairs={{0,8},{1,9},{2,10},{3,11},{4,12},{5,13},{6,14},{7,15},{8,16},{9,17... | collective-permute-start | bytes 1572872 | tf_op jit(solution)/shard_map/ppermute | solution.py:300
  159.6 15.1 %all-to-all-start.2 = ((bf16[8,24,2048]{2,1,0:T(8,128)(2,1)}), bf16[8,24,2048]{2,1,0:T(8,128)(2,1)S(1)}, u32[]{:S(2)}, u32[]{:S(2)}) async-start(bf16[8,24,2048]{2,1,0:T(8,128)(2,1)} %bitcast.32), calls=%async_computation.2 | async-start | bytes 1572864 | tf_op jit(solution)/shard_map/all_to_all | solution.py:306
  170.4 1.1 copy-start.5
  172.7 14.4 %collective-permute-start.9 = (bf16[128,2048]{1,0:T(8,128)(2,1)S(1)}, bf16[128,2048]{1,0:T(8,128)(2,1)S(1)}, u32[]{:S(2)}, u32[]{:S(2)}) collective-permute-start(bf16[128,2048]{1,0:T(8,128)(2,1)S(1)} %shard_map.128), channel_id=1, source_target_pairs={{0,8},{1,9},{2,10},{3,11},{4,12},{5,13},{6,14},{7,15},{8,16},{9,17... | collective-permute-start | bytes 1572872 | tf_op jit(solution)/shard_map/ppermute | solution.py:300
  187.1 1.0 copy-start.10

commit v3 on v2

v3 whole, which is shorter than its diff:
```python
import functools

import jax
import jax.numpy as jnp
from jax import lax
from jax.experimental import pallas as pl
from jax.experimental.pallas import tpu as pltpu
from jax.sharding import PartitionSpec as P


GROUPS = 4
CORES = 2

norm_eps = 1e-05
clamp_limit = 7.0
sigmoid_alpha = 1.702
longest_window = 16
VMEM_BYTES = 12 * 1024 * 1024


def dot32(a, b):
    return jnp.dot(a, b, preferred_element_type=jnp.float32)


def pool_kernel(
    place_ref, rim_ref, rows_ref, docs_ref, *refs, group_width,
):
    out_refs, ext_ref = refs[:-1], refs[-1]
    _, channels = rows_ref.shape
    rim = rim_ref.shape[0]
    block = out_refs[0].shape[0]
    group, mine, edge = place_ref[0], place_ref[1], place_ref[2]
    groups_here = max(1, channels // group_width)
    width = channels // groups_here
    wide = block + rim
    ext_ref[0:rim, :] = rim_ref[...]
    ext_ref[rim:, :] = rows_ref[...]
    rim_docs = (rim_ref[0:1, 0:rim].astype(jnp.float32) - 1.0).astype(jnp.int32)
    rim_docs = jnp.where(edge == 0, -1, rim_docs)
    at_row = lax.broadcasted_iota(jnp.int32, (block, wide), 0)
    at_col = lax.broadcasted_iota(jnp.int32, (block, wide), 1)
    back = at_row + rim - at_col
    for d in range(len(out_refs)):
        index = mine ^ d
        here = docs_ref[pl.ds(index, 1), :]
        previous = docs_ref[pl.ds(jnp.maximum(index - 1, 0), 1), :][:, block - rim :]
        before = jnp.where(index == 0, rim_docs, previous)
        col_docs = jnp.concatenate([before, here], 1)
        row_docs = jnp.sum(
            jnp.where(back == 0, jnp.broadcast_to(col_docs, (block, wide)), 0), 1, keepdims=True
        )
        alike = (col_docs == row_docs) & (back >= 0)
        start = pl.multiple_of(index * block, block)
        values = ext_ref[pl.ds(start, wide), :]
        own = values[rim:, :].astype(jnp.float32)
        for part in range(groups_here):
            window = jnp.left_shift(2, group + part)
            band = jnp.where(alike & (back < window), 1.0, 0.0)
            count = jnp.sum(band, 1, keepdims=True)
            lanes = slice(part * width, (part + 1) * width)
            total = dot32(band.astype(jnp.bfloat16), values[:, lanes])
            out_refs[d][:, lanes] = (total / count - own[:, lanes]).astype(jnp.bfloat16)


def named_experts(where_ref, routes_t, chips):
    offset = lax.broadcasted_iota(jnp.int32, (chips, routes_t.shape[1]), 0)
    here = (offset ^ where_ref[2]) * CORES + where_ref[3] + where_ref[0] * (chips * CORES)
    return [routes_t[j : j + 1, :] == here for j in range(routes_t.shape[0])]


def slot_table(matches, capacity):
    count, tokens = matches[0].shape
    named = matches[0]
    for match in matches[1:]:
        named = named | match
    earlier = (
        lax.broadcasted_iota(jnp.int32, (tokens, tokens), 0)
        < lax.broadcasted_iota(jnp.int32, (tokens, tokens), 1)
    )
    ones = jnp.where(named, 1.0, 0.0)
    rank = dot32(ones.astype(jnp.bfloat16), jnp.where(earlier, 1.0, 0.0).astype(jnp.bfloat16))
    held = jnp.where(named, rank, -1.0).astype(jnp.bfloat16)
    slots = count * capacity
    low = lax.broadcasted_iota(jnp.int32, (slots, count), 1) * capacity
    slot = lax.broadcasted_iota(jnp.int32, (slots, count), 0)
    inside = (slot >= low) & (slot < low + capacity)
    spread = jnp.where(inside, 1.0, 0.0).astype(jnp.bfloat16)
    place = jnp.sum(jnp.where(inside, slot - low, 0), 1, keepdims=True).astype(jnp.float32)
    return dot32(spread, held) == place, spread


def mixer_kernel(
    where_ref, table_ref, gs_ref, stream_ref, gain_ref, *refs
):
    gw_ref, ow_ref, *block_refs = refs[:-3]
    resid_ref, chunk_ref, mixed_ref = refs[-3:]
    groups, width, _ = gw_ref.shape
    tokens, _ = block_refs[0].shape
    for d in range(len(block_refs)):
        mixed_ref[where_ref[1] ^ d] = block_refs[d][...]
    mixed = jnp.concatenate([mixed_ref[d] for d in range(len(block_refs))], 1)
    parts = []
    for g in range(groups):
        lanes = slice(g * width, (g + 1) * width)
        grouped = dot32(mixed[:, lanes], gw_ref[g])
        parts.append((grouped * gs_ref[:, lanes]).astype(jnp.bfloat16))
    mixer_out = dot32(jnp.concatenate(parts, 1), ow_ref[...])
    resid = (stream_ref[...].astype(jnp.float32) + mixer_out).astype(jnp.bfloat16)
    resid_ref[...] = resid
    values = resid.astype(jnp.float32)
    inverse = lax.rsqrt(jnp.mean(values * values, -1, keepdims=True) + norm_eps)
    normed = (values * inverse * gain_ref[...]).astype(jnp.bfloat16)
    chunk_ref[0:tokens, :] = normed
    top = table_ref.shape[0] // 2
    weights = table_ref[top:, :]
    high = weights.astype(jnp.bfloat16)
    low = (weights - high.astype(jnp.float32)).astype(jnp.bfloat16)
    routes_t = table_ref[0:top, :]
    lines = [piece.astype(jnp.float32)[j : j + 1, :] for piece in (routes_t, high, low)
             for j in range(top)]
    line = jnp.concatenate(lines, 1)
    line = jnp.pad(line, ((0, 0), (0, chunk_ref.shape[1] - line.shape[1])))
    rest = chunk_ref.shape[0] - tokens
    chunk_ref[tokens:, :] = jnp.broadcast_to(line, (rest, line.shape[1])).astype(jnp.bfloat16)


def read_table(chunk_ref, tokens, top):
    line = chunk_ref[tokens:, :].astype(jnp.float32)
    rows = [line[0:1, j * tokens : (j + 1) * tokens] for j in range(3 * top)]
    pieces = [jnp.concatenate(rows[k * top : (k + 1) * top], 0) for k in range(3)]
    return pieces[0].astype(jnp.int32), pieces[1], pieces[2]


def call(kernel, shapes, args, flops, scratch=(), limit=VMEM_BYTES):
    specs = [pl.BlockSpec(memory_space=pltpu.SMEM)]
    specs += [pl.BlockSpec(memory_space=pltpu.VMEM)] * (len(args) - 1)
    return pl.pallas_call(
        kernel,
        out_shape=tuple(shapes),
        in_specs=specs,
        out_specs=(pl.BlockSpec(memory_space=pltpu.VMEM),) * len(shapes),
        scratch_shapes=scratch,
        compiler_params=pltpu.CompilerParams(vmem_limit_bytes=limit),
        cost_estimate=pl.CostEstimate(
            flops=flops, transcendentals=0, bytes_accessed=sum(a.nbytes for a in args)
        ),
    )(*args)


def pick_kernel(where_ref, *refs, tokens, top, capacity):
    chunk_refs, send_refs = refs[:CORES], refs[CORES:]
    chips = len(send_refs)
    for k in range(CORES):
        routes_t, _, _ = read_table(chunk_refs[k], tokens, top)
        taken, _ = slot_table(named_experts(where_ref, routes_t, chips), capacity)
        picked = dot32(jnp.where(taken, 1.0, 0.0).astype(jnp.bfloat16), chunk_refs[k][0:tokens, :])
        picked = picked.astype(jnp.bfloat16)
        for d in range(chips):
            rows = picked[d * capacity : (d + 1) * capacity]
            send_refs[d][k * capacity : (k + 1) * capacity, :] = rows


def weighted_sum(where_ref, chunk_ref, back_refs, k, tokens, top, capacity):
    routes_t, *weights = read_table(chunk_ref, tokens, top)
    matches = named_experts(where_ref, routes_t, len(back_refs))
    taken, spread = slot_table(matches, capacity)
    back = jnp.concatenate([ref[k * capacity : (k + 1) * capacity, :] for ref in back_refs], 0)
    total = jnp.zeros((tokens, back.shape[1]), jnp.float32)
    for piece in weights:
        weight = jnp.zeros(matches[0].shape, jnp.float32)
        for j, match in enumerate(matches):
            weight = weight + jnp.where(match, piece[j : j + 1, :], 0.0)
        factor = jnp.where(taken, dot32(spread, weight.astype(jnp.bfloat16)), 0.0)
        total = total + lax.dot_general(
            factor.astype(jnp.bfloat16), back, (((0,), (0,)), ((), ())),
            preferred_element_type=jnp.float32,
        )
    return total


def partner_kernel(where_ref, chunk_ref, *refs, tokens, top, capacity):
    total = weighted_sum(where_ref, chunk_ref, refs[:-1], 1, tokens, top, capacity)
    refs[-1][...] = total.astype(jnp.bfloat16)


def own_kernel(where_ref, chunk_ref, *refs, chips, tokens, top, capacity):
    total = weighted_sum(where_ref, chunk_ref, refs[:chips], 0, tokens, top, capacity)
    for ref in refs[chips:-1]:
        total = total + ref[...].astype(jnp.float32)
    refs[-1][...] = total.astype(jnp.bfloat16)


def expert_kernel(where_ref, *refs):
    chips = (len(refs) - 3) // 2
    row_refs, (gate_ref, up_ref, down_ref), out_refs = refs[:chips], refs[chips : chips + 3], refs[chips + 3 :]
    rows = jnp.concatenate([ref[...] for ref in row_refs], 0)
    hidden = gate_ref.shape[1]
    cut = min(hidden, 256)
    total = None
    for start in range(0, hidden, cut):
        lanes = slice(start, start + cut)
        gated = jnp.minimum(dot32(rows, gate_ref[:, lanes]), clamp_limit)
        linear = jnp.clip(dot32(rows, up_ref[:, lanes]), -clamp_limit, clamp_limit)
        activated = (gated * jax.nn.sigmoid(sigmoid_alpha * gated) * (linear + 1.0)).astype(
            jnp.bfloat16
        )
        part = dot32(activated, down_ref[lanes, :])
        total = part if total is None else total + part
    result = total.astype(jnp.bfloat16)
    length = row_refs[0].shape[0]
    for d in range(chips):
        out_refs[d][...] = result[d * length : (d + 1) * length]


in_vmem = functools.partial(pltpu.with_memory_space_constraint, memory_space=pltpu.VMEM)


def body(
    stream,
    projected,
    segments,
    group_weight,
    group_scale,
    out_weight,
    ffn_gain,
    routes,
    route_weights,
    expert_gate,
    expert_up,
    expert_down,
    *,
    planes,
):
    row_count, channels = projected.shape
    tp_count = lax.axis_size("tp")
    sp_count = lax.axis_size("sp")
    width = channels * tp_count
    group_width = width // GROUPS
    tokens, top = routes.shape
    devices = sp_count * tp_count
    count = devices // planes
    chips = count // CORES
    capacity = 3 * tokens * top // (2 * devices)
    hidden = expert_gate.shape[2]
    every = ("sp", "tp")
    sp_index, tp_index = lax.axis_index("sp"), lax.axis_index("tp")
    device = sp_index * tp_count + tp_index
    where = jnp.stack(
        [device // count, tp_index, device % count // CORES, device % CORES]
    ).astype(jnp.int32)
    place = jnp.stack([tp_index * channels // group_width, tp_index, sp_index]).astype(jnp.int32)
    sizes = dict(tokens=tokens, top=top, capacity=capacity)

    def move(value, to):
        return lax.ppermute(value, every, [(i, to(i)) for i in range(devices)])

    def hop(value):
        return move(value, lambda i: (i + count) % devices)

    def swap(value):
        return move(value, lambda i: i ^ 1)

    def in_plane(blocks):
        moved = [blocks[0]]
        for d in range(1, chips):
            moved.append(move(blocks[d], lambda i: i ^ (d * CORES)))
        return moved

    rim = longest_window
    tail_docs = (segments[row_count - rim :] + 1).astype(jnp.bfloat16)
    payload = jnp.concatenate(
        [
            jnp.pad(tail_docs, (0, channels - rim))[None, :],
            projected[row_count - rim + 1 :],
        ],
        0,
    )
    before = lax.ppermute(payload, "sp", [(i, (i + 1) % sp_count) for i in range(sp_count)])
    mixed = call(
        functools.partial(pool_kernel, group_width=group_width),
        [jax.ShapeDtypeStruct((tokens, channels), jnp.bfloat16)] * tp_count,
        [place, before, in_vmem(projected), segments.reshape(tp_count, tokens)],
        2 * row_count * channels * (tokens + rim),
        [pltpu.VMEM((row_count + rim, channels), jnp.bfloat16)],
    )
    blocks = [mixed[0]]
    for d in range(1, tp_count):
        pairs = [(i, i ^ d) for i in range(tp_count)]
        blocks.append(lax.ppermute(mixed[d], "tp", pairs))
    table = jnp.concatenate([routes.T.astype(jnp.float32), route_weights.T], 0)

    shape = jax.ShapeDtypeStruct((tokens, width), jnp.bfloat16)
    block = jax.ShapeDtypeStruct((CORES * capacity, width), jnp.bfloat16)
    resid, chunk = call(
        mixer_kernel,
        [shape, jax.ShapeDtypeStruct((tokens + 8, width), jnp.bfloat16)],
        [
            where, table, in_vmem(group_scale.reshape(1, -1)), in_vmem(stream),
            in_vmem(ffn_gain.reshape(1, -1)), in_vmem(group_weight), in_vmem(out_weight), *blocks,
        ],
        2 * tokens * width * (width + group_width),
        [pltpu.VMEM((tp_count, tokens, channels), jnp.bfloat16)],
    )
    small = 2 * tokens * count * capacity * width
    matrices = [in_vmem(expert_gate[0]), in_vmem(expert_up[0]), in_vmem(expert_down[0])]

    def dispatch(pair):
        rows = call(
            functools.partial(pick_kernel, **sizes), [block] * chips, [where, *pair],
            small,
        )
        return in_plane(rows)

    def experts(rows):
        results = call(
            expert_kernel, [block] * chips, [where, *rows, *matrices],
            6 * count * capacity * width * hidden,
        )
        return in_plane(results)

    def gather(pair, back, others):
        (given,) = call(
            functools.partial(partner_kernel, **sizes), [shape], [where, pair[1], *back],
            small,
        )
        got = swap(given)
        (total,) = call(
            functools.partial(own_kernel, chips=chips, **sizes), [shape],
            [where, pair[0], *back, got, *others], small,
        )
        return total

    chunks = [chunk]
    for _ in range(1, planes):
        chunks.append(hop(chunks[-1]))
    pairs = [(chunks[s], swap(chunks[s])) for s in range(planes)]
    arrived = [dispatch(pairs[s]) for s in range(planes)]
    returned = [experts(arrived[s]) for s in range(planes)]
    carried = []
    for s in range(1, planes):
        carried = [hop(gather(pairs[s], returned[s], carried))]
    return gather(pairs[0], returned[0], [resid, *carried])


def plane_count(mesh):
    sizes = mesh.shape
    heights = {getattr(d, "coords", (0, 0, -1))[2] for d in mesh.devices.flat}
    if -1 in heights:
        return max(1, sizes["sp"] // max(1, sizes["tp"] // 2))
    return len(heights)


def solution(mesh):
    in_specs = (
        P(("sp", "tp"), None),
        P("sp", "tp"),
        P("sp"),
        P(),
        P(),
        P(),
        P(),
        P(("sp", "tp"), None),
        P(("sp", "tp"), None),
        P(("sp", "tp"), None, None),
        P(("sp", "tp"), None, None),
        P(("sp", "tp"), None, None),
    )
    out_specs = P(("sp", "tp"), None)
    planes = plane_count(mesh)

    def layer(*args):
        return body(*args, planes=planes)

    return jax.shard_map(layer, mesh=mesh, in_specs=in_specs, out_specs=out_specs, check_vma=False)
```

time: 191 us -> 174 us (0.911)
  Pallas kernels: 44.5 us -> 34.4 us
  waiting for transfers between devices: 97.5 us -> 93.5 us
    all_to_all x8 -> x0, starting transfers between devices: 29.3 us -> none  [in_plane(): lax.all_to_all(blocks, every, split_axis=0, concat_axis=0, axis_index_gro...]
    ppermute x6 -> x38, starting transfers between devices: 0.18 us -> 28.6 us  [move(): return lax.ppermute(value, every, [(i, to(i)) for i in range(devices)])]
    all_to_all x8 -> x0, waiting for transfers between devices: 13.8 us -> none  [in_plane(): lax.all_to_all(blocks, every, split_axis=0, concat_axis=0, axis_index_gro...]
    pallas_call x12 -> x18, Pallas kernels: 44.5 us -> 34.4 us  [call(): pl.pallas_call(kernel, out_shape=tuple(shapes), in_specs=specs, out_specs...]
    ppermute x6 -> x38, waiting for transfers between devices: 74.1 us -> 83.9 us  [move(): return lax.ppermute(value, every, [(i, to(i)) for i in range(devices)])]
    unnamed x30 -> x20, local copies, waits for them, and re-layouts: 10.7 us -> 9.14 us
  transfers between devices with their start and end apart: 18 -> 42, of which waited for: 14 -> 26; matrix products, arithmetic and copies ran while one was open for 1% -> 1% of each run, Pallas kernels for 18% -> 17%
where the time goes in v3:
time: 174 us
  waiting for transfers between devices  93.5 us (54%)
  Pallas kernels  34.4 us (20%)
  starting transfers between devices  33.5 us (19%)
  local copies, waits for them, and re-layouts  9.88 us (6%)
  other arithmetic  2.29 us (1%)
    ppermute x38, waiting for transfers between devices, move(): return lax.ppermute(value, every, [(i, to(i)) for i in range(devices)])  83.9 us
    pallas_call x18, Pallas kernels, call(): pl.pallas_call(kernel, out_shape=tuple(shapes), in_specs=specs, out_specs...  34.4 us
    ppermute x38, starting transfers between devices, move(): return lax.ppermute(value, every, [(i, to(i)) for i in range(devices)])  28.6 us
    unnamed x20, local copies, waits for them, and re-layouts  9.14 us
    ppermute x3, waiting for transfers between devices, body(): blocks.append(lax.ppermute(mixed[d], 'tp', pairs))  5.55 us
    ppermute x1, waiting for transfers between devices, body(): lax.ppermute(payload, 'sp', [(i, (i + 1) % sp_count) for i in range(sp_co...  4 us
  transfers between devices with their start and end apart: 42, of which 26 were waited for; matrix products, arithmetic and copies ran while one was open for 1% of the time, Pallas kernels for 17%

profile of v3, /device:TPU:0, one launch (start us, length us, event | category | flops | bytes accessed | tf_op | source)
XLA Modules:
  0.0 173.9 jit_solution(18361095590018403056)
XLA Ops:
  1.5 3.0 %collective-permute-start = (bf16[16,512]{1,0:T(8,128)(2,1)S(1)}, bf16[16,512]{1,0:T(8,128)(2,1)S(1)}, u32[]{:S(2)}, u32[]{:S(2)}) collective-permute-start(bf16[16,512]{1,0:T(8,128)(2,1)S(1)} %pad_maximum_fusion), channel_id=1, source_target_pairs={{0,4},{4,8},{8,12},{12,16},{16,20},{20,24},{24,28},{28,0},{1,5},{5... | collective-permute-start | bytes 49160 | tf_op jit(solution)/shard_map/ppermute | solution.py:278
  5.3 4.0 %collective-permute-done.rim_ref = bf16[16,512]{1,0:T(8,128)(2,1)S(1)} collective-permute-done((bf16[16,512]{1,0:T(8,128)(2,1)S(1)}, bf16[16,512]{1,0:T(8,128)(2,1)S(1)}, u32[]{:S(2)}, u32[]{:S(2)}) %collective-permute-start) | collective-permute-done | bytes 16416 | tf_op jit(solution)/shard_map/ppermute | solution.py:278
  12.2 1.8 %collective-permute-start.2 = (bf16[128,512]{1,0:T(8,128)(2,1)S(1)}, bf16[128,512]{1,0:T(8,128)(2,1)S(1)}, u32[]{:S(2)}, u32[]{:S(2)}) collective-permute-start(bf16[128,512]{1,0:T(8,128)(2,1)S(1)} %get-tuple-element.45), channel_id=1, source_target_pairs={{0,2},{1,3},{2,0},{3,1},{4,6},{5,7},{6,4},{7,5},{8,10},{9,11},{10,... | collective-permute-start | bytes 393224 | tf_op jit(solution)/shard_map/ppermute | solution.py:289
  14.8 3.8 %collective-permute-done.2.refs_4_ = bf16[128,512]{1,0:T(8,128)(2,1)S(1)} collective-permute-done((bf16[128,512]{1,0:T(8,128)(2,1)S(1)}, bf16[128,512]{1,0:T(8,128)(2,1)S(1)}, u32[]{:S(2)}, u32[]{:S(2)}) %collective-permute-start.2) | collective-permute-done | bytes 131104 | tf_op jit(solution)/shard_map/ppermute | solution.py:289
  18.6 1.7 collective-permute-done.3.refs_5_
  20.3 3.4 %copy-done.3 = bf16[2048,2048]{1,0:T(8,128)(2,1)S(1)} copy-done((bf16[2048,2048]{1,0:T(8,128)(2,1)S(1)}, bf16[2048,2048]{1,0:T(8,128)(2,1)}, u32[]{:S(2)}) %copy-start.3) | copy-done | bytes 8388632
  23.7 1.6 copy-done.4
  27.8 2.4 %shard_map.119 = (bf16[128,2048]{1,0:T(8,128)(2,1)S(1)}, bf16[136,2048]{1,0:T(8,128)(2,1)S(1)}) custom-call(s32[4]{0:T(128)S(1)} %pad_add_fusion.where_ref, f32[8,128]{1,0:T(8,128)S(1)} %pad_maximum_fusion.1.table_ref, f32[1,2048]{1,0:T(1,128)S(1)} %bitcast.27, bf16[128,2048]{1,0:T(8,128)(2,1)S(1)} %copy-done.6, f32[1,2048]{1,0:T(1,128)S(1)} %bitcast.28, ...), custom_call_target="tpu_custom_call" | custom-call | flops 1342177280 | bytes 11554832 | tf_op jit(solution)/shard_map/pallas_call | solution.py:137
  30.2 16.7 %collective-permute-done.12.refs_0_.chunk_ref = bf16[136,2048]{1,0:T(8,128)(2,1)S(1)} collective-permute-done((bf16[136,2048]{1,0:T(8,128)(2,1)S(1)}, bf16[136,2048]{1,0:T(8,128)(2,1)S(1)}, u32[]{:S(2)}, u32[]{:S(2)}) %collective-permute-start.12) | collective-permute-done | bytes 557088 | tf_op jit(solution)/shard_map/ppermute | solution.py:255
  46.9 2.0 %collective-permute-done.31.refs_1_.chunk_ref = bf16[136,2048]{1,0:T(8,128)(2,1)S(1)} collective-permute-done((bf16[136,2048]{1,0:T(8,128)(2,1)S(1)}, bf16[136,2048]{1,0:T(8,128)(2,1)S(1)}, u32[]{:S(2)}, u32[]{:S(2)}) %collective-permute-start.31) | collective-permute-done | bytes 557088 | tf_op jit(solution)/shard_map/ppermute | solution.py:255
  48.9 1.4 shard_map.129
  50.3 1.8 %collective-permute-start.32 = (bf16[48,2048]{1,0:T(8,128)(2,1)S(1)}, bf16[48,2048]{1,0:T(8,128)(2,1)S(1)}, u32[]{:S(2)}, u32[]{:S(2)}) collective-permute-start(bf16[48,2048]{1,0:T(8,128)(2,1)S(1)} %get-tuple-element.74), channel_id=1, source_target_pairs={{0,2},{1,3},{2,0},{3,1},{4,6},{5,7},{6,4},{7,5},{8,10},{9,11},{10,... | collective-permute-start | bytes 589832 | tf_op jit(solution)/shard_map/ppermute | solution.py:255
  52.0 1.8 %collective-permute-start.34 = (bf16[48,2048]{1,0:T(8,128)(2,1)S(1)}, bf16[48,2048]{1,0:T(8,128)(2,1)S(1)}, u32[]{:S(2)}, u32[]{:S(2)}) collective-permute-start(bf16[48,2048]{1,0:T(8,128)(2,1)S(1)} %get-tuple-element.76), channel_id=1, source_target_pairs={{0,6},{1,7},{2,4},{3,5},{4,2},{5,3},{6,0},{7,1},{8,14},{9,15},{10,... | collective-permute-start | bytes 589832 | tf_op jit(solution)/shard_map/ppermute | solution.py:255
  53.8 9.9 %collective-permute-done.13.refs_0_.chunk_ref = bf16[136,2048]{1,0:T(8,128)(2,1)S(1)} collective-permute-done((bf16[136,2048]{1,0:T(8,128)(2,1)S(1)}, bf16[136,2048]{1,0:T(8,128)(2,1)S(1)}, u32[]{:S(2)}, u32[]{:S(2)}) %collective-permute-start.13) | collective-permute-done | bytes 557088 | tf_op jit(solution)/shard_map/ppermute | solution.py:255
  63.8 3.6 %shard_map.130 = (bf16[48,2048]{1,0:T(8,128)(2,1)S(1)}, bf16[48,2048]{1,0:T(8,128)(2,1)S(1)}, bf16[48,2048]{1,0:T(8,128)(2,1)S(1)}, bf16[48,2048]{1,0:T(8,128)(2,1)S(1)}) custom-call(s32[4]{0:T(128)S(1)} %pad_add_fusion.where_ref, bf16[48,2048]{1,0:T(8,128)(2,1)S(1)} %get-tuple-element.73.refs_0_, bf16[48,2048]{1,0:T(8,128)(2,1)S(1)} %collective-permute-done.32.refs_1_, ...), custom_call_target="tpu_custom_call" | custom-call | flops 2415919104 | bytes 13369360 | tf_op jit(solution)/shard_map/pallas_call | solution.py:137
  67.4 1.8 %collective-permute-start.35 = (bf16[48,2048]{1,0:T(8,128)(2,1)S(1)}, bf16[48,2048]{1,0:T(8,128)(2,1)S(1)}, u32[]{:S(2)}, u32[]{:S(2)}) collective-permute-start(bf16[48,2048]{1,0:T(8,128)(2,1)S(1)} %get-tuple-element.78), channel_id=1, source_target_pairs={{0,2},{1,3},{2,0},{3,1},{4,6},{5,7},{6,4},{7,5},{8,10},{9,11},{10,... | collective-permute-start | bytes 589832 | tf_op jit(solution)/shard_map/ppermute | solution.py:255
  69.2 1.8 %collective-permute-start.37 = (bf16[48,2048]{1,0:T(8,128)(2,1)S(1)}, bf16[48,2048]{1,0:T(8,128)(2,1)S(1)}, u32[]{:S(2)}, u32[]{:S(2)}) collective-permute-start(bf16[48,2048]{1,0:T(8,128)(2,1)S(1)} %get-tuple-element.80), channel_id=1, source_target_pairs={{0,6},{1,7},{2,4},{3,5},{4,2},{5,3},{6,0},{7,1},{8,14},{9,15},{10,... | collective-permute-start | bytes 589832 | tf_op jit(solution)/shard_map/ppermute | solution.py:255
  71.0 8.7 %collective-permute-done.14.refs_0_.chunk_ref = bf16[136,2048]{1,0:T(8,128)(2,1)S(1)} collective-permute-done((bf16[136,2048]{1,0:T(8,128)(2,1)S(1)}, bf16[136,2048]{1,0:T(8,128)(2,1)S(1)}, u32[]{:S(2)}, u32[]{:S(2)}) %collective-permute-start.14) | collective-permute-done | bytes 557088 | tf_op jit(solution)/shard_map/ppermute | solution.py:255
  79.7 1.4 shard_map.126
  81.1 1.8 %collective-permute-start.24 = (bf16[48,2048]{1,0:T(8,128)(2,1)S(1)}, bf16[48,2048]{1,0:T(8,128)(2,1)S(1)}, u32[]{:S(2)}, u32[]{:S(2)}) collective-permute-start(bf16[48,2048]{1,0:T(8,128)(2,1)S(1)} %get-tuple-element.66), channel_id=1, source_target_pairs={{0,2},{1,3},{2,0},{3,1},{4,6},{5,7},{6,4},{7,5},{8,10},{9,11},{10,... | collective-permute-start | bytes 589832 | tf_op jit(solution)/shard_map/ppermute | solution.py:255
  82.9 1.8 %collective-permute-start.26 = (bf16[48,2048]{1,0:T(8,128)(2,1)S(1)}, bf16[48,2048]{1,0:T(8,128)(2,1)S(1)}, u32[]{:S(2)}, u32[]{:S(2)}) collective-permute-start(bf16[48,2048]{1,0:T(8,128)(2,1)S(1)} %get-tuple-element.68), channel_id=1, source_target_pairs={{0,6},{1,7},{2,4},{3,5},{4,2},{5,3},{6,0},{7,1},{8,14},{9,15},{10,... | collective-permute-start | bytes 589832 | tf_op jit(solution)/shard_map/ppermute | solution.py:255
  86.0 2.5 %collective-permute-done.24.refs_1_ = bf16[48,2048]{1,0:T(8,128)(2,1)S(1)} collective-permute-done((bf16[48,2048]{1,0:T(8,128)(2,1)S(1)}, bf16[48,2048]{1,0:T(8,128)(2,1)S(1)}, u32[]{:S(2)}, u32[]{:S(2)}) %collective-permute-start.24) | collective-permute-done | bytes 196640 | tf_op jit(solution)/shard_map/ppermute | solution.py:255
  88.5 2.2 %collective-permute-done.25.refs_2_ = bf16[48,2048]{1,0:T(8,128)(2,1)S(1)} collective-permute-done((bf16[48,2048]{1,0:T(8,128)(2,1)S(1)}, bf16[48,2048]{1,0:T(8,128)(2,1)S(1)}, u32[]{:S(2)}, u32[]{:S(2)}) %collective-permute-start.25) | collective-permute-done | bytes 196640 | tf_op jit(solution)/shard_map/ppermute | solution.py:255
  90.7 3.3 %collective-permute-done.26.refs_3_ = bf16[48,2048]{1,0:T(8,128)(2,1)S(1)} collective-permute-done((bf16[48,2048]{1,0:T(8,128)(2,1)S(1)}, bf16[48,2048]{1,0:T(8,128)(2,1)S(1)}, u32[]{:S(2)}, u32[]{:S(2)}) %collective-permute-start.26) | collective-permute-done | bytes 196640 | tf_op jit(solution)/shard_map/ppermute | solution.py:255
  94.0 3.6 %shard_map.127 = (bf16[48,2048]{1,0:T(8,128)(2,1)S(1)}, bf16[48,2048]{1,0:T(8,128)(2,1)S(1)}, bf16[48,2048]{1,0:T(8,128)(2,1)S(1)}, bf16[48,2048]{1,0:T(8,128)(2,1)S(1)}) custom-call(s32[4]{0:T(128)S(1)} %pad_add_fusion.where_ref, bf16[48,2048]{1,0:T(8,128)(2,1)S(1)} %get-tuple-element.65.refs_0_, bf16[48,2048]{1,0:T(8,128)(2,1)S(1)} %collective-permute-done.24.refs_1_, ...), custom_call_target="tpu_custom_call" | custom-call | flops 2415919104 | bytes 13369360 | tf_op jit(solution)/shard_map/pallas_call | solution.py:137
  97.6 1.7 %collective-permute-start.27 = (bf16[48,2048]{1,0:T(8,128)(2,1)S(1)}, bf16[48,2048]{1,0:T(8,128)(2,1)S(1)}, u32[]{:S(2)}, u32[]{:S(2)}) collective-permute-start(bf16[48,2048]{1,0:T(8,128)(2,1)S(1)} %get-tuple-element.70), channel_id=1, source_target_pairs={{0,2},{1,3},{2,0},{3,1},{4,6},{5,7},{6,4},{7,5},{8,10},{9,11},{10,... | collective-permute-start | bytes 589832 | tf_op jit(solution)/shard_map/ppermute | solution.py:255
  99.6 1.5 collective-permute-start.29
  101.1 1.4 shard_map.123
  102.5 1.7 collective-permute-start.16
  105.3 1.8 %collective-permute-done.28.refs_2_ = bf16[48,2048]{1,0:T(8,128)(2,1)S(1)} collective-permute-done((bf16[48,2048]{1,0:T(8,128)(2,1)S(1)}, bf16[48,2048]{1,0:T(8,128)(2,1)S(1)}, u32[]{:S(2)}, u32[]{:S(2)}) %collective-permute-start.28) | collective-permute-done | bytes 196640 | tf_op jit(solution)/shard_map/ppermute | solution.py:255
  107.1 1.4 collective-permute-start.18
  109.7 1.4 collective-permute-done.29.refs_3_
  112.9 2.6 %collective-permute-done.17.refs_2_ = bf16[48,2048]{1,0:T(8,128)(2,1)S(1)} collective-permute-done((bf16[48,2048]{1,0:T(8,128)(2,1)S(1)}, bf16[48,2048]{1,0:T(8,128)(2,1)S(1)}, u32[]{:S(2)}, u32[]{:S(2)}) %collective-permute-start.17) | collective-permute-done | bytes 196640 | tf_op jit(solution)/shard_map/ppermute | solution.py:255
  115.5 2.2 %collective-permute-done.18.refs_3_ = bf16[48,2048]{1,0:T(8,128)(2,1)S(1)} collective-permute-done((bf16[48,2048]{1,0:T(8,128)(2,1)S(1)}, bf16[48,2048]{1,0:T(8,128)(2,1)S(1)}, u32[]{:S(2)}, u32[]{:S(2)}) %collective-permute-start.18) | collective-permute-done | bytes 196640 | tf_op jit(solution)/shard_map/ppermute | solution.py:255
  117.7 3.6 %shard_map.124 = (bf16[48,2048]{1,0:T(8,128)(2,1)S(1)}, bf16[48,2048]{1,0:T(8,128)(2,1)S(1)}, bf16[48,2048]{1,0:T(8,128)(2,1)S(1)}, bf16[48,2048]{1,0:T(8,128)(2,1)S(1)}) custom-call(s32[4]{0:T(128)S(1)} %pad_add_fusion.where_ref, bf16[48,2048]{1,0:T(8,128)(2,1)S(1)} %get-tuple-element.57.refs_0_, bf16[48,2048]{1,0:T(8,128)(2,1)S(1)} %collective-permute-done.16.refs_1_, ...), custom_call_target="tpu_custom_call" | custom-call | flops 2415919104 | bytes 13369360 | tf_op jit(solution)/shard_map/pallas_call | solution.py:137
  121.3 1.7 collective-permute-start.19
  124.9 1.4 shard_map.120
  126.3 1.7 collective-permute-start.5
  128.6 2.0 %collective-permute-done.19.refs_1_ = bf16[48,2048]{1,0:T(8,128)(2,1)S(1)} collective-permute-done((bf16[48,2048]{1,0:T(8,128)(2,1)S(1)}, bf16[48,2048]{1,0:T(8,128)(2,1)S(1)}, u32[]{:S(2)}, u32[]{:S(2)}) %collective-permute-start.19) | collective-permute-done | bytes 196640 | tf_op jit(solution)/shard_map/ppermute | solution.py:255
  130.5 1.4 collective-permute-start.7
  133.3 1.6 collective-permute-done.21.refs_3_
  138.3 2.0 %collective-permute-done.7.refs_3_ = bf16[48,2048]{1,0:T(8,128)(2,1)S(1)} collective-permute-done((bf16[48,2048]{1,0:T(8,128)(2,1)S(1)}, bf16[48,2048]{1,0:T(8,128)(2,1)S(1)}, u32[]{:S(2)}, u32[]{:S(2)}) %collective-permute-start.7) | collective-permute-done | bytes 196640 | tf_op jit(solution)/shard_map/ppermute | solution.py:255
  140.4 3.6 %shard_map.121 = (bf16[48,2048]{1,0:T(8,128)(2,1)S(1)}, bf16[48,2048]{1,0:T(8,128)(2,1)S(1)}, bf16[48,2048]{1,0:T(8,128)(2,1)S(1)}, bf16[48,2048]{1,0:T(8,128)(2,1)S(1)}) custom-call(s32[4]{0:T(128)S(1)} %pad_add_fusion.where_ref, bf16[48,2048]{1,0:T(8,128)(2,1)S(1)} %get-tuple-element.48.refs_0_, bf16[48,2048]{1,0:T(8,128)(2,1)S(1)} %collective-permute-done.5.refs_1_, ...), custom_call_target="tpu_custom_call" | custom-call | flops 2415919104 | bytes 13369360 | tf_op jit(solution)/shard_map/pallas_call | solution.py:137
  144.0 1.9 %collective-permute-start.10 = (bf16[48,2048]{1,0:T(8,128)(2,1)S(1)}, bf16[48,2048]{1,0:T(8,128)(2,1)S(1)}, u32[]{:S(2)}, u32[]{:S(2)}) collective-permute-start(bf16[48,2048]{1,0:T(8,128)(2,1)S(1)} %get-tuple-element.55), channel_id=1, source_target_pairs={{0,6},{1,7},{2,4},{3,5},{4,2},{5,3},{6,0},{7,1},{8,14},{9,15},{10,... | collective-permute-start | bytes 589832 | tf_op jit(solution)/shard_map/ppermute | solution.py:255
  147.6 3.3 %collective-permute-done.10.refs_3_ = bf16[48,2048]{1,0:T(8,128)(2,1)S(1)} collective-permute-done((bf16[48,2048]{1,0:T(8,128)(2,1)S(1)}, bf16[48,2048]{1,0:T(8,128)(2,1)S(1)}, u32[]{:S(2)}, u32[]{:S(2)}) %collective-permute-start.10) | collective-permute-done | bytes 196640 | tf_op jit(solution)/shard_map/ppermute | solution.py:255
  150.9 2.0 %collective-permute-done.8.refs_1_ = bf16[48,2048]{1,0:T(8,128)(2,1)S(1)} collective-permute-done((bf16[48,2048]{1,0:T(8,128)(2,1)S(1)}, bf16[48,2048]{1,0:T(8,128)(2,1)S(1)}, u32[]{:S(2)}, u32[]{:S(2)}) %collective-permute-start.8) | collective-permute-done | bytes 196640 | tf_op jit(solution)/shard_map/ppermute | solution.py:255
  156.2 15.6 %collective-permute-done.41.refs_6_ = bf16[128,2048]{1,0:T(8,128)(2,1)S(1)} collective-permute-done((bf16[128,2048]{1,0:T(8,128)(2,1)S(1)}, bf16[128,2048]{1,0:T(8,128)(2,1)S(1)}, u32[]{:S(2)}, u32[]{:S(2)}) %collective-permute-start.41) | collective-permute-done | bytes 524320 | tf_op jit(solution)/shard_map/ppermute | solution.py:255
  171.8 2.1 %shard_map.135 = bf16[128,2048]{1,0:T(8,128)(2,1)} custom-call(s32[4]{0:T(128)S(1)} %pad_add_fusion.where_ref, bf16[136,2048]{1,0:T(8,128)(2,1)S(1)} %get-tuple-element.47.refs_0_.chunk_ref, bf16[48,2048]{1,0:T(8,128)(2,1)S(1)} %get-tuple-element.52.refs_0_, bf16[48,2048]{1,0:T(8,128)(2,1)S(1)} %collective-permute-done.8.refs_1_, ...), custom_call_target="tpu_custom_call" | custom-call | flops 100663296 | bytes 2916368 | tf_op jit(solution)/shard_map/pallas_call | solution.py:137
  (83 shorter events, 26.4 us)
Async XLA Ops:
  1.5 7.8 %collective-permute-start = (bf16[16,512]{1,0:T(8,128)(2,1)S(1)}, bf16[16,512]{1,0:T(8,128)(2,1)S(1)}, u32[]{:S(2)}, u32[]{:S(2)}) collective-permute-start(bf16[16,512]{1,0:T(8,128)(2,1)S(1)} %pad_maximum_fusion), channel_id=1, source_target_pairs={{0,4},{4,8},{8,12},{12,16},{16,20},{20,24},{24,28},{28,0},{1,5},{5... | collective-permute-start | bytes 49160 | tf_op jit(solution)/shard_map/ppermute | solution.py:278
  9.3 1.0 copy-start.5
  12.1 2.7 %collective-permute-start.1 = (bf16[128,512]{1,0:T(8,128)(2,1)S(1)}, bf16[128,512]{1,0:T(8,128)(2,1)S(1)}, u32[]{:S(2)}, u32[]{:S(2)}) collective-permute-start(bf16[128,512]{1,0:T(8,128)(2,1)S(1)} %get-tuple-element.44), channel_id=1, source_target_pairs={{0,1},{1,0},{2,3},{3,2},{4,5},{5,4},{6,7},{7,6},{8,9},{9,8},{10,11... | collective-permute-start | bytes 393224 | tf_op jit(solution)/shard_map/ppermute | solution.py:289
  12.2 6.4 %collective-permute-start.2 = (bf16[128,512]{1,0:T(8,128)(2,1)S(1)}, bf16[128,512]{1,0:T(8,128)(2,1)S(1)}, u32[]{:S(2)}, u32[]{:S(2)}) collective-permute-start(bf16[128,512]{1,0:T(8,128)(2,1)S(1)} %get-tuple-element.45), channel_id=1, source_target_pairs={{0,2},{1,3},{2,0},{3,1},{4,6},{5,7},{6,4},{7,5},{8,10},{9,11},{10,... | collective-permute-start | bytes 393224 | tf_op jit(solution)/shard_map/ppermute | solution.py:289
  14.0 6.4 %collective-permute-start.3 = (bf16[128,512]{1,0:T(8,128)(2,1)S(1)}, bf16[128,512]{1,0:T(8,128)(2,1)S(1)}, u32[]{:S(2)}, u32[]{:S(2)}) collective-permute-start(bf16[128,512]{1,0:T(8,128)(2,1)S(1)} %get-tuple-element.46), channel_id=1, source_target_pairs={{0,3},{1,2},{2,1},{3,0},{4,7},{5,6},{6,5},{7,4},{8,11},{9,10},{10,... | collective-permute-start | bytes 393224 | tf_op jit(solution)/shard_map/ppermute | solution.py:289
  20.3 3.4 %copy-start.3 = (bf16[2048,2048]{1,0:T(8,128)(2,1)S(1)}, bf16[2048,2048]{1,0:T(8,128)(2,1)}, u32[]{:S(2)}) copy-start(bf16[2048,2048]{1,0:T(8,128)(2,1)} %refs_1_.1) | copy-start | bytes 25165828
  23.7 1.6 copy-start.4
  27.8 36.0 %copy-start = (bf16[1,2048,1024]{2,1,0:T(8,128)(2,1)S(1)}, bf16[1,2048,1024]{2,1,0:T(8,128)(2,1)}, u32[]{:S(2)}) copy-start(bf16[1,2048,1024]{2,1,0:T(8,128)(2,1)} %param.21) | copy-start | bytes 12582916
  27.8 36.0 %copy-start.1 = (bf16[1,2048,1024]{2,1,0:T(8,128)(2,1)S(1)}, bf16[1,2048,1024]{2,1,0:T(8,128)(2,1)}, u32[]{:S(2)}) copy-start(bf16[1,2048,1024]{2,1,0:T(8,128)(2,1)} %param.22) | copy-start | bytes 12582916
  27.8 36.0 %copy-start.2 = (bf16[1,1024,2048]{2,1,0:T(8,128)(2,1)S(1)}, bf16[1,1024,2048]{2,1,0:T(8,128)(2,1)}, u32[]{:S(2)}) copy-start(bf16[1,1024,2048]{2,1,0:T(8,128)(2,1)} %param.23) | copy-start | bytes 12582916
  30.2 16.7 %collective-permute-start.12 = (bf16[136,2048]{1,0:T(8,128)(2,1)S(1)}, bf16[136,2048]{1,0:T(8,128)(2,1)S(1)}, u32[]{:S(2)}, u32[]{:S(2)}) collective-permute-start(bf16[136,2048]{1,0:T(8,128)(2,1)S(1)} %get-tuple-element.47.refs_0_.chunk_ref), channel_id=1, source_target_pairs={{0,8},{1,9},{2,10},{3,11},{4,12},{5,13},{6,14},{7,15},{8,16},{9,17... | collective-permute-start | bytes 1671176 | tf_op jit(solution)/shard_map/ppermute | solution.py:255
  46.9 2.0 %collective-permute-start.31 = (bf16[136,2048]{1,0:T(8,128)(2,1)S(1)}, bf16[136,2048]{1,0:T(8,128)(2,1)S(1)}, u32[]{:S(2)}, u32[]{:S(2)}) collective-permute-start(bf16[136,2048]{1,0:T(8,128)(2,1)S(1)} %collective-permute-done.12.refs_0_.chunk_ref), channel_id=1, source_target_pairs={{0,1},{1,0},{2,3},{3,2},{4,5},{5,4},{6,7},{7,6},{8,9},{9,8},{10,11... | collective-permute-start | bytes 1671176 | tf_op jit(solution)/shard_map/ppermute | solution.py:255
  46.9 16.8 %collective-permute-start.13 = (bf16[136,2048]{1,0:T(8,128)(2,1)S(1)}, bf16[136,2048]{1,0:T(8,128)(2,1)S(1)}, u32[]{:S(2)}, u32[]{:S(2)}) collective-permute-start(bf16[136,2048]{1,0:T(8,128)(2,1)S(1)} %collective-permute-done.12.refs_0_.chunk_ref), channel_id=1, source_target_pairs={{0,8},{1,9},{2,10},{3,11},{4,12},{5,13},{6,14},{7,15},{8,16},{9,17... | collective-permute-start | bytes 1671176 | tf_op jit(solution)/shard_map/ppermute | solution.py:255
  50.3 13.5 %collective-permute-start.32 = (bf16[48,2048]{1,0:T(8,128)(2,1)S(1)}, bf16[48,2048]{1,0:T(8,128)(2,1)S(1)}, u32[]{:S(2)}, u32[]{:S(2)}) collective-permute-start(bf16[48,2048]{1,0:T(8,128)(2,1)S(1)} %get-tuple-element.74), channel_id=1, source_target_pairs={{0,2},{1,3},{2,0},{3,1},{4,6},{5,7},{6,4},{7,5},{8,10},{9,11},{10,... | collective-permute-start | bytes 589832 | tf_op jit(solution)/shard_map/ppermute | solution.py:255
  52.0 11.7 %collective-permute-start.33 = (bf16[48,2048]{1,0:T(8,128)(2,1)S(1)}, bf16[48,2048]{1,0:T(8,128)(2,1)S(1)}, u32[]{:S(2)}, u32[]{:S(2)}) collective-permute-start(bf16[48,2048]{1,0:T(8,128)(2,1)S(1)} %get-tuple-element.75), channel_id=1, source_target_pairs={{0,4},{1,5},{2,6},{3,7},{4,0},{5,1},{6,2},{7,3},{8,12},{9,13},{10,... | collective-permute-start | bytes 589832 | tf_op jit(solution)/shard_map/ppermute | solution.py:255
  52.0 11.7 %collective-permute-start.34 = (bf16[48,2048]{1,0:T(8,128)(2,1)S(1)}, bf16[48,2048]{1,0:T(8,128)(2,1)S(1)}, u32[]{:S(2)}, u32[]{:S(2)}) collective-permute-start(bf16[48,2048]{1,0:T(8,128)(2,1)S(1)} %get-tuple-element.76), channel_id=1, source_target_pairs={{0,6},{1,7},{2,4},{3,5},{4,2},{5,3},{6,0},{7,1},{8,14},{9,15},{10,... | collective-permute-start | bytes 589832 | tf_op jit(solution)/shard_map/ppermute | solution.py:255
  63.7 16.0 %collective-permute-start.14 = (bf16[136,2048]{1,0:T(8,128)(2,1)S(1)}, bf16[136,2048]{1,0:T(8,128)(2,1)S(1)}, u32[]{:S(2)}, u32[]{:S(2)}) collective-permute-start(bf16[136,2048]{1,0:T(8,128)(2,1)S(1)} %collective-permute-done.13.refs_0_.chunk_ref), channel_id=1, source_target_pairs={{0,8},{1,9},{2,10},{3,11},{4,12},{5,13},{6,14},{7,15},{8,16},{9,17... | collective-permute-start | bytes 1671176 | tf_op jit(solution)/shard_map/ppermute | solution.py:255
  63.7 16.0 %collective-permute-start.23 = (bf16[136,2048]{1,0:T(8,128)(2,1)S(1)}, bf16[136,2048]{1,0:T(8,128)(2,1)S(1)}, u32[]{:S(2)}, u32[]{:S(2)}) collective-permute-start(bf16[136,2048]{1,0:T(8,128)(2,1)S(1)} %collective-permute-done.13.refs_0_.chunk_ref), channel_id=1, source_target_pairs={{0,1},{1,0},{2,3},{3,2},{4,5},{5,4},{6,7},{7,6},{8,9},{9,8},{10,11... | collective-permute-start | bytes 1671176 | tf_op jit(solution)/shard_map/ppermute | solution.py:255
  67.4 15.5 %collective-permute-start.35 = (bf16[48,2048]{1,0:T(8,128)(2,1)S(1)}, bf16[48,2048]{1,0:T(8,128)(2,1)S(1)}, u32[]{:S(2)}, u32[]{:S(2)}) collective-permute-start(bf16[48,2048]{1,0:T(8,128)(2,1)S(1)} %get-tuple-element.78), channel_id=1, source_target_pairs={{0,2},{1,3},{2,0},{3,1},{4,6},{5,7},{6,4},{7,5},{8,10},{9,11},{10,... | collective-permute-start | bytes 589832 | tf_op jit(solution)/shard_map/ppermute | solution.py:255
  69.2 13.7 %collective-permute-start.36 = (bf16[48,2048]{1,0:T(8,128)(2,1)S(1)}, bf16[48,2048]{1,0:T(8,128)(2,1)S(1)}, u32[]{:S(2)}, u32[]{:S(2)}) collective-permute-start(bf16[48,2048]{1,0:T(8,128)(2,1)S(1)} %get-tuple-element.79), channel_id=1, source_target_pairs={{0,4},{1,5},{2,6},{3,7},{4,0},{5,1},{6,2},{7,3},{8,12},{9,13},{10,... | collective-permute-start | bytes 589832 | tf_op jit(solution)/shard_map/ppermute | solution.py:255
  69.2 15.5 %collective-permute-start.37 = (bf16[48,2048]{1,0:T(8,128)(2,1)S(1)}, bf16[48,2048]{1,0:T(8,128)(2,1)S(1)}, u32[]{:S(2)}, u32[]{:S(2)}) collective-permute-start(bf16[48,2048]{1,0:T(8,128)(2,1)S(1)} %get-tuple-element.80), channel_id=1, source_target_pairs={{0,6},{1,7},{2,4},{3,5},{4,2},{5,3},{6,0},{7,1},{8,14},{9,15},{10,... | collective-permute-start | bytes 589832 | tf_op jit(solution)/shard_map/ppermute | solution.py:255
  79.7 21.4 %collective-permute-start.15 = (bf16[136,2048]{1,0:T(8,128)(2,1)S(1)}, bf16[136,2048]{1,0:T(8,128)(2,1)S(1)}, u32[]{:S(2)}, u32[]{:S(2)}) collective-permute-start(bf16[136,2048]{1,0:T(8,128)(2,1)S(1)} %collective-permute-done.14.refs_0_.chunk_ref), channel_id=1, source_target_pairs={{0,1},{1,0},{2,3},{3,2},{4,5},{5,4},{6,7},{7,6},{8,9},{9,8},{10,11... | collective-permute-start | bytes 1671176 | tf_op jit(solution)/shard_map/ppermute | solution.py:255
  81.1 7.4 %collective-permute-start.24 = (bf16[48,2048]{1,0:T(8,128)(2,1)S(1)}, bf16[48,2048]{1,0:T(8,128)(2,1)S(1)}, u32[]{:S(2)}, u32[]{:S(2)}) collective-permute-start(bf16[48,2048]{1,0:T(8,128)(2,1)S(1)} %get-tuple-element.66), channel_id=1, source_target_pairs={{0,2},{1,3},{2,0},{3,1},{4,6},{5,7},{6,4},{7,5},{8,10},{9,11},{10,... | collective-permute-start | bytes 589832 | tf_op jit(solution)/shard_map/ppermute | solution.py:255
  82.9 7.8 %collective-permute-start.25 = (bf16[48,2048]{1,0:T(8,128)(2,1)S(1)}, bf16[48,2048]{1,0:T(8,128)(2,1)S(1)}, u32[]{:S(2)}, u32[]{:S(2)}) collective-permute-start(bf16[48,2048]{1,0:T(8,128)(2,1)S(1)} %get-tuple-element.67), channel_id=1, source_target_pairs={{0,4},{1,5},{2,6},{3,7},{4,0},{5,1},{6,2},{7,3},{8,12},{9,13},{10,... | collective-permute-start | bytes 589832 | tf_op jit(solution)/shard_map/ppermute | solution.py:255
  82.9 11.0 %collective-permute-start.26 = (bf16[48,2048]{1,0:T(8,128)(2,1)S(1)}, bf16[48,2048]{1,0:T(8,128)(2,1)S(1)}, u32[]{:S(2)}, u32[]{:S(2)}) collective-permute-start(bf16[48,2048]{1,0:T(8,128)(2,1)S(1)} %get-tuple-element.68), channel_id=1, source_target_pairs={{0,6},{1,7},{2,4},{3,5},{4,2},{5,3},{6,0},{7,1},{8,14},{9,15},{10,... | collective-permute-start | bytes 589832 | tf_op jit(solution)/shard_map/ppermute | solution.py:255
  85.9 18.3 %collective-permute-start.38 = (bf16[128,2048]{1,0:T(8,128)(2,1)S(1)}, bf16[128,2048]{1,0:T(8,128)(2,1)S(1)}, u32[]{:S(2)}, u32[]{:S(2)}) collective-permute-start(bf16[128,2048]{1,0:T(8,128)(2,1)S(1)} %shard_map.131), channel_id=1, source_target_pairs={{0,1},{1,0},{2,3},{3,2},{4,5},{5,4},{6,7},{7,6},{8,9},{9,8},{10,11... | collective-permute-start | bytes 1572872 | tf_op jit(solution)/shard_map/ppermute | solution.py:255
  97.6 7.7 %collective-permute-start.27 = (bf16[48,2048]{1,0:T(8,128)(2,1)S(1)}, bf16[48,2048]{1,0:T(8,128)(2,1)S(1)}, u32[]{:S(2)}, u32[]{:S(2)}) collective-permute-start(bf16[48,2048]{1,0:T(8,128)(2,1)S(1)} %get-tuple-element.70), channel_id=1, source_target_pairs={{0,2},{1,3},{2,0},{3,1},{4,6},{5,7},{6,4},{7,5},{8,10},{9,11},{10,... | collective-permute-start | bytes 589832 | tf_op jit(solution)/shard_map/ppermute | solution.py:255
  99.3 7.8 %collective-permute-start.28 = (bf16[48,2048]{1,0:T(8,128)(2,1)S(1)}, bf16[48,2048]{1,0:T(8,128)(2,1)S(1)}, u32[]{:S(2)}, u32[]{:S(2)}) collective-permute-start(bf16[48,2048]{1,0:T(8,128)(2,1)S(1)} %get-tuple-element.71), channel_id=1, source_target_pairs={{0,4},{1,5},{2,6},{3,7},{4,0},{5,1},{6,2},{7,3},{8,12},{9,13},{10,... | collective-permute-start | bytes 589832 | tf_op jit(solution)/shard_map/ppermute | solution.py:255
  99.6 11.5 %collective-permute-start.29 = (bf16[48,2048]{1,0:T(8,128)(2,1)S(1)}, bf16[48,2048]{1,0:T(8,128)(2,1)S(1)}, u32[]{:S(2)}, u32[]{:S(2)}) collective-permute-start(bf16[48,2048]{1,0:T(8,128)(2,1)S(1)} %get-tuple-element.72), channel_id=1, source_target_pairs={{0,6},{1,7},{2,4},{3,5},{4,2},{5,3},{6,0},{7,1},{8,14},{9,15},{10,... | collective-permute-start | bytes 589832 | tf_op jit(solution)/shard_map/ppermute | solution.py:255
  102.5 10.4 %collective-permute-start.16 = (bf16[48,2048]{1,0:T(8,128)(2,1)S(1)}, bf16[48,2048]{1,0:T(8,128)(2,1)S(1)}, u32[]{:S(2)}, u32[]{:S(2)}) collective-permute-start(bf16[48,2048]{1,0:T(8,128)(2,1)S(1)} %get-tuple-element.58), channel_id=1, source_target_pairs={{0,2},{1,3},{2,0},{3,1},{4,6},{5,7},{6,4},{7,5},{8,10},{9,11},{10,... | collective-permute-start | bytes 589832 | tf_op jit(solution)/shard_map/ppermute | solution.py:255
  104.3 19.3 %collective-permute-start.4 = (bf16[136,2048]{1,0:T(8,128)(2,1)S(1)}, bf16[136,2048]{1,0:T(8,128)(2,1)S(1)}, u32[]{:S(2)}, u32[]{:S(2)}) collective-permute-start(bf16[136,2048]{1,0:T(8,128)(2,1)S(1)} %get-tuple-element.47.refs_0_.chunk_ref), channel_id=1, source_target_pairs={{0,1},{1,0},{2,3},{3,2},{4,5},{5,4},{6,7},{7,6},{8,9},{9,8},{10,11... | collective-permute-start | bytes 1671176 | tf_op jit(solution)/shard_map/ppermute | solution.py:255
  105.2 10.3 %collective-permute-start.17 = (bf16[48,2048]{1,0:T(8,128)(2,1)S(1)}, bf16[48,2048]{1,0:T(8,128)(2,1)S(1)}, u32[]{:S(2)}, u32[]{:S(2)}) collective-permute-start(bf16[48,2048]{1,0:T(8,128)(2,1)S(1)} %get-tuple-element.59), channel_id=1, source_target_pairs={{0,4},{1,5},{2,6},{3,7},{4,0},{5,1},{6,2},{7,3},{8,12},{9,13},{10,... | collective-permute-start | bytes 589832 | tf_op jit(solution)/shard_map/ppermute | solution.py:255
  107.1 10.6 %collective-permute-start.18 = (bf16[48,2048]{1,0:T(8,128)(2,1)S(1)}, bf16[48,2048]{1,0:T(8,128)(2,1)S(1)}, u32[]{:S(2)}, u32[]{:S(2)}) collective-permute-start(bf16[48,2048]{1,0:T(8,128)(2,1)S(1)} %get-tuple-element.60), channel_id=1, source_target_pairs={{0,6},{1,7},{2,4},{3,5},{4,2},{5,3},{6,0},{7,1},{8,14},{9,15},{10,... | collective-permute-start | bytes 589832 | tf_op jit(solution)/shard_map/ppermute | solution.py:255
  111.1 15.2 %collective-permute-start.39 = (bf16[128,2048]{1,0:T(8,128)(2,1)S(1)}, bf16[128,2048]{1,0:T(8,128)(2,1)S(1)}, u32[]{:S(2)}, u32[]{:S(2)}) collective-permute-start(bf16[128,2048]{1,0:T(8,128)(2,1)S(1)} %shard_map.132), channel_id=1, source_target_pairs={{0,8},{1,9},{2,10},{3,11},{4,12},{5,13},{6,14},{7,15},{8,16},{9,17... | collective-permute-start | bytes 1572872 | tf_op jit(solution)/shard_map/ppermute | solution.py:255
  112.9 15.0 %collective-permute-start.30 = (bf16[128,2048]{1,0:T(8,128)(2,1)S(1)}, bf16[128,2048]{1,0:T(8,128)(2,1)S(1)}, u32[]{:S(2)}, u32[]{:S(2)}) collective-permute-start(bf16[128,2048]{1,0:T(8,128)(2,1)S(1)} %shard_map.128), channel_id=1, source_target_pairs={{0,1},{1,0},{2,3},{3,2},{4,5},{5,4},{6,7},{7,6},{8,9},{9,8},{10,11... | collective-permute-start | bytes 1572872 | tf_op jit(solution)/shard_map/ppermute | solution.py:255
  121.3 9.2 %collective-permute-start.19 = (bf16[48,2048]{1,0:T(8,128)(2,1)S(1)}, bf16[48,2048]{1,0:T(8,128)(2,1)S(1)}, u32[]{:S(2)}, u32[]{:S(2)}) collective-permute-start(bf16[48,2048]{1,0:T(8,128)(2,1)S(1)} %get-tuple-element.62), channel_id=1, source_target_pairs={{0,2},{1,3},{2,0},{3,1},{4,6},{5,7},{6,4},{7,5},{8,10},{9,11},{10,... | collective-permute-start | bytes 589832 | tf_op jit(solution)/shard_map/ppermute | solution.py:255
  123.0 10.3 %collective-permute-start.20 = (bf16[48,2048]{1,0:T(8,128)(2,1)S(1)}, bf16[48,2048]{1,0:T(8,128)(2,1)S(1)}, u32[]{:S(2)}, u32[]{:S(2)}) collective-permute-start(bf16[48,2048]{1,0:T(8,128)(2,1)S(1)} %get-tuple-element.63), channel_id=1, source_target_pairs={{0,4},{1,5},{2,6},{3,7},{4,0},{5,1},{6,2},{7,3},{8,12},{9,13},{10,... | collective-permute-start | bytes 589832 | tf_op jit(solution)/shard_map/ppermute | solution.py:255
  123.6 11.3 %collective-permute-start.21 = (bf16[48,2048]{1,0:T(8,128)(2,1)S(1)}, bf16[48,2048]{1,0:T(8,128)(2,1)S(1)}, u32[]{:S(2)}, u32[]{:S(2)}) collective-permute-start(bf16[48,2048]{1,0:T(8,128)(2,1)S(1)} %get-tuple-element.64), channel_id=1, source_target_pairs={{0,6},{1,7},{2,4},{3,5},{4,2},{5,3},{6,0},{7,1},{8,14},{9,15},{10,... | collective-permute-start | bytes 589832 | tf_op jit(solution)/shard_map/ppermute | solution.py:255
  126.3 11.3 %collective-permute-start.5 = (bf16[48,2048]{1,0:T(8,128)(2,1)S(1)}, bf16[48,2048]{1,0:T(8,128)(2,1)S(1)}, u32[]{:S(2)}, u32[]{:S(2)}) collective-permute-start(bf16[48,2048]{1,0:T(8,128)(2,1)S(1)} %get-tuple-element.49), channel_id=1, source_target_pairs={{0,2},{1,3},{2,0},{3,1},{4,6},{5,7},{6,4},{7,5},{8,10},{9,11},{10,... | collective-permute-start | bytes 589832 | tf_op jit(solution)/shard_map/ppermute | solution.py:255
  128.0 10.4 %collective-permute-start.6 = (bf16[48,2048]{1,0:T(8,128)(2,1)S(1)}, bf16[48,2048]{1,0:T(8,128)(2,1)S(1)}, u32[]{:S(2)}, u32[]{:S(2)}) collective-permute-start(bf16[48,2048]{1,0:T(8,128)(2,1)S(1)} %get-tuple-element.50), channel_id=1, source_target_pairs={{0,4},{1,5},{2,6},{3,7},{4,0},{5,1},{6,2},{7,3},{8,12},{9,13},{10,... | collective-permute-start | bytes 589832 | tf_op jit(solution)/shard_map/ppermute | solution.py:255
  130.5 9.8 %collective-permute-start.7 = (bf16[48,2048]{1,0:T(8,128)(2,1)S(1)}, bf16[48,2048]{1,0:T(8,128)(2,1)S(1)}, u32[]{:S(2)}, u32[]{:S(2)}) collective-permute-start(bf16[48,2048]{1,0:T(8,128)(2,1)S(1)} %get-tuple-element.51), channel_id=1, source_target_pairs={{0,6},{1,7},{2,4},{3,5},{4,2},{5,3},{6,0},{7,1},{8,14},{9,15},{10,... | collective-permute-start | bytes 589832 | tf_op jit(solution)/shard_map/ppermute | solution.py:255
  133.3 21.0 %collective-permute-start.40 = (bf16[128,2048]{1,0:T(8,128)(2,1)S(1)}, bf16[128,2048]{1,0:T(8,128)(2,1)S(1)}, u32[]{:S(2)}, u32[]{:S(2)}) collective-permute-start(bf16[128,2048]{1,0:T(8,128)(2,1)S(1)} %shard_map.133), channel_id=1, source_target_pairs={{0,8},{1,9},{2,10},{3,11},{4,12},{5,13},{6,14},{7,15},{8,16},{9,17... | collective-permute-start | bytes 1572872 | tf_op jit(solution)/shard_map/ppermute | solution.py:255
  136.2 18.1 %collective-permute-start.22 = (bf16[128,2048]{1,0:T(8,128)(2,1)S(1)}, bf16[128,2048]{1,0:T(8,128)(2,1)S(1)}, u32[]{:S(2)}, u32[]{:S(2)}) collective-permute-start(bf16[128,2048]{1,0:T(8,128)(2,1)S(1)} %shard_map.125), channel_id=1, source_target_pairs={{0,1},{1,0},{2,3},{3,2},{4,5},{5,4},{6,7},{7,6},{8,9},{9,8},{10,11... | collective-permute-start | bytes 1572872 | tf_op jit(solution)/shard_map/ppermute | solution.py:255
  144.0 6.9 %collective-permute-start.10 = (bf16[48,2048]{1,0:T(8,128)(2,1)S(1)}, bf16[48,2048]{1,0:T(8,128)(2,1)S(1)}, u32[]{:S(2)}, u32[]{:S(2)}) collective-permute-start(bf16[48,2048]{1,0:T(8,128)(2,1)S(1)} %get-tuple-element.55), channel_id=1, source_target_pairs={{0,6},{1,7},{2,4},{3,5},{4,2},{5,3},{6,0},{7,1},{8,14},{9,15},{10,... | collective-permute-start | bytes 589832 | tf_op jit(solution)/shard_map/ppermute | solution.py:255
  145.9 6.9 %collective-permute-start.8 = (bf16[48,2048]{1,0:T(8,128)(2,1)S(1)}, bf16[48,2048]{1,0:T(8,128)(2,1)S(1)}, u32[]{:S(2)}, u32[]{:S(2)}) collective-permute-start(bf16[48,2048]{1,0:T(8,128)(2,1)S(1)} %get-tuple-element.53), channel_id=1, source_target_pairs={{0,2},{1,3},{2,0},{3,1},{4,6},{5,7},{6,4},{7,5},{8,10},{9,11},{10,... | collective-permute-start | bytes 589832 | tf_op jit(solution)/shard_map/ppermute | solution.py:255
  146.4 6.6 %collective-permute-start.9 = (bf16[48,2048]{1,0:T(8,128)(2,1)S(1)}, bf16[48,2048]{1,0:T(8,128)(2,1)S(1)}, u32[]{:S(2)}, u32[]{:S(2)}) collective-permute-start(bf16[48,2048]{1,0:T(8,128)(2,1)S(1)} %get-tuple-element.54), channel_id=1, source_target_pairs={{0,4},{1,5},{2,6},{3,7},{4,0},{5,1},{6,2},{7,3},{8,12},{9,13},{10,... | collective-permute-start | bytes 589832 | tf_op jit(solution)/shard_map/ppermute | solution.py:255
  154.2 2.0 %collective-permute-start.11 = (bf16[128,2048]{1,0:T(8,128)(2,1)S(1)}, bf16[128,2048]{1,0:T(8,128)(2,1)S(1)}, u32[]{:S(2)}, u32[]{:S(2)}) collective-permute-start(bf16[128,2048]{1,0:T(8,128)(2,1)S(1)} %shard_map.122), channel_id=1, source_target_pairs={{0,1},{1,0},{2,3},{3,2},{4,5},{5,4},{6,7},{7,6},{8,9},{9,8},{10,11... | collective-permute-start | bytes 1572872 | tf_op jit(solution)/shard_map/ppermute | solution.py:255
  155.6 16.2 %collective-permute-start.41 = (bf16[128,2048]{1,0:T(8,128)(2,1)S(1)}, bf16[128,2048]{1,0:T(8,128)(2,1)S(1)}, u32[]{:S(2)}, u32[]{:S(2)}) collective-permute-start(bf16[128,2048]{1,0:T(8,128)(2,1)S(1)} %shard_map.134), channel_id=1, source_target_pairs={{0,8},{1,9},{2,10},{3,11},{4,12},{5,13},{6,14},{7,15},{8,16},{9,17... | collective-permute-start | bytes 1572872 | tf_op jit(solution)/shard_map/ppermute | solution.py:255
  (4 other events, 3.1 us)

commit v4 on v3

v4 whole, which is shorter than its diff:
```python
import functools

import jax
import jax.numpy as jnp
from jax import lax
from jax.experimental import pallas as pl
from jax.experimental.pallas import tpu as pltpu
from jax.sharding import PartitionSpec as P


GROUPS = 4
CORES = 2
COVER_FLOPS = 40_000_000_000

norm_eps = 1e-05
clamp_limit = 7.0
sigmoid_alpha = 1.702
longest_window = 16
VMEM_BYTES = 12 * 1024 * 1024


def dot32(a, b):
    return jnp.dot(a, b, preferred_element_type=jnp.float32)


def cut_kernel(where_ref, rows_ref, docs_ref, *refs):
    out_refs, rim_ref, ext_ref = refs[:-2], refs[-2], refs[-1]
    row_count, channels = rows_ref.shape
    rim = rim_ref.shape[0]
    block = row_count // len(out_refs)
    ext_ref[0:rim, :] = jnp.zeros((rim, channels), jnp.bfloat16)
    ext_ref[rim:, :] = rows_ref[...]
    for d in range(len(out_refs)):
        start = pl.multiple_of((where_ref[1] ^ d) * block, block)
        out_refs[d][...] = ext_ref[pl.ds(start, block + rim), :]
    docs = docs_ref[docs_ref.shape[0] - 1 :, :][:, block - rim :] + 1
    line = jnp.concatenate(
        [docs.astype(jnp.float32), jnp.zeros((1, channels - rim), jnp.float32)], 1
    )
    tail = rows_ref[row_count - rim :, :].astype(jnp.float32)
    first = lax.broadcasted_iota(jnp.int32, (rim, channels), 0) == 0
    rim_ref[...] = jnp.where(first, line, tail).astype(jnp.bfloat16)


def pool_rows(where_ref, docs_ref, block_refs, rim_refs, ext_ref, groups):
    mine = where_ref[1]
    parts, tokens_rim, channels = ext_ref.shape
    rim = rim_refs[0].shape[0]
    block = tokens_rim - rim
    for d in range(parts):
        ext_ref[mine ^ d] = block_refs[d][...]

    @pl.when(mine == 0)
    def _():
        for d in range(parts):
            ext_ref[d, 0:rim, :] = rim_refs[d][...]

    rim_docs = (rim_refs[0][0:1, 0:rim].astype(jnp.float32) - 1.0).astype(jnp.int32)
    rim_docs = jnp.where(where_ref[4] == 0, -1, rim_docs)
    here = docs_ref[pl.ds(mine, 1), :]
    previous = docs_ref[pl.ds(jnp.maximum(mine - 1, 0), 1), :][:, block - rim :]
    col_docs = jnp.concatenate([jnp.where(mine == 0, rim_docs, previous), here], 1)
    at_row = lax.broadcasted_iota(jnp.int32, (block, tokens_rim), 0)
    at_col = lax.broadcasted_iota(jnp.int32, (block, tokens_rim), 1)
    back = at_row + rim - at_col
    row_docs = jnp.sum(
        jnp.where(back == 0, jnp.broadcast_to(col_docs, back.shape), 0), 1, keepdims=True
    )
    alike = (col_docs == row_docs) & (back >= 0)
    values = jnp.concatenate([ext_ref[d] for d in range(parts)], 1)
    width = parts * channels // groups
    mixed = []
    for g in range(groups):
        lanes = values[:, g * width : (g + 1) * width]
        band = jnp.where(alike & (back < 2 << g), 1.0, 0.0)
        count = jnp.sum(band, 1, keepdims=True)
        total = dot32(band.astype(jnp.bfloat16), lanes)
        mixed.append((total / count - lanes[rim:, :].astype(jnp.float32)).astype(jnp.bfloat16))
    return mixed


def named_experts(where_ref, routes_t, chips):
    offset = lax.broadcasted_iota(jnp.int32, (chips, routes_t.shape[1]), 0)
    here = (offset ^ where_ref[2]) * CORES + where_ref[3] + where_ref[0] * (chips * CORES)
    return [routes_t[j : j + 1, :] == here for j in range(routes_t.shape[0])]


def slot_table(matches, capacity):
    count, tokens = matches[0].shape
    named = matches[0]
    for match in matches[1:]:
        named = named | match
    earlier = (
        lax.broadcasted_iota(jnp.int32, (tokens, tokens), 0)
        < lax.broadcasted_iota(jnp.int32, (tokens, tokens), 1)
    )
    ones = jnp.where(named, 1.0, 0.0)
    rank = dot32(ones.astype(jnp.bfloat16), jnp.where(earlier, 1.0, 0.0).astype(jnp.bfloat16))
    held = jnp.where(named, rank, -1.0).astype(jnp.bfloat16)
    slots = count * capacity
    low = lax.broadcasted_iota(jnp.int32, (slots, count), 1) * capacity
    slot = lax.broadcasted_iota(jnp.int32, (slots, count), 0)
    inside = (slot >= low) & (slot < low + capacity)
    spread = jnp.where(inside, 1.0, 0.0).astype(jnp.bfloat16)
    place = jnp.sum(jnp.where(inside, slot - low, 0), 1, keepdims=True).astype(jnp.float32)
    return dot32(spread, held) == place, spread


def mixer_kernel(
    where_ref, routes_ref, weights_ref, docs_ref, gs_ref, stream_ref, gain_ref, gw_ref, ow_ref,
    *refs
):
    resid_ref, upper_ref, lower_ref, ext_ref = refs[-4:]
    parts = ext_ref.shape[0]
    groups, width, _ = gw_ref.shape
    tokens = stream_ref.shape[0]
    mixed = pool_rows(where_ref, docs_ref, refs[:parts], refs[parts : 2 * parts], ext_ref, groups)
    scaled = []
    for g in range(groups):
        lanes = slice(g * width, (g + 1) * width)
        scaled.append((dot32(mixed[g], gw_ref[g]) * gs_ref[:, lanes]).astype(jnp.bfloat16))
    mixer_out = dot32(jnp.concatenate(scaled, 1), ow_ref[...])
    resid = (stream_ref[...].astype(jnp.float32) + mixer_out).astype(jnp.bfloat16)
    resid_ref[...] = resid
    values = resid.astype(jnp.float32)
    inverse = lax.rsqrt(jnp.mean(values * values, -1, keepdims=True) + norm_eps)
    normed = (values * inverse * gain_ref[...]).astype(jnp.bfloat16)
    half = upper_ref.shape[0]
    upper_ref[...] = normed[0:half]
    lower_ref[0 : tokens - half, :] = normed[half:]
    top = routes_ref.shape[0]
    weights = weights_ref[...]
    high = weights.astype(jnp.bfloat16)
    low = (weights - high.astype(jnp.float32)).astype(jnp.bfloat16)
    routes_t = routes_ref[...]
    lines = [piece.astype(jnp.float32)[j : j + 1, :] for piece in (routes_t, high, low)
             for j in range(top)]
    line = jnp.concatenate(lines, 1)
    line = jnp.pad(line, ((0, 0), (0, lower_ref.shape[1] - line.shape[1])))
    rest = lower_ref.shape[0] - (tokens - half)
    lower_ref[tokens - half :, :] = jnp.broadcast_to(line, (rest, line.shape[1])).astype(jnp.bfloat16)


def read_table(lower_ref, tokens, top):
    line = lower_ref[lower_ref.shape[0] - 8 :, :].astype(jnp.float32)
    rows = [line[0:1, j * tokens : (j + 1) * tokens] for j in range(3 * top)]
    pieces = [jnp.concatenate(rows[k * top : (k + 1) * top], 0) for k in range(3)]
    return pieces[0].astype(jnp.int32), pieces[1], pieces[2]


def call(kernel, shapes, args, flops, scratch=(), limit=VMEM_BYTES):
    specs = [pl.BlockSpec(memory_space=pltpu.SMEM)]
    specs += [pl.BlockSpec(memory_space=pltpu.VMEM)] * (len(args) - 1)
    return pl.pallas_call(
        kernel,
        out_shape=tuple(shapes),
        in_specs=specs,
        out_specs=(pl.BlockSpec(memory_space=pltpu.VMEM),) * len(shapes),
        scratch_shapes=scratch,
        compiler_params=pltpu.CompilerParams(vmem_limit_bytes=limit),
        cost_estimate=pl.CostEstimate(
            flops=flops, transcendentals=0, bytes_accessed=sum(a.nbytes for a in args)
        ),
    )(*args)


def pick_kernel(where_ref, *refs, tokens, top, capacity):
    chunk_refs, send_refs = refs[: 2 * CORES], refs[2 * CORES :]
    chips = len(send_refs)
    for k in range(CORES):
        upper_ref, lower_ref = chunk_refs[2 * k : 2 * k + 2]
        routes_t, _, _ = read_table(lower_ref, tokens, top)
        taken, _ = slot_table(named_experts(where_ref, routes_t, chips), capacity)
        rest = tokens - upper_ref.shape[0]
        rows = jnp.concatenate([upper_ref[...], lower_ref[0:rest, :]], 0)
        picked = dot32(jnp.where(taken, 1.0, 0.0).astype(jnp.bfloat16), rows)
        picked = picked.astype(jnp.bfloat16)
        for d in range(chips):
            rows = picked[d * capacity : (d + 1) * capacity]
            send_refs[d][k * capacity : (k + 1) * capacity, :] = rows


def weighted_sum(where_ref, lower_ref, back_refs, k, tokens, top, capacity):
    routes_t, *weights = read_table(lower_ref, tokens, top)
    matches = named_experts(where_ref, routes_t, len(back_refs))
    taken, spread = slot_table(matches, capacity)
    back = jnp.concatenate([ref[k * capacity : (k + 1) * capacity, :] for ref in back_refs], 0)
    total = jnp.zeros((tokens, back.shape[1]), jnp.float32)
    for piece in weights:
        weight = jnp.zeros(matches[0].shape, jnp.float32)
        for j, match in enumerate(matches):
            weight = weight + jnp.where(match, piece[j : j + 1, :], 0.0)
        factor = jnp.where(taken, dot32(spread, weight.astype(jnp.bfloat16)), 0.0)
        total = total + lax.dot_general(
            factor.astype(jnp.bfloat16), back, (((0,), (0,)), ((), ())),
            preferred_element_type=jnp.float32,
        )
    return total


def share_kernel(where_ref, own_ref, other_ref, *refs, tokens, top, capacity):
    back_refs, (given_ref, kept_ref) = refs[:-2], refs[-2:]
    total = weighted_sum(where_ref, other_ref, back_refs, 1, tokens, top, capacity)
    given_ref[...] = total.astype(jnp.bfloat16)
    kept_ref[...] = weighted_sum(where_ref, own_ref, back_refs, 0, tokens, top, capacity)


def sum_kernel(where_ref, kept_ref, got_ref, *refs, start):
    size = refs[-1].shape[0]
    rows = slice(start, start + size)
    total = kept_ref[rows, :] + got_ref[rows, :].astype(jnp.float32)
    for ref in refs[:-1]:
        total = total + ref[...].astype(jnp.float32)
    refs[-1][...] = total.astype(jnp.bfloat16)


def final_kernel(where_ref, kept_ref, got_ref, resid_ref, *refs):
    total = kept_ref[...] + got_ref[...].astype(jnp.float32) + resid_ref[...].astype(jnp.float32)
    if len(refs) > 1:
        total = total + jnp.concatenate([ref[...] for ref in refs[:-1]], 0).astype(jnp.float32)
    refs[-1][...] = total.astype(jnp.bfloat16)


def expert_kernel(where_ref, *refs):
    chips = (len(refs) - 3) // 2
    row_refs, (gate_ref, up_ref, down_ref), out_refs = refs[:chips], refs[chips : chips + 3], refs[chips + 3 :]
    rows = jnp.concatenate([ref[...] for ref in row_refs], 0)
    hidden = gate_ref.shape[1]
    cut = min(hidden, 256)
    total = None
    for start in range(0, hidden, cut):
        lanes = slice(start, start + cut)
        gated = jnp.minimum(dot32(rows, gate_ref[:, lanes]), clamp_limit)
        linear = jnp.clip(dot32(rows, up_ref[:, lanes]), -clamp_limit, clamp_limit)
        activated = (gated * jax.nn.sigmoid(sigmoid_alpha * gated) * (linear + 1.0)).astype(
            jnp.bfloat16
        )
        part = dot32(activated, down_ref[lanes, :])
        total = part if total is None else total + part
    result = total.astype(jnp.bfloat16)
    length = row_refs[0].shape[0]
    for d in range(chips):
        out_refs[d][...] = result[d * length : (d + 1) * length]


in_vmem = functools.partial(pltpu.with_memory_space_constraint, memory_space=pltpu.VMEM)


def body(
    stream,
    projected,
    segments,
    group_weight,
    group_scale,
    out_weight,
    ffn_gain,
    routes,
    route_weights,
    expert_gate,
    expert_up,
    expert_down,
    *,
    planes,
):
    row_count, channels = projected.shape
    tp_count = lax.axis_size("tp")
    sp_count = lax.axis_size("sp")
    width = channels * tp_count
    group_width = width // GROUPS
    tokens, top = routes.shape
    devices = sp_count * tp_count
    count = devices // planes
    chips = count // CORES
    capacity = 3 * tokens * top // (2 * devices)
    hidden = expert_gate.shape[2]
    every = ("sp", "tp")
    sp_index, tp_index = lax.axis_index("sp"), lax.axis_index("tp")
    device = sp_index * tp_count + tp_index
    where = jnp.stack(
        [device // count, tp_index, device % count // CORES, device % CORES, sp_index]
    ).astype(jnp.int32)
    sizes = dict(tokens=tokens, top=top, capacity=capacity)

    def move(value, to):
        return lax.ppermute(value, every, [(i, to(i)) for i in range(devices)])

    def hop(value):
        return move(value, lambda i: (i + count) % devices)

    def swap(value):
        return move(value, lambda i: i ^ 1)

    def in_plane(blocks):
        moved = [blocks[0]]
        for d in range(1, chips):
            moved.append(move(blocks[d], lambda i: i ^ (d * CORES)))
        return moved

    rim = longest_window
    docs = segments.reshape(tp_count, tokens)
    part = jax.ShapeDtypeStruct((tokens + rim, channels), jnp.bfloat16)
    *cuts, tail = call(
        cut_kernel,
        [part] * tp_count + [jax.ShapeDtypeStruct((rim, channels), jnp.bfloat16)],
        [where, projected, docs],
        COVER_FLOPS,
        [pltpu.VMEM((row_count + rim, channels), jnp.bfloat16)],
    )

    def beside(i, d, ahead):
        sp, tp = i // tp_count, i % tp_count
        return (sp + ahead) % sp_count * tp_count + (tp ^ d)

    blocks, rims = [cuts[0]], []
    for d in range(1, tp_count):
        blocks.append(move(cuts[d], lambda i: beside(i, d, 0)))
    for d in range(tp_count):
        rims.append(move(tail, lambda i: beside(i, d, 1)))

    shape = jax.ShapeDtypeStruct((tokens, width), jnp.bfloat16)
    block = jax.ShapeDtypeStruct((CORES * capacity, width), jnp.bfloat16)
    half = tokens // 2
    piece = jax.ShapeDtypeStruct((half, width), jnp.bfloat16)
    resid, *chunk = call(
        mixer_kernel,
        [shape, piece, jax.ShapeDtypeStruct((tokens - half + 8, width), jnp.bfloat16)],
        [
            where, routes.T, route_weights.T, docs, in_vmem(group_scale.reshape(1, -1)),
            in_vmem(stream), in_vmem(ffn_gain.reshape(1, -1)), in_vmem(group_weight),
            in_vmem(out_weight), *blocks, *rims,
        ],
        2 * tokens * width * (width + group_width),
        [pltpu.VMEM((tp_count, tokens + rim, channels), jnp.bfloat16)],
    )
    small = 2 * tokens * count * capacity * width
    matrices = [in_vmem(expert_gate[0]), in_vmem(expert_up[0]), in_vmem(expert_down[0])]

    def dispatch(pair):
        rows = call(
            functools.partial(pick_kernel, **sizes), [block] * chips, [where, *pair],
            small,
        )
        return in_plane(rows)

    def experts(rows):
        results = call(
            expert_kernel, [block] * chips, [where, *rows, *matrices],
            6 * count * capacity * width * hidden,
        )
        return in_plane(results)

    def share(pair, back):
        given, kept = call(
            functools.partial(share_kernel, **sizes),
            [shape, jax.ShapeDtypeStruct(shape.shape, jnp.float32)],
            [where, pair[1], pair[3], *back], 2 * small,
        )
        return kept, swap(given)

    chunks = [chunk]
    for _ in range(1, planes):
        chunks.append([hop(chunks[-1][h]) for h in range(2)])
    pairs = []
    for s in range(planes):
        pairs.append(chunks[s] + [swap(chunks[s][h]) for h in range(2)])
    arrived = [dispatch(pairs[s]) for s in range(planes)]
    returned = [experts(arrived[s]) for s in range(planes)]
    carried = [[], []]
    for s in range(1, planes):
        shares = share(pairs[s], returned[s])
        for h in range(2):
            (total,) = call(
                functools.partial(sum_kernel, start=h * half), [piece],
                [where, *shares, *carried[h]], tokens * width,
            )
            carried[h] = [hop(total)]
    shares = share(pairs[0], returned[0])
    (out,) = call(
        final_kernel, [shape], [where, *shares, resid, *carried[0], *carried[1]],
        tokens * width,
    )
    return out


def plane_count(mesh):
    sizes = mesh.shape
    heights = {getattr(d, "coords", (0, 0, -1))[2] for d in mesh.devices.flat}
    if -1 in heights:
        return max(1, sizes["sp"] // max(1, sizes["tp"] // 2))
    return len(heights)


def solution(mesh):
    in_specs = (
        P(("sp", "tp"), None),
        P("sp", "tp"),
        P("sp"),
        P(),
        P(),
        P(),
        P(),
        P(("sp", "tp"), None),
        P(("sp", "tp"), None),
        P(("sp", "tp"), None, None),
        P(("sp", "tp"), None, None),
        P(("sp", "tp"), None, None),
    )
    out_specs = P(("sp", "tp"), None)
    planes = plane_count(mesh)

    def layer(*args):
        return body(*args, planes=planes)

    return jax.shard_map(layer, mesh=mesh, in_specs=in_specs, out_specs=out_specs, check_vma=False)
```

time: 174 us -> 174 us (level)
  waiting for transfers between devices: 93.5 us -> 102 us
  local copies, waits for them, and re-layouts: 9.88 us -> 2.19 us
  other arithmetic: 2.29 us -> 0.01 us
    ppermute x38 -> x55, waiting for transfers between devices: 83.9 us -> 102 us  [move(): return lax.ppermute(value, every, [(i, to(i)) for i in range(devices)])]
    ppermute x4 -> x0, waiting for transfers between devices: 9.54 us -> none  [the longest x3 5.55 us: body(): blocks.append(lax.ppermute(mixed[d], 'tp', pairs))]
    unnamed x20 -> x26, local copies, waits for them, and re-layouts: 9.14 us -> 2.11 us
    ppermute x38 -> x55, starting transfers between devices: 28.6 us -> 33.9 us  [move(): return lax.ppermute(value, every, [(i, to(i)) for i in range(devices)])]
    ppermute x4 -> x0, starting transfers between devices: 4.94 us -> none  [the longest x1 3.02 us: body(): lax.ppermute(payload, 'sp', [(i, (i + 1) % sp_count) for i in range(sp_co...]
    pallas_call x18 -> x21, Pallas kernels: 34.4 us -> 36.1 us  [call(): pl.pallas_call(kernel, out_shape=tuple(shapes), in_specs=specs, out_specs...]
  transfers between devices with their start and end apart: 42 -> 55, of which waited for: 26 -> 28; matrix products, arithmetic and copies ran while one was open for 1% -> 0% of each run, Pallas kernels for 17% -> 18%
where the time goes in v4:
time: 174 us
  waiting for transfers between devices  102 us (59%)
  Pallas kernels  36.1 us (21%)
  starting transfers between devices  33.9 us (19%)
  local copies, waits for them, and re-layouts  2.19 us (1%)
    ppermute x55, waiting for transfers between devices, move(): return lax.ppermute(value, every, [(i, to(i)) for i in range(devices)])  102 us
    pallas_call x21, Pallas kernels, call(): pl.pallas_call(kernel, out_shape=tuple(shapes), in_specs=specs, out_specs...  36.1 us
    ppermute x55, starting transfers between devices, move(): return lax.ppermute(value, every, [(i, to(i)) for i in range(devices)])  33.9 us
  transfers between devices with their start and end apart: 55, of which 28 were waited for; matrix products, arithmetic and copies ran while one was open for 0% of the time, Pallas kernels for 18%

profile of v4, /device:TPU:0, one launch (start us, length us, event | category | flops | bytes accessed | tf_op | source)
XLA Modules:
  0.0 174.2 jit_solution(9847768653180622360)
XLA Ops:
  3.4 2.6 %collective-permute-start.1 = (bf16[144,512]{1,0:T(8,128)(2,1)S(1)}, bf16[144,512]{1,0:T(8,128)(2,1)S(1)}, u32[]{:S(2)}, u32[]{:S(2)}) collective-permute-start(bf16[144,512]{1,0:T(8,128)(2,1)S(1)} %get-tuple-element.55), channel_id=1, source_target_pairs={{0,2},{1,3},{2,0},{3,1},{4,6},{5,7},{6,4},{7,5},{8,10},{9,11},{10,... | collective-permute-start | bytes 442376 | tf_op jit(solution)/shard_map/ppermute | solution.py:285
  6.0 1.7 collective-permute-start.3
  7.7 1.2 collective-permute-start.4
  8.9 3.5 %collective-permute-done.3.refs_4_ = bf16[16,512]{1,0:T(8,128)(2,1)S(1)} collective-permute-done((bf16[16,512]{1,0:T(8,128)(2,1)S(1)}, bf16[16,512]{1,0:T(8,128)(2,1)S(1)}, u32[]{:S(2)}, u32[]{:S(2)}) %collective-permute-start.3) | collective-permute-done | bytes 16416 | tf_op jit(solution)/shard_map/ppermute | solution.py:285
  13.6 6.2 %collective-permute-done.5.refs_6_ = bf16[16,512]{1,0:T(8,128)(2,1)S(1)} collective-permute-done((bf16[16,512]{1,0:T(8,128)(2,1)S(1)}, bf16[16,512]{1,0:T(8,128)(2,1)S(1)}, u32[]{:S(2)}, u32[]{:S(2)}) %collective-permute-start.5) | collective-permute-done | bytes 16416 | tf_op jit(solution)/shard_map/ppermute | solution.py:285
  20.5 2.7 %shard_map.119 = (bf16[128,2048]{1,0:T(8,128)(2,1)S(1)}, bf16[64,2048]{1,0:T(8,128)(2,1)S(1)}, bf16[72,2048]{1,0:T(8,128)(2,1)S(1)}) custom-call(s32[5]{0:T(128)S(1)} %stack.23.where_ref, s32[4,128]{1,0:T(4,128)S(1)} %bitcast.29, f32[4,128]{1,0:T(4,128)S(1)} %bitcast.30, s32[4,128]{1,0:T(4,128)S(1)} %bitcast.32, f32[1,2048]{1,0:T(1,128)S(1)} %bitcast.27, ...), custom_call_target="tpu_custom_call" | custom-call | flops 1342177280 | bytes 11687956 | tf_op jit(solution)/shard_map/pallas_call | solution.py:154
  23.4 11.5 %collective-permute-done.16.refs_1_.own_ref = bf16[72,2048]{1,0:T(8,128)(2,1)S(1)} collective-permute-done((bf16[72,2048]{1,0:T(8,128)(2,1)S(1)}, bf16[72,2048]{1,0:T(8,128)(2,1)S(1)}, u32[]{:S(2)}, u32[]{:S(2)}) %collective-permute-start.16) | collective-permute-done | bytes 294944 | tf_op jit(solution)/shard_map/ppermute | solution.py:285
  34.9 5.6 %collective-permute-done.20.refs_0_ = bf16[64,2048]{1,0:T(8,128)(2,1)S(1)} collective-permute-done((bf16[64,2048]{1,0:T(8,128)(2,1)S(1)}, bf16[64,2048]{1,0:T(8,128)(2,1)S(1)}, u32[]{:S(2)}, u32[]{:S(2)}) %collective-permute-start.20) | collective-permute-done | bytes 262176 | tf_op jit(solution)/shard_map/ppermute | solution.py:285
  41.0 5.8 %collective-permute-done.17.refs_1_.own_ref = bf16[72,2048]{1,0:T(8,128)(2,1)S(1)} collective-permute-done((bf16[72,2048]{1,0:T(8,128)(2,1)S(1)}, bf16[72,2048]{1,0:T(8,128)(2,1)S(1)}, u32[]{:S(2)}, u32[]{:S(2)}) %collective-permute-start.17) | collective-permute-done | bytes 294944 | tf_op jit(solution)/shard_map/ppermute | solution.py:285
  46.8 4.8 %collective-permute-done.21.refs_0_ = bf16[64,2048]{1,0:T(8,128)(2,1)S(1)} collective-permute-done((bf16[64,2048]{1,0:T(8,128)(2,1)S(1)}, bf16[64,2048]{1,0:T(8,128)(2,1)S(1)}, u32[]{:S(2)}, u32[]{:S(2)}) %collective-permute-start.21) | collective-permute-done | bytes 262176 | tf_op jit(solution)/shard_map/ppermute | solution.py:285
  51.9 1.4 shard_map.129
  53.3 1.6 collective-permute-start.42
  54.9 2.0 %collective-permute-start.44 = (bf16[48,2048]{1,0:T(8,128)(2,1)S(1)}, bf16[48,2048]{1,0:T(8,128)(2,1)S(1)}, u32[]{:S(2)}, u32[]{:S(2)}) collective-permute-start(bf16[48,2048]{1,0:T(8,128)(2,1)S(1)} %get-tuple-element.94), channel_id=1, source_target_pairs={{0,6},{1,7},{2,4},{3,5},{4,2},{5,3},{6,0},{7,1},{8,14},{9,15},{10,... | collective-permute-start | bytes 589832 | tf_op jit(solution)/shard_map/ppermute | solution.py:285
  56.8 1.4 shard_map.126
  58.2 2.2 %collective-permute-done.42.refs_1_ = bf16[48,2048]{1,0:T(8,128)(2,1)S(1)} collective-permute-done((bf16[48,2048]{1,0:T(8,128)(2,1)S(1)}, bf16[48,2048]{1,0:T(8,128)(2,1)S(1)}, u32[]{:S(2)}, u32[]{:S(2)}) %collective-permute-start.42) | collective-permute-done | bytes 196640 | tf_op jit(solution)/shard_map/ppermute | solution.py:285
  60.4 2.2 %collective-permute-done.43.refs_2_ = bf16[48,2048]{1,0:T(8,128)(2,1)S(1)} collective-permute-done((bf16[48,2048]{1,0:T(8,128)(2,1)S(1)}, bf16[48,2048]{1,0:T(8,128)(2,1)S(1)}, u32[]{:S(2)}, u32[]{:S(2)}) %collective-permute-start.43) | collective-permute-done | bytes 196640 | tf_op jit(solution)/shard_map/ppermute | solution.py:285
  62.6 3.2 %collective-permute-done.44.refs_3_ = bf16[48,2048]{1,0:T(8,128)(2,1)S(1)} collective-permute-done((bf16[48,2048]{1,0:T(8,128)(2,1)S(1)}, bf16[48,2048]{1,0:T(8,128)(2,1)S(1)}, u32[]{:S(2)}, u32[]{:S(2)}) %collective-permute-start.44) | collective-permute-done | bytes 196640 | tf_op jit(solution)/shard_map/ppermute | solution.py:285
  65.8 1.5 collective-permute-start.33
  68.4 3.0 %collective-permute-start.35 = (bf16[48,2048]{1,0:T(8,128)(2,1)S(1)}, bf16[48,2048]{1,0:T(8,128)(2,1)S(1)}, u32[]{:S(2)}, u32[]{:S(2)}) collective-permute-start(bf16[48,2048]{1,0:T(8,128)(2,1)S(1)} %get-tuple-element.84), channel_id=1, source_target_pairs={{0,6},{1,7},{2,4},{3,5},{4,2},{5,3},{6,0},{7,1},{8,14},{9,15},{10,... | collective-permute-start | bytes 589832 | tf_op jit(solution)/shard_map/ppermute | solution.py:285
  71.4 3.6 %shard_map.130 = (bf16[48,2048]{1,0:T(8,128)(2,1)S(1)}, bf16[48,2048]{1,0:T(8,128)(2,1)S(1)}, bf16[48,2048]{1,0:T(8,128)(2,1)S(1)}, bf16[48,2048]{1,0:T(8,128)(2,1)S(1)}) custom-call(s32[5]{0:T(128)S(1)} %stack.23.where_ref, bf16[48,2048]{1,0:T(8,128)(2,1)S(1)} %get-tuple-element.91.refs_0_, bf16[48,2048]{1,0:T(8,128)(2,1)S(1)} %collective-permute-done.42.refs_1_, ...), custom_call_target="tpu_custom_call" | custom-call | flops 2415919104 | bytes 13369364 | tf_op jit(solution)/shard_map/pallas_call | solution.py:154
  76.2 4.0 %collective-permute-done.35.refs_3_ = bf16[48,2048]{1,0:T(8,128)(2,1)S(1)} collective-permute-done((bf16[48,2048]{1,0:T(8,128)(2,1)S(1)}, bf16[48,2048]{1,0:T(8,128)(2,1)S(1)}, u32[]{:S(2)}, u32[]{:S(2)}) %collective-permute-start.35) | collective-permute-done | bytes 196640 | tf_op jit(solution)/shard_map/ppermute | solution.py:285
  80.2 3.6 %shard_map.127 = (bf16[48,2048]{1,0:T(8,128)(2,1)S(1)}, bf16[48,2048]{1,0:T(8,128)(2,1)S(1)}, bf16[48,2048]{1,0:T(8,128)(2,1)S(1)}, bf16[48,2048]{1,0:T(8,128)(2,1)S(1)}) custom-call(s32[5]{0:T(128)S(1)} %stack.23.where_ref, bf16[48,2048]{1,0:T(8,128)(2,1)S(1)} %get-tuple-element.81.refs_0_, bf16[48,2048]{1,0:T(8,128)(2,1)S(1)} %collective-permute-done.33.refs_1_, ...), custom_call_target="tpu_custom_call" | custom-call | flops 2415919104 | bytes 13369364 | tf_op jit(solution)/shard_map/pallas_call | solution.py:154
  84.2 1.7 collective-permute-start.47
  85.8 1.5 collective-permute-start.36
  87.7 1.7 collective-permute-start.38
  89.3 1.4 shard_map.123
  92.3 3.5 %collective-permute-done.47.refs_3_ = bf16[48,2048]{1,0:T(8,128)(2,1)S(1)} collective-permute-done((bf16[48,2048]{1,0:T(8,128)(2,1)S(1)}, bf16[48,2048]{1,0:T(8,128)(2,1)S(1)}, u32[]{:S(2)}, u32[]{:S(2)}) %collective-permute-start.47) | collective-permute-done | bytes 196640 | tf_op jit(solution)/shard_map/ppermute | solution.py:285
  96.1 1.7 collective-permute-done.36.refs_1_
  97.8 1.2 collective-permute-start.26
  99.1 1.9 %shard_map.131 = (bf16[128,2048]{1,0:T(8,128)(2,1)S(1)}, f32[128,2048]{1,0:T(8,128)S(1)}) custom-call(s32[5]{0:T(128)S(1)} %stack.23.where_ref, bf16[72,2048]{1,0:T(8,128)(2,1)S(1)} %collective-permute-done.16.refs_1_.own_ref, bf16[72,2048]{1,0:T(8,128)(2,1)S(1)} %collective-permute-done.40.refs_3_.other_ref, ...), custom_call_target="tpu_custom_call" | custom-call | flops 201326592 | bytes 1376276 | tf_op jit(solution)/shard_map/pallas_call | solution.py:154
  101.0 1.4 shard_map.120
  102.4 1.9 %collective-permute-done.38.refs_3_ = bf16[48,2048]{1,0:T(8,128)(2,1)S(1)} collective-permute-done((bf16[48,2048]{1,0:T(8,128)(2,1)S(1)}, bf16[48,2048]{1,0:T(8,128)(2,1)S(1)}, u32[]{:S(2)}, u32[]{:S(2)}) %collective-permute-start.38) | collective-permute-done | bytes 196640 | tf_op jit(solution)/shard_map/ppermute | solution.py:285
  104.6 1.9 %shard_map.128 = (bf16[128,2048]{1,0:T(8,128)(2,1)S(1)}, f32[128,2048]{1,0:T(8,128)S(1)}) custom-call(s32[5]{0:T(128)S(1)} %stack.23.where_ref, bf16[72,2048]{1,0:T(8,128)(2,1)S(1)} %collective-permute-done.17.refs_1_.own_ref, bf16[72,2048]{1,0:T(8,128)(2,1)S(1)} %collective-permute-done.31.refs_3_.other_ref, ...), custom_call_target="tpu_custom_call" | custom-call | flops 201326592 | bytes 1376276 | tf_op jit(solution)/shard_map/pallas_call | solution.py:154
  106.5 2.7 %collective-permute-start.11 = (bf16[48,2048]{1,0:T(8,128)(2,1)S(1)}, bf16[48,2048]{1,0:T(8,128)(2,1)S(1)}, u32[]{:S(2)}, u32[]{:S(2)}) collective-permute-start(bf16[48,2048]{1,0:T(8,128)(2,1)S(1)} %get-tuple-element.63), channel_id=1, source_target_pairs={{0,6},{1,7},{2,4},{3,5},{4,2},{5,3},{6,0},{7,1},{8,14},{9,15},{10,... | collective-permute-start | bytes 589832 | tf_op jit(solution)/shard_map/ppermute | solution.py:285
  109.7 3.0 %collective-permute-done.26.refs_3_ = bf16[48,2048]{1,0:T(8,128)(2,1)S(1)} collective-permute-done((bf16[48,2048]{1,0:T(8,128)(2,1)S(1)}, bf16[48,2048]{1,0:T(8,128)(2,1)S(1)}, u32[]{:S(2)}, u32[]{:S(2)}) %collective-permute-start.26) | collective-permute-done | bytes 196640 | tf_op jit(solution)/shard_map/ppermute | solution.py:285
  112.7 3.6 %shard_map.124 = (bf16[48,2048]{1,0:T(8,128)(2,1)S(1)}, bf16[48,2048]{1,0:T(8,128)(2,1)S(1)}, bf16[48,2048]{1,0:T(8,128)(2,1)S(1)}, bf16[48,2048]{1,0:T(8,128)(2,1)S(1)}) custom-call(s32[5]{0:T(128)S(1)} %stack.23.where_ref, bf16[48,2048]{1,0:T(8,128)(2,1)S(1)} %get-tuple-element.71.refs_0_, bf16[48,2048]{1,0:T(8,128)(2,1)S(1)} %collective-permute-done.24.refs_1_, ...), custom_call_target="tpu_custom_call" | custom-call | flops 2415919104 | bytes 13369364 | tf_op jit(solution)/shard_map/pallas_call | solution.py:154
  118.0 2.8 %collective-permute-done.11.refs_3_ = bf16[48,2048]{1,0:T(8,128)(2,1)S(1)} collective-permute-done((bf16[48,2048]{1,0:T(8,128)(2,1)S(1)}, bf16[48,2048]{1,0:T(8,128)(2,1)S(1)}, u32[]{:S(2)}, u32[]{:S(2)}) %collective-permute-start.11) | collective-permute-done | bytes 196640 | tf_op jit(solution)/shard_map/ppermute | solution.py:285
  121.1 2.7 %collective-permute-start.29 = (bf16[48,2048]{1,0:T(8,128)(2,1)S(1)}, bf16[48,2048]{1,0:T(8,128)(2,1)S(1)}, u32[]{:S(2)}, u32[]{:S(2)}) collective-permute-start(bf16[48,2048]{1,0:T(8,128)(2,1)S(1)} %get-tuple-element.78), channel_id=1, source_target_pairs={{0,6},{1,7},{2,4},{3,5},{4,2},{5,3},{6,0},{7,1},{8,14},{9,15},{10,... | collective-permute-start | bytes 589832 | tf_op jit(solution)/shard_map/ppermute | solution.py:285
  123.8 3.6 %shard_map.121 = (bf16[48,2048]{1,0:T(8,128)(2,1)S(1)}, bf16[48,2048]{1,0:T(8,128)(2,1)S(1)}, bf16[48,2048]{1,0:T(8,128)(2,1)S(1)}, bf16[48,2048]{1,0:T(8,128)(2,1)S(1)}) custom-call(s32[5]{0:T(128)S(1)} %stack.23.where_ref, bf16[48,2048]{1,0:T(8,128)(2,1)S(1)} %get-tuple-element.60.refs_0_, bf16[48,2048]{1,0:T(8,128)(2,1)S(1)} %collective-permute-done.9.refs_1_, ...), custom_call_target="tpu_custom_call" | custom-call | flops 2415919104 | bytes 13369364 | tf_op jit(solution)/shard_map/pallas_call | solution.py:154
  129.6 4.3 %collective-permute-done.29.refs_3_ = bf16[48,2048]{1,0:T(8,128)(2,1)S(1)} collective-permute-done((bf16[48,2048]{1,0:T(8,128)(2,1)S(1)}, bf16[48,2048]{1,0:T(8,128)(2,1)S(1)}, u32[]{:S(2)}, u32[]{:S(2)}) %collective-permute-start.29) | collective-permute-done | bytes 196640 | tf_op jit(solution)/shard_map/ppermute | solution.py:285
  133.8 1.9 %shard_map.125 = (bf16[128,2048]{1,0:T(8,128)(2,1)S(1)}, f32[128,2048]{1,0:T(8,128)S(1)}) custom-call(s32[5]{0:T(128)S(1)} %stack.23.where_ref, bf16[72,2048]{1,0:T(8,128)(2,1)S(1)} %collective-permute-done.18.refs_1_.own_ref, bf16[72,2048]{1,0:T(8,128)(2,1)S(1)} %collective-permute-done.19.refs_3_.other_ref, ...), custom_call_target="tpu_custom_call" | custom-call | flops 201326592 | bytes 1376276 | tf_op jit(solution)/shard_map/pallas_call | solution.py:154
  136.9 7.1 %collective-permute-done.14.refs_3_ = bf16[48,2048]{1,0:T(8,128)(2,1)S(1)} collective-permute-done((bf16[48,2048]{1,0:T(8,128)(2,1)S(1)}, bf16[48,2048]{1,0:T(8,128)(2,1)S(1)}, u32[]{:S(2)}, u32[]{:S(2)}) %collective-permute-start.14) | collective-permute-done | bytes 196640 | tf_op jit(solution)/shard_map/ppermute | solution.py:285
  144.1 1.9 %shard_map.122 = (bf16[128,2048]{1,0:T(8,128)(2,1)S(1)}, f32[128,2048]{1,0:T(8,128)S(1)}) custom-call(s32[5]{0:T(128)S(1)} %stack.23.where_ref, bf16[72,2048]{1,0:T(8,128)(2,1)S(1)} %get-tuple-element.58.refs_1_.own_ref, bf16[72,2048]{1,0:T(8,128)(2,1)S(1)} %collective-permute-done.7.refs_3_.other_ref, bf16[48,2048]{1,0:T(8,128)(2,1)S(1)} %get-tuple-element.64.refs_0_, ...), custom_call_target="tpu_custom_call" | custom-call | flops 201326592 | bytes 1376276 | tf_op jit(solution)/shard_map/pallas_call | solution.py:154
  148.3 9.3 %collective-permute-done.53.refs_0_ = bf16[64,2048]{1,0:T(8,128)(2,1)S(1)} collective-permute-done((bf16[64,2048]{1,0:T(8,128)(2,1)S(1)}, bf16[64,2048]{1,0:T(8,128)(2,1)S(1)}, u32[]{:S(2)}, u32[]{:S(2)}) %collective-permute-start.53) | collective-permute-done | bytes 262176 | tf_op jit(solution)/shard_map/ppermute | solution.py:285
  158.3 4.9 %collective-permute-done.50.refs_0_ = bf16[64,2048]{1,0:T(8,128)(2,1)S(1)} collective-permute-done((bf16[64,2048]{1,0:T(8,128)(2,1)S(1)}, bf16[64,2048]{1,0:T(8,128)(2,1)S(1)}, u32[]{:S(2)}, u32[]{:S(2)}) %collective-permute-start.50) | collective-permute-done | bytes 262176 | tf_op jit(solution)/shard_map/ppermute | solution.py:285
  163.9 5.3 %collective-permute-done.54.refs_1_ = bf16[64,2048]{1,0:T(8,128)(2,1)S(1)} collective-permute-done((bf16[64,2048]{1,0:T(8,128)(2,1)S(1)}, bf16[64,2048]{1,0:T(8,128)(2,1)S(1)}, u32[]{:S(2)}, u32[]{:S(2)}) %collective-permute-start.54) | collective-permute-done | bytes 262176 | tf_op jit(solution)/shard_map/ppermute | solution.py:285
  169.3 3.3 %collective-permute-done.51.refs_0_ = bf16[64,2048]{1,0:T(8,128)(2,1)S(1)} collective-permute-done((bf16[64,2048]{1,0:T(8,128)(2,1)S(1)}, bf16[64,2048]{1,0:T(8,128)(2,1)S(1)}, u32[]{:S(2)}, u32[]{:S(2)}) %collective-permute-start.51) | collective-permute-done | bytes 262176 | tf_op jit(solution)/shard_map/ppermute | solution.py:285
  172.6 1.6 shard_map.138
  (111 shorter events, 20.7 us)
Async XLA Ops:
  2.8 17.5 %collective-permute-start = (bf16[144,512]{1,0:T(8,128)(2,1)S(1)}, bf16[144,512]{1,0:T(8,128)(2,1)S(1)}, u32[]{:S(2)}, u32[]{:S(2)}) collective-permute-start(bf16[144,512]{1,0:T(8,128)(2,1)S(1)} %get-tuple-element.54), channel_id=1, source_target_pairs={{0,1},{1,0},{2,3},{3,2},{4,5},{5,4},{6,7},{7,6},{8,9},{9,8},{10,11... | collective-permute-start | bytes 442376 | tf_op jit(solution)/shard_map/ppermute | solution.py:285
  3.4 17.0 %collective-permute-start.1 = (bf16[144,512]{1,0:T(8,128)(2,1)S(1)}, bf16[144,512]{1,0:T(8,128)(2,1)S(1)}, u32[]{:S(2)}, u32[]{:S(2)}) collective-permute-start(bf16[144,512]{1,0:T(8,128)(2,1)S(1)} %get-tuple-element.55), channel_id=1, source_target_pairs={{0,2},{1,3},{2,0},{3,1},{4,6},{5,7},{6,4},{7,5},{8,10},{9,11},{10,... | collective-permute-start | bytes 442376 | tf_op jit(solution)/shard_map/ppermute | solution.py:285
  6.0 14.4 %collective-permute-start.2 = (bf16[144,512]{1,0:T(8,128)(2,1)S(1)}, bf16[144,512]{1,0:T(8,128)(2,1)S(1)}, u32[]{:S(2)}, u32[]{:S(2)}) collective-permute-start(bf16[144,512]{1,0:T(8,128)(2,1)S(1)} %get-tuple-element.56), channel_id=1, source_target_pairs={{0,3},{1,2},{2,1},{3,0},{4,7},{5,6},{6,5},{7,4},{8,11},{9,10},{10,... | collective-permute-start | bytes 442376 | tf_op jit(solution)/shard_map/ppermute | solution.py:285
  23.2 11.7 %collective-permute-start.16 = (bf16[72,2048]{1,0:T(8,128)(2,1)S(1)}, bf16[72,2048]{1,0:T(8,128)(2,1)S(1)}, u32[]{:S(2)}, u32[]{:S(2)}) collective-permute-start(bf16[72,2048]{1,0:T(8,128)(2,1)S(1)} %get-tuple-element.58.refs_1_.own_ref), channel_id=1, source_target_pairs={{0,8},{1,9},{2,10},{3,11},{4,12},{5,13},{6,14},{7,15},{8,16},{9,17... | collective-permute-start | bytes 884744 | tf_op jit(solution)/shard_map/ppermute | solution.py:285
  23.2 17.3 %collective-permute-start.20 = (bf16[64,2048]{1,0:T(8,128)(2,1)S(1)}, bf16[64,2048]{1,0:T(8,128)(2,1)S(1)}, u32[]{:S(2)}, u32[]{:S(2)}) collective-permute-start(bf16[64,2048]{1,0:T(8,128)(2,1)S(1)} %get-tuple-element.59.refs_0_), channel_id=1, source_target_pairs={{0,8},{1,9},{2,10},{3,11},{4,12},{5,13},{6,14},{7,15},{8,16},{9,17... | collective-permute-start | bytes 786440 | tf_op jit(solution)/shard_map/ppermute | solution.py:285
  34.9 11.9 %collective-permute-start.17 = (bf16[72,2048]{1,0:T(8,128)(2,1)S(1)}, bf16[72,2048]{1,0:T(8,128)(2,1)S(1)}, u32[]{:S(2)}, u32[]{:S(2)}) collective-permute-start(bf16[72,2048]{1,0:T(8,128)(2,1)S(1)} %collective-permute-done.16.refs_1_.own_ref), channel_id=1, source_target_pairs={{0,8},{1,9},{2,10},{3,11},{4,12},{5,13},{6,14},{7,15},{8,16},{9,17... | collective-permute-start | bytes 884744 | tf_op jit(solution)/shard_map/ppermute | solution.py:285
  40.5 11.1 %collective-permute-start.21 = (bf16[64,2048]{1,0:T(8,128)(2,1)S(1)}, bf16[64,2048]{1,0:T(8,128)(2,1)S(1)}, u32[]{:S(2)}, u32[]{:S(2)}) collective-permute-start(bf16[64,2048]{1,0:T(8,128)(2,1)S(1)} %collective-permute-done.20.refs_0_), channel_id=1, source_target_pairs={{0,8},{1,9},{2,10},{3,11},{4,12},{5,13},{6,14},{7,15},{8,16},{9,17... | collective-permute-start | bytes 786440 | tf_op jit(solution)/shard_map/ppermute | solution.py:285
  40.5 11.1 %collective-permute-start.41 = (bf16[64,2048]{1,0:T(8,128)(2,1)S(1)}, bf16[64,2048]{1,0:T(8,128)(2,1)S(1)}, u32[]{:S(2)}, u32[]{:S(2)}) collective-permute-start(bf16[64,2048]{1,0:T(8,128)(2,1)S(1)} %collective-permute-done.20.refs_0_), channel_id=1, source_target_pairs={{0,1},{1,0},{2,3},{3,2},{4,5},{5,4},{6,7},{7,6},{8,9},{9,8},{10,11... | collective-permute-start | bytes 786440 | tf_op jit(solution)/shard_map/ppermute | solution.py:285
  40.5 11.3 %collective-permute-start.40 = (bf16[72,2048]{1,0:T(8,128)(2,1)S(1)}, bf16[72,2048]{1,0:T(8,128)(2,1)S(1)}, u32[]{:S(2)}, u32[]{:S(2)}) collective-permute-start(bf16[72,2048]{1,0:T(8,128)(2,1)S(1)} %collective-permute-done.16.refs_1_.own_ref), channel_id=1, source_target_pairs={{0,1},{1,0},{2,3},{3,2},{4,5},{5,4},{6,7},{7,6},{8,9},{9,8},{10,11... | collective-permute-start | bytes 884744 | tf_op jit(solution)/shard_map/ppermute | solution.py:285
  46.8 8.0 %collective-permute-start.31 = (bf16[72,2048]{1,0:T(8,128)(2,1)S(1)}, bf16[72,2048]{1,0:T(8,128)(2,1)S(1)}, u32[]{:S(2)}, u32[]{:S(2)}) collective-permute-start(bf16[72,2048]{1,0:T(8,128)(2,1)S(1)} %collective-permute-done.17.refs_1_.own_ref), channel_id=1, source_target_pairs={{0,1},{1,0},{2,3},{3,2},{4,5},{5,4},{6,7},{7,6},{8,9},{9,8},{10,11... | collective-permute-start | bytes 884744 | tf_op jit(solution)/shard_map/ppermute | solution.py:285
  51.6 16.8 %collective-permute-start.18 = (bf16[72,2048]{1,0:T(8,128)(2,1)S(1)}, bf16[72,2048]{1,0:T(8,128)(2,1)S(1)}, u32[]{:S(2)}, u32[]{:S(2)}) collective-permute-start(bf16[72,2048]{1,0:T(8,128)(2,1)S(1)} %collective-permute-done.17.refs_1_.own_ref), channel_id=1, source_target_pairs={{0,8},{1,9},{2,10},{3,11},{4,12},{5,13},{6,14},{7,15},{8,16},{9,17... | collective-permute-start | bytes 884744 | tf_op jit(solution)/shard_map/ppermute | solution.py:285
  51.6 16.8 %collective-permute-start.22 = (bf16[64,2048]{1,0:T(8,128)(2,1)S(1)}, bf16[64,2048]{1,0:T(8,128)(2,1)S(1)}, u32[]{:S(2)}, u32[]{:S(2)}) collective-permute-start(bf16[64,2048]{1,0:T(8,128)(2,1)S(1)} %collective-permute-done.21.refs_0_), channel_id=1, source_target_pairs={{0,8},{1,9},{2,10},{3,11},{4,12},{5,13},{6,14},{7,15},{8,16},{9,17... | collective-permute-start | bytes 786440 | tf_op jit(solution)/shard_map/ppermute | solution.py:285
  54.9 7.8 %collective-permute-start.43 = (bf16[48,2048]{1,0:T(8,128)(2,1)S(1)}, bf16[48,2048]{1,0:T(8,128)(2,1)S(1)}, u32[]{:S(2)}, u32[]{:S(2)}) collective-permute-start(bf16[48,2048]{1,0:T(8,128)(2,1)S(1)} %get-tuple-element.93), channel_id=1, source_target_pairs={{0,4},{1,5},{2,6},{3,7},{4,0},{5,1},{6,2},{7,3},{8,12},{9,13},{10,... | collective-permute-start | bytes 589832 | tf_op jit(solution)/shard_map/ppermute | solution.py:285
  54.9 10.9 %collective-permute-start.44 = (bf16[48,2048]{1,0:T(8,128)(2,1)S(1)}, bf16[48,2048]{1,0:T(8,128)(2,1)S(1)}, u32[]{:S(2)}, u32[]{:S(2)}) collective-permute-start(bf16[48,2048]{1,0:T(8,128)(2,1)S(1)} %get-tuple-element.94), channel_id=1, source_target_pairs={{0,6},{1,7},{2,4},{3,5},{4,2},{5,3},{6,0},{7,1},{8,14},{9,15},{10,... | collective-permute-start | bytes 589832 | tf_op jit(solution)/shard_map/ppermute | solution.py:285
  60.4 23.7 %collective-permute-start.7 = (bf16[72,2048]{1,0:T(8,128)(2,1)S(1)}, bf16[72,2048]{1,0:T(8,128)(2,1)S(1)}, u32[]{:S(2)}, u32[]{:S(2)}) collective-permute-start(bf16[72,2048]{1,0:T(8,128)(2,1)S(1)} %get-tuple-element.58.refs_1_.own_ref), channel_id=1, source_target_pairs={{0,1},{1,0},{2,3},{3,2},{4,5},{5,4},{6,7},{7,6},{8,9},{9,8},{10,11... | collective-permute-start | bytes 884744 | tf_op jit(solution)/shard_map/ppermute | solution.py:285
  62.6 21.2 %collective-permute-start.8 = (bf16[64,2048]{1,0:T(8,128)(2,1)S(1)}, bf16[64,2048]{1,0:T(8,128)(2,1)S(1)}, u32[]{:S(2)}, u32[]{:S(2)}) collective-permute-start(bf16[64,2048]{1,0:T(8,128)(2,1)S(1)} %get-tuple-element.59.refs_0_), channel_id=1, source_target_pairs={{0,1},{1,0},{2,3},{3,2},{4,5},{5,4},{6,7},{7,6},{8,9},{9,8},{10,11... | collective-permute-start | bytes 786440 | tf_op jit(solution)/shard_map/ppermute | solution.py:285
  65.8 9.3 %collective-permute-start.33 = (bf16[48,2048]{1,0:T(8,128)(2,1)S(1)}, bf16[48,2048]{1,0:T(8,128)(2,1)S(1)}, u32[]{:S(2)}, u32[]{:S(2)}) collective-permute-start(bf16[48,2048]{1,0:T(8,128)(2,1)S(1)} %get-tuple-element.82), channel_id=1, source_target_pairs={{0,2},{1,3},{2,0},{3,1},{4,6},{5,7},{6,4},{7,5},{8,10},{9,11},{10,... | collective-permute-start | bytes 589832 | tf_op jit(solution)/shard_map/ppermute | solution.py:285
  68.4 7.8 %collective-permute-start.34 = (bf16[48,2048]{1,0:T(8,128)(2,1)S(1)}, bf16[48,2048]{1,0:T(8,128)(2,1)S(1)}, u32[]{:S(2)}, u32[]{:S(2)}) collective-permute-start(bf16[48,2048]{1,0:T(8,128)(2,1)S(1)} %get-tuple-element.83), channel_id=1, source_target_pairs={{0,4},{1,5},{2,6},{3,7},{4,0},{5,1},{6,2},{7,3},{8,12},{9,13},{10,... | collective-permute-start | bytes 589832 | tf_op jit(solution)/shard_map/ppermute | solution.py:285
  68.4 11.7 %collective-permute-start.35 = (bf16[48,2048]{1,0:T(8,128)(2,1)S(1)}, bf16[48,2048]{1,0:T(8,128)(2,1)S(1)}, u32[]{:S(2)}, u32[]{:S(2)}) collective-permute-start(bf16[48,2048]{1,0:T(8,128)(2,1)S(1)} %get-tuple-element.84), channel_id=1, source_target_pairs={{0,6},{1,7},{2,4},{3,5},{4,2},{5,3},{6,0},{7,1},{8,14},{9,15},{10,... | collective-permute-start | bytes 589832 | tf_op jit(solution)/shard_map/ppermute | solution.py:285
  75.1 10.8 %collective-permute-start.45 = (bf16[48,2048]{1,0:T(8,128)(2,1)S(1)}, bf16[48,2048]{1,0:T(8,128)(2,1)S(1)}, u32[]{:S(2)}, u32[]{:S(2)}) collective-permute-start(bf16[48,2048]{1,0:T(8,128)(2,1)S(1)} %get-tuple-element.96), channel_id=1, source_target_pairs={{0,2},{1,3},{2,0},{3,1},{4,6},{5,7},{6,4},{7,5},{8,10},{9,11},{10,... | collective-permute-start | bytes 589832 | tf_op jit(solution)/shard_map/ppermute | solution.py:285
  76.2 11.2 %collective-permute-start.23 = (bf16[64,2048]{1,0:T(8,128)(2,1)S(1)}, bf16[64,2048]{1,0:T(8,128)(2,1)S(1)}, u32[]{:S(2)}, u32[]{:S(2)}) collective-permute-start(bf16[64,2048]{1,0:T(8,128)(2,1)S(1)} %collective-permute-done.22.refs_0_), channel_id=1, source_target_pairs={{0,1},{1,0},{2,3},{3,2},{4,5},{5,4},{6,7},{7,6},{8,9},{9,8},{10,11... | collective-permute-start | bytes 786440 | tf_op jit(solution)/shard_map/ppermute | solution.py:285
  83.8 7.8 %collective-permute-start.46 = (bf16[48,2048]{1,0:T(8,128)(2,1)S(1)}, bf16[48,2048]{1,0:T(8,128)(2,1)S(1)}, u32[]{:S(2)}, u32[]{:S(2)}) collective-permute-start(bf16[48,2048]{1,0:T(8,128)(2,1)S(1)} %get-tuple-element.97), channel_id=1, source_target_pairs={{0,4},{1,5},{2,6},{3,7},{4,0},{5,1},{6,2},{7,3},{8,12},{9,13},{10,... | collective-permute-start | bytes 589832 | tf_op jit(solution)/shard_map/ppermute | solution.py:285
  84.2 11.7 %collective-permute-start.47 = (bf16[48,2048]{1,0:T(8,128)(2,1)S(1)}, bf16[48,2048]{1,0:T(8,128)(2,1)S(1)}, u32[]{:S(2)}, u32[]{:S(2)}) collective-permute-start(bf16[48,2048]{1,0:T(8,128)(2,1)S(1)} %get-tuple-element.98), channel_id=1, source_target_pairs={{0,6},{1,7},{2,4},{3,5},{4,2},{5,3},{6,0},{7,1},{8,14},{9,15},{10,... | collective-permute-start | bytes 589832 | tf_op jit(solution)/shard_map/ppermute | solution.py:285
  85.8 12.0 %collective-permute-start.36 = (bf16[48,2048]{1,0:T(8,128)(2,1)S(1)}, bf16[48,2048]{1,0:T(8,128)(2,1)S(1)}, u32[]{:S(2)}, u32[]{:S(2)}) collective-permute-start(bf16[48,2048]{1,0:T(8,128)(2,1)S(1)} %get-tuple-element.86), channel_id=1, source_target_pairs={{0,2},{1,3},{2,0},{3,1},{4,6},{5,7},{6,4},{7,5},{8,10},{9,11},{10,... | collective-permute-start | bytes 589832 | tf_op jit(solution)/shard_map/ppermute | solution.py:285
  87.4 13.6 %collective-permute-start.37 = (bf16[48,2048]{1,0:T(8,128)(2,1)S(1)}, bf16[48,2048]{1,0:T(8,128)(2,1)S(1)}, u32[]{:S(2)}, u32[]{:S(2)}) collective-permute-start(bf16[48,2048]{1,0:T(8,128)(2,1)S(1)} %get-tuple-element.87), channel_id=1, source_target_pairs={{0,4},{1,5},{2,6},{3,7},{4,0},{5,1},{6,2},{7,3},{8,12},{9,13},{10,... | collective-permute-start | bytes 589832 | tf_op jit(solution)/shard_map/ppermute | solution.py:285
  87.7 16.7 %collective-permute-start.38 = (bf16[48,2048]{1,0:T(8,128)(2,1)S(1)}, bf16[48,2048]{1,0:T(8,128)(2,1)S(1)}, u32[]{:S(2)}, u32[]{:S(2)}) collective-permute-start(bf16[48,2048]{1,0:T(8,128)(2,1)S(1)} %get-tuple-element.88), channel_id=1, source_target_pairs={{0,6},{1,7},{2,4},{3,5},{4,2},{5,3},{6,0},{7,1},{8,14},{9,15},{10,... | collective-permute-start | bytes 589832 | tf_op jit(solution)/shard_map/ppermute | solution.py:285
  91.6 14.8 %collective-permute-start.24 = (bf16[48,2048]{1,0:T(8,128)(2,1)S(1)}, bf16[48,2048]{1,0:T(8,128)(2,1)S(1)}, u32[]{:S(2)}, u32[]{:S(2)}) collective-permute-start(bf16[48,2048]{1,0:T(8,128)(2,1)S(1)} %get-tuple-element.72), channel_id=1, source_target_pairs={{0,2},{1,3},{2,0},{3,1},{4,6},{5,7},{6,4},{7,5},{8,10},{9,11},{10,... | collective-permute-start | bytes 589832 | tf_op jit(solution)/shard_map/ppermute | solution.py:285
  95.8 13.4 %collective-permute-start.25 = (bf16[48,2048]{1,0:T(8,128)(2,1)S(1)}, bf16[48,2048]{1,0:T(8,128)(2,1)S(1)}, u32[]{:S(2)}, u32[]{:S(2)}) collective-permute-start(bf16[48,2048]{1,0:T(8,128)(2,1)S(1)} %get-tuple-element.73), channel_id=1, source_target_pairs={{0,4},{1,5},{2,6},{3,7},{4,0},{5,1},{6,2},{7,3},{8,12},{9,13},{10,... | collective-permute-start | bytes 589832 | tf_op jit(solution)/shard_map/ppermute | solution.py:285
  97.8 14.9 %collective-permute-start.26 = (bf16[48,2048]{1,0:T(8,128)(2,1)S(1)}, bf16[48,2048]{1,0:T(8,128)(2,1)S(1)}, u32[]{:S(2)}, u32[]{:S(2)}) collective-permute-start(bf16[48,2048]{1,0:T(8,128)(2,1)S(1)} %get-tuple-element.74), channel_id=1, source_target_pairs={{0,6},{1,7},{2,4},{3,5},{4,2},{5,3},{6,0},{7,1},{8,14},{9,15},{10,... | collective-permute-start | bytes 589832 | tf_op jit(solution)/shard_map/ppermute | solution.py:285
  100.9 26.5 %collective-permute-start.48 = (bf16[128,2048]{1,0:T(8,128)(2,1)S(1)}, bf16[128,2048]{1,0:T(8,128)(2,1)S(1)}, u32[]{:S(2)}, u32[]{:S(2)}) collective-permute-start(bf16[128,2048]{1,0:T(8,128)(2,1)S(1)} %get-tuple-element.100), channel_id=1, source_target_pairs={{0,1},{1,0},{2,3},{3,2},{4,5},{5,4},{6,7},{7,6},{8,9},{9,8},{10,11... | collective-permute-start | bytes 1572872 | tf_op jit(solution)/shard_map/ppermute | solution.py:285
  104.3 12.7 %collective-permute-start.10 = (bf16[48,2048]{1,0:T(8,128)(2,1)S(1)}, bf16[48,2048]{1,0:T(8,128)(2,1)S(1)}, u32[]{:S(2)}, u32[]{:S(2)}) collective-permute-start(bf16[48,2048]{1,0:T(8,128)(2,1)S(1)} %get-tuple-element.62), channel_id=1, source_target_pairs={{0,4},{1,5},{2,6},{3,7},{4,0},{5,1},{6,2},{7,3},{8,12},{9,13},{10,... | collective-permute-start | bytes 589832 | tf_op jit(solution)/shard_map/ppermute | solution.py:285
  106.5 14.3 %collective-permute-start.11 = (bf16[48,2048]{1,0:T(8,128)(2,1)S(1)}, bf16[48,2048]{1,0:T(8,128)(2,1)S(1)}, u32[]{:S(2)}, u32[]{:S(2)}) collective-permute-start(bf16[48,2048]{1,0:T(8,128)(2,1)S(1)} %get-tuple-element.63), channel_id=1, source_target_pairs={{0,6},{1,7},{2,4},{3,5},{4,2},{5,3},{6,0},{7,1},{8,14},{9,15},{10,... | collective-permute-start | bytes 589832 | tf_op jit(solution)/shard_map/ppermute | solution.py:285
  109.2 11.9 %collective-permute-start.9 = (bf16[48,2048]{1,0:T(8,128)(2,1)S(1)}, bf16[48,2048]{1,0:T(8,128)(2,1)S(1)}, u32[]{:S(2)}, u32[]{:S(2)}) collective-permute-start(bf16[48,2048]{1,0:T(8,128)(2,1)S(1)} %get-tuple-element.61), channel_id=1, source_target_pairs={{0,2},{1,3},{2,0},{3,1},{4,6},{5,7},{6,4},{7,5},{8,10},{9,11},{10,... | collective-permute-start | bytes 589832 | tf_op jit(solution)/shard_map/ppermute | solution.py:285
  112.7 33.2 %collective-permute-start.39 = (bf16[128,2048]{1,0:T(8,128)(2,1)S(1)}, bf16[128,2048]{1,0:T(8,128)(2,1)S(1)}, u32[]{:S(2)}, u32[]{:S(2)}) collective-permute-start(bf16[128,2048]{1,0:T(8,128)(2,1)S(1)} %get-tuple-element.90), channel_id=1, source_target_pairs={{0,1},{1,0},{2,3},{3,2},{4,5},{5,4},{6,7},{7,6},{8,9},{9,8},{10,11... | collective-permute-start | bytes 1572872 | tf_op jit(solution)/shard_map/ppermute | solution.py:285
  117.0 11.0 %collective-permute-start.27 = (bf16[48,2048]{1,0:T(8,128)(2,1)S(1)}, bf16[48,2048]{1,0:T(8,128)(2,1)S(1)}, u32[]{:S(2)}, u32[]{:S(2)}) collective-permute-start(bf16[48,2048]{1,0:T(8,128)(2,1)S(1)} %get-tuple-element.76), channel_id=1, source_target_pairs={{0,2},{1,3},{2,0},{3,1},{4,6},{5,7},{6,4},{7,5},{8,10},{9,11},{10,... | collective-permute-start | bytes 589832 | tf_op jit(solution)/shard_map/ppermute | solution.py:285
  120.8 8.7 %collective-permute-start.28 = (bf16[48,2048]{1,0:T(8,128)(2,1)S(1)}, bf16[48,2048]{1,0:T(8,128)(2,1)S(1)}, u32[]{:S(2)}, u32[]{:S(2)}) collective-permute-start(bf16[48,2048]{1,0:T(8,128)(2,1)S(1)} %get-tuple-element.77), channel_id=1, source_target_pairs={{0,4},{1,5},{2,6},{3,7},{4,0},{5,1},{6,2},{7,3},{8,12},{9,13},{10,... | collective-permute-start | bytes 589832 | tf_op jit(solution)/shard_map/ppermute | solution.py:285
  121.1 12.7 %collective-permute-start.29 = (bf16[48,2048]{1,0:T(8,128)(2,1)S(1)}, bf16[48,2048]{1,0:T(8,128)(2,1)S(1)}, u32[]{:S(2)}, u32[]{:S(2)}) collective-permute-start(bf16[48,2048]{1,0:T(8,128)(2,1)S(1)} %get-tuple-element.78), channel_id=1, source_target_pairs={{0,6},{1,7},{2,4},{3,5},{4,2},{5,3},{6,0},{7,1},{8,14},{9,15},{10,... | collective-permute-start | bytes 589832 | tf_op jit(solution)/shard_map/ppermute | solution.py:285
  127.5 8.9 %collective-permute-start.12 = (bf16[48,2048]{1,0:T(8,128)(2,1)S(1)}, bf16[48,2048]{1,0:T(8,128)(2,1)S(1)}, u32[]{:S(2)}, u32[]{:S(2)}) collective-permute-start(bf16[48,2048]{1,0:T(8,128)(2,1)S(1)} %get-tuple-element.65), channel_id=1, source_target_pairs={{0,2},{1,3},{2,0},{3,1},{4,6},{5,7},{6,4},{7,5},{8,10},{9,11},{10,... | collective-permute-start | bytes 589832 | tf_op jit(solution)/shard_map/ppermute | solution.py:285
  128.0 8.4 %collective-permute-start.13 = (bf16[48,2048]{1,0:T(8,128)(2,1)S(1)}, bf16[48,2048]{1,0:T(8,128)(2,1)S(1)}, u32[]{:S(2)}, u32[]{:S(2)}) collective-permute-start(bf16[48,2048]{1,0:T(8,128)(2,1)S(1)} %get-tuple-element.66), channel_id=1, source_target_pairs={{0,4},{1,5},{2,6},{3,7},{4,0},{5,1},{6,2},{7,3},{8,12},{9,13},{10,... | collective-permute-start | bytes 589832 | tf_op jit(solution)/shard_map/ppermute | solution.py:285
  129.5 16.4 %collective-permute-start.52 = (bf16[64,2048]{1,0:T(8,128)(2,1)S(1)}, bf16[64,2048]{1,0:T(8,128)(2,1)S(1)}, u32[]{:S(2)}, u32[]{:S(2)}) collective-permute-start(bf16[64,2048]{1,0:T(8,128)(2,1)S(1)} %shard_map.135), channel_id=1, source_target_pairs={{0,8},{1,9},{2,10},{3,11},{4,12},{5,13},{6,14},{7,15},{8,16},{9,17... | collective-permute-start | bytes 786440 | tf_op jit(solution)/shard_map/ppermute | solution.py:285
  135.7 21.9 %collective-permute-start.30 = (bf16[128,2048]{1,0:T(8,128)(2,1)S(1)}, bf16[128,2048]{1,0:T(8,128)(2,1)S(1)}, u32[]{:S(2)}, u32[]{:S(2)}) collective-permute-start(bf16[128,2048]{1,0:T(8,128)(2,1)S(1)} %get-tuple-element.80), channel_id=1, source_target_pairs={{0,1},{1,0},{2,3},{3,2},{4,5},{5,4},{6,7},{7,6},{8,9},{9,8},{10,11... | collective-permute-start | bytes 1572872 | tf_op jit(solution)/shard_map/ppermute | solution.py:285
  136.4 10.9 %collective-permute-start.49 = (bf16[64,2048]{1,0:T(8,128)(2,1)S(1)}, bf16[64,2048]{1,0:T(8,128)(2,1)S(1)}, u32[]{:S(2)}, u32[]{:S(2)}) collective-permute-start(bf16[64,2048]{1,0:T(8,128)(2,1)S(1)} %shard_map.132), channel_id=1, source_target_pairs={{0,8},{1,9},{2,10},{3,11},{4,12},{5,13},{6,14},{7,15},{8,16},{9,17... | collective-permute-start | bytes 786440 | tf_op jit(solution)/shard_map/ppermute | solution.py:285
  136.4 7.7 %collective-permute-start.14 = (bf16[48,2048]{1,0:T(8,128)(2,1)S(1)}, bf16[48,2048]{1,0:T(8,128)(2,1)S(1)}, u32[]{:S(2)}, u32[]{:S(2)}) collective-permute-start(bf16[48,2048]{1,0:T(8,128)(2,1)S(1)} %get-tuple-element.67), channel_id=1, source_target_pairs={{0,6},{1,7},{2,4},{3,5},{4,2},{5,3},{6,0},{7,1},{8,14},{9,15},{10,... | collective-permute-start | bytes 589832 | tf_op jit(solution)/shard_map/ppermute | solution.py:285
  146.6 11.0 %collective-permute-start.53 = (bf16[64,2048]{1,0:T(8,128)(2,1)S(1)}, bf16[64,2048]{1,0:T(8,128)(2,1)S(1)}, u32[]{:S(2)}, u32[]{:S(2)}) collective-permute-start(bf16[64,2048]{1,0:T(8,128)(2,1)S(1)} %shard_map.136), channel_id=1, source_target_pairs={{0,8},{1,9},{2,10},{3,11},{4,12},{5,13},{6,14},{7,15},{8,16},{9,17... | collective-permute-start | bytes 786440 | tf_op jit(solution)/shard_map/ppermute | solution.py:285
  147.3 16.6 %collective-permute-start.15 = (bf16[128,2048]{1,0:T(8,128)(2,1)S(1)}, bf16[128,2048]{1,0:T(8,128)(2,1)S(1)}, u32[]{:S(2)}, u32[]{:S(2)}) collective-permute-start(bf16[128,2048]{1,0:T(8,128)(2,1)S(1)} %get-tuple-element.69), channel_id=1, source_target_pairs={{0,1},{1,0},{2,3},{3,2},{4,5},{5,4},{6,7},{7,6},{8,9},{9,8},{10,11... | collective-permute-start | bytes 1572872 | tf_op jit(solution)/shard_map/ppermute | solution.py:285
  147.9 15.3 %collective-permute-start.50 = (bf16[64,2048]{1,0:T(8,128)(2,1)S(1)}, bf16[64,2048]{1,0:T(8,128)(2,1)S(1)}, u32[]{:S(2)}, u32[]{:S(2)}) collective-permute-start(bf16[64,2048]{1,0:T(8,128)(2,1)S(1)} %shard_map.133), channel_id=1, source_target_pairs={{0,8},{1,9},{2,10},{3,11},{4,12},{5,13},{6,14},{7,15},{8,16},{9,17... | collective-permute-start | bytes 786440 | tf_op jit(solution)/shard_map/ppermute | solution.py:285
  158.2 11.0 %collective-permute-start.54 = (bf16[64,2048]{1,0:T(8,128)(2,1)S(1)}, bf16[64,2048]{1,0:T(8,128)(2,1)S(1)}, u32[]{:S(2)}, u32[]{:S(2)}) collective-permute-start(bf16[64,2048]{1,0:T(8,128)(2,1)S(1)} %shard_map.137), channel_id=1, source_target_pairs={{0,8},{1,9},{2,10},{3,11},{4,12},{5,13},{6,14},{7,15},{8,16},{9,17... | collective-permute-start | bytes 786440 | tf_op jit(solution)/shard_map/ppermute | solution.py:285
  163.8 8.8 %collective-permute-start.51 = (bf16[64,2048]{1,0:T(8,128)(2,1)S(1)}, bf16[64,2048]{1,0:T(8,128)(2,1)S(1)}, u32[]{:S(2)}, u32[]{:S(2)}) collective-permute-start(bf16[64,2048]{1,0:T(8,128)(2,1)S(1)} %shard_map.134), channel_id=1, source_target_pairs={{0,8},{1,9},{2,10},{3,11},{4,12},{5,13},{6,14},{7,15},{8,16},{9,17... | collective-permute-start | bytes 786440 | tf_op jit(solution)/shard_map/ppermute | solution.py:285
  (20 other events, 347.2 us)

commit v5 on v4

--- a/solution.py
+++ b/solution.py
@@ -79,31 +79,38 @@
     return mixed
 
 
-def named_experts(where_ref, routes_t, chips):
-    offset = lax.broadcasted_iota(jnp.int32, (chips, routes_t.shape[1]), 0)
+def slot_tables(where_ref, tables, chips, capacity):
+    tokens = tables[0][0].shape[1]
+    offset = lax.broadcasted_iota(jnp.int32, (chips, tokens), 0)
     here = (offset ^ where_ref[2]) * CORES + where_ref[3] + where_ref[0] * (chips * CORES)
-    return [routes_t[j : j + 1, :] == here for j in range(routes_t.shape[0])]
-
-
-def slot_table(matches, capacity):
-    count, tokens = matches[0].shape
-    named = matches[0]
-    for match in matches[1:]:
-        named = named | match
+    named, highs, lows = [], [], []
+    for routes_t, high, low in tables:
+        matches = [routes_t[j : j + 1, :] == here for j in range(routes_t.shape[0])]
+        named.append(sum(jnp.where(m, 1.0, 0.0) for m in matches))
+        highs.append(sum(jnp.where(m, high[j : j + 1, :], 0.0) for j, m in enumerate(matches)))
+        lows.append(sum(jnp.where(m, low[j : j + 1, :], 0.0) for j, m in enumerate(matches)))
+    named, high, low = (jnp.concatenate(parts, 0) for parts in (named, highs, lows))
+    lines = named.shape[0]
     earlier = (
         lax.broadcasted_iota(jnp.int32, (tokens, tokens), 0)
         < lax.broadcasted_iota(jnp.int32, (tokens, tokens), 1)
     )
-    ones = jnp.where(named, 1.0, 0.0)
-    rank = dot32(ones.astype(jnp.bfloat16), jnp.where(earlier, 1.0, 0.0).astype(jnp.bfloat16))
-    held = jnp.where(named, rank, -1.0).astype(jnp.bfloat16)
-    slots = count * capacity
-    low = lax.broadcasted_iota(jnp.int32, (slots, count), 1) * capacity
-    slot = lax.broadcasted_iota(jnp.int32, (slots, count), 0)
-    inside = (slot >= low) & (slot < low + capacity)
+    rank = dot32(named.astype(jnp.bfloat16), jnp.where(earlier, 1.0, 0.0).astype(jnp.bfloat16))
+    held = jnp.where(named > 0.0, rank, -1.0)
+    slots = lines * capacity
+    low_slot = lax.broadcasted_iota(jnp.int32, (slots, lines), 1) * capacity
+    slot = lax.broadcasted_iota(jnp.int32, (slots, lines), 0)
+    inside = (slot >= low_slot) & (slot < low_slot + capacity)
     spread = jnp.where(inside, 1.0, 0.0).astype(jnp.bfloat16)
-    place = jnp.sum(jnp.where(inside, slot - low, 0), 1, keepdims=True).astype(jnp.float32)
-    return dot32(spread, held) == place, spread
+    place = jnp.sum(jnp.where(inside, slot - low_slot, 0), 1, keepdims=True).astype(jnp.float32)
+    wide = jnp.concatenate([held, high, low], 1).astype(jnp.bfloat16)
+    wide = dot32(spread, wide)
+    taken = wide[:, 0:tokens] == place
+    factors = [
+        jnp.where(taken, wide[:, k * tokens : (k + 1) * tokens], 0.0).astype(jnp.bfloat16)
+        for k in (1, 2)
+    ]
+    return jnp.where(taken, 1.0, 0.0).astype(jnp.bfloat16), factors
 
 
 def mixer_kernel(
@@ -165,44 +172,38 @@
 
 
 def pick_kernel(where_ref, *refs, tokens, top, capacity):
-    chunk_refs, send_refs = refs[: 2 * CORES], refs[2 * CORES :]
+    chunk_refs, send_refs, factor_ref = refs[: 2 * CORES], refs[2 * CORES : -1], refs[-1]
     chips = len(send_refs)
+    tables = [read_table(chunk_refs[2 * k + 1], tokens, top) for k in range(CORES)]
+    taken, factors = slot_tables(where_ref, tables, chips, capacity)
+    size = chips * capacity
     for k in range(CORES):
         upper_ref, lower_ref = chunk_refs[2 * k : 2 * k + 2]
-        routes_t, _, _ = read_table(lower_ref, tokens, top)
-        taken, _ = slot_table(named_experts(where_ref, routes_t, chips), capacity)
         rest = tokens - upper_ref.shape[0]
         rows = jnp.concatenate([upper_ref[...], lower_ref[0:rest, :]], 0)
-        picked = dot32(jnp.where(taken, 1.0, 0.0).astype(jnp.bfloat16), rows)
-        picked = picked.astype(jnp.bfloat16)
+        part = slice(k * size, (k + 1) * size)
+        picked = dot32(taken[part], rows).astype(jnp.bfloat16)
         for d in range(chips):
             rows = picked[d * capacity : (d + 1) * capacity]
             send_refs[d][k * capacity : (k + 1) * capacity, :] = rows
-
-
-def weighted_sum(where_ref, lower_ref, back_refs, k, tokens, top, capacity):
-    routes_t, *weights = read_table(lower_ref, tokens, top)
-    matches = named_experts(where_ref, routes_t, len(back_refs))
-    taken, spread = slot_table(matches, capacity)
-    back = jnp.concatenate([ref[k * capacity : (k + 1) * capacity, :] for ref in back_refs], 0)
-    total = jnp.zeros((tokens, back.shape[1]), jnp.float32)
-    for piece in weights:
-        weight = jnp.zeros(matches[0].shape, jnp.float32)
-        for j, match in enumerate(matches):
-            weight = weight + jnp.where(match, piece[j : j + 1, :], 0.0)
-        factor = jnp.where(taken, dot32(spread, weight.astype(jnp.bfloat16)), 0.0)
-        total = total + lax.dot_general(
-            factor.astype(jnp.bfloat16), back, (((0,), (0,)), ((), ())),
-            preferred_element_type=jnp.float32,
-        )
-    return total
-
-
-def share_kernel(where_ref, own_ref, other_ref, *refs, tokens, top, capacity):
+        for f in range(2):
+            start = (2 * k + f) * size
+            factor_ref[start : start + size, :] = factors[f][part]
+
+
+def weighted_sum(factor_ref, back_refs, k, capacity):
+    size = 2 * len(back_refs) * capacity
+    back = [ref[k * capacity : (k + 1) * capacity, :] for ref in back_refs]
+    return lax.dot_general(
+        factor_ref[k * size : (k + 1) * size, :], jnp.concatenate(back + back, 0),
+        (((0,), (0,)), ((), ())), preferred_element_type=jnp.float32,
+    )
+
+
+def share_kernel(where_ref, factor_ref, *refs, capacity):
     back_refs, (given_ref, kept_ref) = refs[:-2], refs[-2:]
-    total = weighted_sum(where_ref, other_ref, back_refs, 1, tokens, top, capacity)
-    given_ref[...] = total.astype(jnp.bfloat16)
-    kept_ref[...] = weighted_sum(where_ref, own_ref, back_refs, 0, tokens, top, capacity)
+    given_ref[...] = weighted_sum(factor_ref, back_refs, 1, capacity).astype(jnp.bfloat16)
+    kept_ref[...] = weighted_sum(factor_ref, back_refs, 0, capacity)
 
 
 def sum_kernel(where_ref, kept_ref, got_ref, *refs, start):
@@ -284,8 +285,11 @@
     def move(value, to):
         return lax.ppermute(value, every, [(i, to(i)) for i in range(devices)])
 
+    ring = list(range(1, planes, 2)) + list(range((planes - 1) // 2 * 2, -1, -2))
+    after = {ring[k - 1]: plane for k, plane in enumerate(ring)}
+
     def hop(value):
-        return move(value, lambda i: (i + count) % devices)
+        return move(value, lambda i: after[i // count] * count + i % count)
 
     def swap(value):
         return move(value, lambda i: i ^ 1)
@@ -307,15 +311,12 @@
         [pltpu.VMEM((row_count + rim, channels), jnp.bfloat16)],
     )
 
-    def beside(i, d, ahead):
-        sp, tp = i // tp_count, i % tp_count
-        return (sp + ahead) % sp_count * tp_count + (tp ^ d)
-
-    blocks, rims = [cuts[0]], []
+    rims = [move(tail, lambda i: (i + tp_count) % devices)]
+    blocks = [cuts[0]]
     for d in range(1, tp_count):
-        blocks.append(move(cuts[d], lambda i: beside(i, d, 0)))
-    for d in range(tp_count):
-        rims.append(move(tail, lambda i: beside(i, d, 1)))
+        blocks.append(move(cuts[d], lambda i: i ^ d))
+    for d in range(1, tp_count):
+        rims.append(move(rims[0], lambda i: i ^ d))
 
     shape = jax.ShapeDtypeStruct((tokens, width), jnp.bfloat16)
     block = jax.ShapeDtypeStruct((CORES * capacity, width), jnp.bfloat16)
@@ -335,12 +336,14 @@
     small = 2 * tokens * count * capacity * width
     matrices = [in_vmem(expert_gate[0]), in_vmem(expert_up[0]), in_vmem(expert_down[0])]
 
+    factor = jax.ShapeDtypeStruct((2 * count * capacity, tokens), jnp.bfloat16)
+
     def dispatch(pair):
-        rows = call(
-            functools.partial(pick_kernel, **sizes), [block] * chips, [where, *pair],
-            small,
+        *rows, factors = call(
+            functools.partial(pick_kernel, **sizes), [block] * chips + [factor],
+            [where, *pair], small,
         )
-        return in_plane(rows)
+        return in_plane(rows), factors
 
     def experts(rows):
         results = call(
@@ -349,11 +352,11 @@
         )
         return in_plane(results)
 
-    def share(pair, back):
+    def share(factors, back):
         given, kept = call(
-            functools.partial(share_kernel, **sizes),
+            functools.partial(share_kernel, capacity=capacity),
             [shape, jax.ShapeDtypeStruct(shape.shape, jnp.float32)],
-            [where, pair[1], pair[3], *back], 2 * small,
+            [where, factors, *back], 2 * small,
         )
         return kept, swap(given)
 
@@ -364,17 +367,17 @@
     for s in range(planes):
         pairs.append(chunks[s] + [swap(chunks[s][h]) for h in range(2)])
     arrived = [dispatch(pairs[s]) for s in range(planes)]
-    returned = [experts(arrived[s]) for s in range(planes)]
+    returned = [experts(arrived[s][0]) for s in range(planes)]
     carried = [[], []]
     for s in range(1, planes):
-        shares = share(pairs[s], returned[s])
+        shares = share(arrived[s][1], returned[s])
         for h in range(2):
             (total,) = call(
                 functools.partial(sum_kernel, start=h * half), [piece],
                 [where, *shares, *carried[h]], tokens * width,
             )
             carried[h] = [hop(total)]
-    shares = share(pairs[0], returned[0])
+    shares = share(arrived[0][1], returned[0])
     (out,) = call(
         final_kernel, [shape], [where, *shares, resid, *carried[0], *carried[1]],
         tokens * width,

time: 174 us -> 167 us (0.960)
  waiting for transfers between devices: 102 us -> 87.8 us
  starting transfers between devices: 33.9 us -> 44.8 us
  Pallas kernels: 36.1 us -> 31.8 us
    ppermute x55, waiting for transfers between devices: 102 us -> 87.8 us  [move(): return lax.ppermute(value, every, [(i, to(i)) for i in range(devices)])]
    ppermute x55, starting transfers between devices: 33.9 us -> 44.8 us  [move(): return lax.ppermute(value, every, [(i, to(i)) for i in range(devices)])]
    pallas_call x21, Pallas kernels: 36.1 us -> 31.8 us  [call(): pl.pallas_call(kernel, out_shape=tuple(shapes), in_specs=specs, out_specs...]
  transfers between devices with their start and end apart: 55 -> 55, of which waited for: 28 -> 28; matrix products, arithmetic and copies ran while one was open for 0% -> 0% of each run, Pallas kernels for 18% -> 16%
where the time goes in v5:
time: 167 us
  waiting for transfers between devices  87.8 us (53%)
  starting transfers between devices  44.8 us (27%)
  Pallas kernels  31.8 us (19%)
  local copies, waits for them, and re-layouts  2.19 us (1%)
    ppermute x55, waiting for transfers between devices, move(): return lax.ppermute(value, every, [(i, to(i)) for i in range(devices)])  87.8 us
    ppermute x55, starting transfers between devices, move(): return lax.ppermute(value, every, [(i, to(i)) for i in range(devices)])  44.8 us
    pallas_call x21, Pallas kernels, call(): pl.pallas_call(kernel, out_shape=tuple(shapes), in_specs=specs, out_specs...  31.8 us
  transfers between devices with their start and end apart: 55, of which 28 were waited for; matrix products, arithmetic and copies ran while one was open for 0% of the time, Pallas kernels for 16%

profile of v5, /device:TPU:0, one launch (start us, length us, event | category | flops | bytes accessed | tf_op | source)
XLA Modules:
  0.0 167.1 jit_solution(16609824578800668512)
XLA Ops:
  0.9 1.2 copy-done.10
  3.4 2.6 %collective-permute-start.1 = (bf16[144,512]{1,0:T(8,128)(2,1)S(1)}, bf16[144,512]{1,0:T(8,128)(2,1)S(1)}, u32[]{:S(2)}, u32[]{:S(2)}) collective-permute-start(bf16[144,512]{1,0:T(8,128)(2,1)S(1)} %get-tuple-element.59), channel_id=1, source_target_pairs={{0,2},{1,3},{2,0},{3,1},{4,6},{5,7},{6,4},{7,5},{8,10},{9,11},{10,... | collective-permute-start | bytes 442376 | tf_op jit(solution)/shard_map/ppermute | solution.py:286
  6.0 1.7 %collective-permute-start.3 = (bf16[16,512]{1,0:T(8,128)(2,1)S(1)}, bf16[16,512]{1,0:T(8,128)(2,1)S(1)}, u32[]{:S(2)}, u32[]{:S(2)}) collective-permute-start(bf16[16,512]{1,0:T(8,128)(2,1)S(1)} %get-tuple-element.61), channel_id=1, source_target_pairs={{0,4},{1,5},{2,6},{3,7},{4,8},{5,9},{6,10},{7,11},{8,12},{9,13},{1... | collective-permute-start | bytes 49160 | tf_op jit(solution)/shard_map/ppermute | solution.py:286
  7.7 4.8 %collective-permute-done.3.refs_4_ = bf16[16,512]{1,0:T(8,128)(2,1)S(1)} collective-permute-done((bf16[16,512]{1,0:T(8,128)(2,1)S(1)}, bf16[16,512]{1,0:T(8,128)(2,1)S(1)}, u32[]{:S(2)}, u32[]{:S(2)}) %collective-permute-start.3) | collective-permute-done | bytes 16416 | tf_op jit(solution)/shard_map/ppermute | solution.py:286
  12.5 1.7 %collective-permute-start.5 = (bf16[16,512]{1,0:T(8,128)(2,1)S(1)}, bf16[16,512]{1,0:T(8,128)(2,1)S(1)}, u32[]{:S(2)}, u32[]{:S(2)}) collective-permute-start(bf16[16,512]{1,0:T(8,128)(2,1)S(1)} %collective-permute-done.3.refs_4_), channel_id=1, source_target_pairs={{0,2},{1,3},{2,0},{3,1},{4,6},{5,7},{6,4},{7,5},{8,10},{9,11},{10,... | collective-permute-start | bytes 49160 | tf_op jit(solution)/shard_map/ppermute | solution.py:286
  16.2 1.1 collective-permute-done.6.refs_7_
  17.5 2.7 %shard_map.119 = (bf16[128,2048]{1,0:T(8,128)(2,1)S(1)}, bf16[64,2048]{1,0:T(8,128)(2,1)S(1)}, bf16[72,2048]{1,0:T(8,128)(2,1)S(1)}) custom-call(s32[5]{0:T(128)S(1)} %stack.23.where_ref, s32[4,128]{1,0:T(4,128)S(1)} %bitcast.29, f32[4,128]{1,0:T(4,128)S(1)} %bitcast.30, s32[4,128]{1,0:T(4,128)S(1)} %bitcast.32, f32[1,2048]{1,0:T(1,128)S(1)} %bitcast.27, ...), custom_call_target="tpu_custom_call" | custom-call | flops 1342177280 | bytes 11687956 | tf_op jit(solution)/shard_map/pallas_call | solution.py:161
  20.2 2.4 %collective-permute-start.16 = (bf16[64,2048]{1,0:T(8,128)(2,1)S(1)}, bf16[64,2048]{1,0:T(8,128)(2,1)S(1)}, u32[]{:S(2)}, u32[]{:S(2)}) collective-permute-start(bf16[64,2048]{1,0:T(8,128)(2,1)S(1)} %get-tuple-element.62.refs_0_), channel_id=1, source_target_pairs={{0,8},{1,9},{2,10},{3,11},{4,12},{5,13},{6,14},{7,15},{8,24},{9,25... | collective-permute-start | bytes 786440 | tf_op jit(solution)/shard_map/ppermute | solution.py:286
  22.6 8.4 %collective-permute-done.19.refs_1_ = bf16[72,2048]{1,0:T(8,128)(2,1)S(1)} collective-permute-done((bf16[72,2048]{1,0:T(8,128)(2,1)S(1)}, bf16[72,2048]{1,0:T(8,128)(2,1)S(1)}, u32[]{:S(2)}, u32[]{:S(2)}) %collective-permute-start.19) | collective-permute-done | bytes 294944 | tf_op jit(solution)/shard_map/ppermute | solution.py:286
  31.0 5.6 %collective-permute-done.16.refs_0_ = bf16[64,2048]{1,0:T(8,128)(2,1)S(1)} collective-permute-done((bf16[64,2048]{1,0:T(8,128)(2,1)S(1)}, bf16[64,2048]{1,0:T(8,128)(2,1)S(1)}, u32[]{:S(2)}, u32[]{:S(2)}) %collective-permute-start.16) | collective-permute-done | bytes 262176 | tf_op jit(solution)/shard_map/ppermute | solution.py:286
  37.1 5.8 %collective-permute-done.20.refs_1_ = bf16[72,2048]{1,0:T(8,128)(2,1)S(1)} collective-permute-done((bf16[72,2048]{1,0:T(8,128)(2,1)S(1)}, bf16[72,2048]{1,0:T(8,128)(2,1)S(1)}, u32[]{:S(2)}, u32[]{:S(2)}) %collective-permute-start.20) | collective-permute-done | bytes 294944 | tf_op jit(solution)/shard_map/ppermute | solution.py:286
  42.9 4.9 %collective-permute-done.17.refs_0_ = bf16[64,2048]{1,0:T(8,128)(2,1)S(1)} collective-permute-done((bf16[64,2048]{1,0:T(8,128)(2,1)S(1)}, bf16[64,2048]{1,0:T(8,128)(2,1)S(1)}, u32[]{:S(2)}, u32[]{:S(2)}) %collective-permute-start.17) | collective-permute-done | bytes 262176 | tf_op jit(solution)/shard_map/ppermute | solution.py:286
  47.8 2.4 %collective-permute-start.18 = (bf16[64,2048]{1,0:T(8,128)(2,1)S(1)}, bf16[64,2048]{1,0:T(8,128)(2,1)S(1)}, u32[]{:S(2)}, u32[]{:S(2)}) collective-permute-start(bf16[64,2048]{1,0:T(8,128)(2,1)S(1)} %collective-permute-done.17.refs_0_), channel_id=1, source_target_pairs={{0,8},{1,9},{2,10},{3,11},{4,12},{5,13},{6,14},{7,15},{8,24},{9,25... | collective-permute-start | bytes 786440 | tf_op jit(solution)/shard_map/ppermute | solution.py:286
  50.2 1.1 shard_map.129
  51.3 1.2 collective-permute-start.42
  53.1 1.8 %collective-permute-start.44 = (bf16[48,2048]{1,0:T(8,128)(2,1)S(1)}, bf16[48,2048]{1,0:T(8,128)(2,1)S(1)}, u32[]{:S(2)}, u32[]{:S(2)}) collective-permute-start(bf16[48,2048]{1,0:T(8,128)(2,1)S(1)} %get-tuple-element.102), channel_id=1, source_target_pairs={{0,6},{1,7},{2,4},{3,5},{4,2},{5,3},{6,0},{7,1},{8,14},{9,15},{10,... | collective-permute-start | bytes 589832 | tf_op jit(solution)/shard_map/ppermute | solution.py:286
  56.0 2.2 %collective-permute-done.42.refs_1_ = bf16[48,2048]{1,0:T(8,128)(2,1)S(1)} collective-permute-done((bf16[48,2048]{1,0:T(8,128)(2,1)S(1)}, bf16[48,2048]{1,0:T(8,128)(2,1)S(1)}, u32[]{:S(2)}, u32[]{:S(2)}) %collective-permute-start.42) | collective-permute-done | bytes 196640 | tf_op jit(solution)/shard_map/ppermute | solution.py:286
  58.3 2.0 %collective-permute-done.43.refs_2_ = bf16[48,2048]{1,0:T(8,128)(2,1)S(1)} collective-permute-done((bf16[48,2048]{1,0:T(8,128)(2,1)S(1)}, bf16[48,2048]{1,0:T(8,128)(2,1)S(1)}, u32[]{:S(2)}, u32[]{:S(2)}) %collective-permute-start.43) | collective-permute-done | bytes 196640 | tf_op jit(solution)/shard_map/ppermute | solution.py:286
  60.3 3.3 %collective-permute-done.44.refs_3_ = bf16[48,2048]{1,0:T(8,128)(2,1)S(1)} collective-permute-done((bf16[48,2048]{1,0:T(8,128)(2,1)S(1)}, bf16[48,2048]{1,0:T(8,128)(2,1)S(1)}, u32[]{:S(2)}, u32[]{:S(2)}) %collective-permute-start.44) | collective-permute-done | bytes 196640 | tf_op jit(solution)/shard_map/ppermute | solution.py:286
  65.3 1.8 %collective-permute-start.35 = (bf16[48,2048]{1,0:T(8,128)(2,1)S(1)}, bf16[48,2048]{1,0:T(8,128)(2,1)S(1)}, u32[]{:S(2)}, u32[]{:S(2)}) collective-permute-start(bf16[48,2048]{1,0:T(8,128)(2,1)S(1)} %get-tuple-element.91), channel_id=1, source_target_pairs={{0,6},{1,7},{2,4},{3,5},{4,2},{5,3},{6,0},{7,1},{8,14},{9,15},{10,... | collective-permute-start | bytes 589832 | tf_op jit(solution)/shard_map/ppermute | solution.py:286
  67.0 3.6 %shard_map.130 = (bf16[48,2048]{1,0:T(8,128)(2,1)S(1)}, bf16[48,2048]{1,0:T(8,128)(2,1)S(1)}, bf16[48,2048]{1,0:T(8,128)(2,1)S(1)}, bf16[48,2048]{1,0:T(8,128)(2,1)S(1)}) custom-call(s32[5]{0:T(128)S(1)} %stack.23.where_ref, bf16[48,2048]{1,0:T(8,128)(2,1)S(1)} %get-tuple-element.99.refs_0_, bf16[48,2048]{1,0:T(8,128)(2,1)S(1)} %collective-permute-done.42.refs_1_, ...), custom_call_target="tpu_custom_call" | custom-call | flops 2415919104 | bytes 13369364 | tf_op jit(solution)/shard_map/pallas_call | solution.py:161
  70.7 1.2 collective-permute-start.45
  72.3 2.7 %collective-permute-done.35.refs_3_ = bf16[48,2048]{1,0:T(8,128)(2,1)S(1)} collective-permute-done((bf16[48,2048]{1,0:T(8,128)(2,1)S(1)}, bf16[48,2048]{1,0:T(8,128)(2,1)S(1)}, u32[]{:S(2)}, u32[]{:S(2)}) %collective-permute-start.35) | collective-permute-done | bytes 196640 | tf_op jit(solution)/shard_map/ppermute | solution.py:286
  75.1 3.6 %shard_map.127 = (bf16[48,2048]{1,0:T(8,128)(2,1)S(1)}, bf16[48,2048]{1,0:T(8,128)(2,1)S(1)}, bf16[48,2048]{1,0:T(8,128)(2,1)S(1)}, bf16[48,2048]{1,0:T(8,128)(2,1)S(1)}) custom-call(s32[5]{0:T(128)S(1)} %stack.23.where_ref, bf16[48,2048]{1,0:T(8,128)(2,1)S(1)} %get-tuple-element.88.refs_0_, bf16[48,2048]{1,0:T(8,128)(2,1)S(1)} %collective-permute-done.33.refs_1_, ...), custom_call_target="tpu_custom_call" | custom-call | flops 2415919104 | bytes 13369364 | tf_op jit(solution)/shard_map/pallas_call | solution.py:161
  79.0 2.1 %collective-permute-start.47 = (bf16[48,2048]{1,0:T(8,128)(2,1)S(1)}, bf16[48,2048]{1,0:T(8,128)(2,1)S(1)}, u32[]{:S(2)}, u32[]{:S(2)}) collective-permute-start(bf16[48,2048]{1,0:T(8,128)(2,1)S(1)} %get-tuple-element.106), channel_id=1, source_target_pairs={{0,6},{1,7},{2,4},{3,5},{4,2},{5,3},{6,0},{7,1},{8,14},{9,15},{10,... | collective-permute-start | bytes 589832 | tf_op jit(solution)/shard_map/ppermute | solution.py:286
  81.1 1.2 collective-permute-start.36
  82.5 2.1 %collective-permute-start.38 = (bf16[48,2048]{1,0:T(8,128)(2,1)S(1)}, bf16[48,2048]{1,0:T(8,128)(2,1)S(1)}, u32[]{:S(2)}, u32[]{:S(2)}) collective-permute-start(bf16[48,2048]{1,0:T(8,128)(2,1)S(1)} %get-tuple-element.95), channel_id=1, source_target_pairs={{0,6},{1,7},{2,4},{3,5},{4,2},{5,3},{6,0},{7,1},{8,14},{9,15},{10,... | collective-permute-start | bytes 589832 | tf_op jit(solution)/shard_map/ppermute | solution.py:286
  84.6 1.1 shard_map.123
  87.4 3.7 %collective-permute-done.47.refs_3_ = bf16[48,2048]{1,0:T(8,128)(2,1)S(1)} collective-permute-done((bf16[48,2048]{1,0:T(8,128)(2,1)S(1)}, bf16[48,2048]{1,0:T(8,128)(2,1)S(1)}, u32[]{:S(2)}, u32[]{:S(2)}) %collective-permute-start.47) | collective-permute-done | bytes 196640 | tf_op jit(solution)/shard_map/ppermute | solution.py:286
  91.5 1.6 collective-permute-done.36.refs_1_
  96.2 3.4 %collective-permute-done.38.refs_3_ = bf16[48,2048]{1,0:T(8,128)(2,1)S(1)} collective-permute-done((bf16[48,2048]{1,0:T(8,128)(2,1)S(1)}, bf16[48,2048]{1,0:T(8,128)(2,1)S(1)}, u32[]{:S(2)}, u32[]{:S(2)}) %collective-permute-start.38) | collective-permute-done | bytes 196640 | tf_op jit(solution)/shard_map/ppermute | solution.py:286
  100.9 2.4 %collective-permute-start.11 = (bf16[48,2048]{1,0:T(8,128)(2,1)S(1)}, bf16[48,2048]{1,0:T(8,128)(2,1)S(1)}, u32[]{:S(2)}, u32[]{:S(2)}) collective-permute-start(bf16[48,2048]{1,0:T(8,128)(2,1)S(1)} %get-tuple-element.68), channel_id=1, source_target_pairs={{0,6},{1,7},{2,4},{3,5},{4,2},{5,3},{6,0},{7,1},{8,14},{9,15},{10,... | collective-permute-start | bytes 589832 | tf_op jit(solution)/shard_map/ppermute | solution.py:286
  104.3 3.7 %collective-permute-done.26.refs_3_ = bf16[48,2048]{1,0:T(8,128)(2,1)S(1)} collective-permute-done((bf16[48,2048]{1,0:T(8,128)(2,1)S(1)}, bf16[48,2048]{1,0:T(8,128)(2,1)S(1)}, u32[]{:S(2)}, u32[]{:S(2)}) %collective-permute-start.26) | collective-permute-done | bytes 196640 | tf_op jit(solution)/shard_map/ppermute | solution.py:286
  108.0 3.6 %shard_map.124 = (bf16[48,2048]{1,0:T(8,128)(2,1)S(1)}, bf16[48,2048]{1,0:T(8,128)(2,1)S(1)}, bf16[48,2048]{1,0:T(8,128)(2,1)S(1)}, bf16[48,2048]{1,0:T(8,128)(2,1)S(1)}) custom-call(s32[5]{0:T(128)S(1)} %stack.23.where_ref, bf16[48,2048]{1,0:T(8,128)(2,1)S(1)} %get-tuple-element.77.refs_0_, bf16[48,2048]{1,0:T(8,128)(2,1)S(1)} %collective-permute-done.24.refs_1_, ...), custom_call_target="tpu_custom_call" | custom-call | flops 2415919104 | bytes 13369364 | tf_op jit(solution)/shard_map/pallas_call | solution.py:161
  112.9 3.1 %collective-permute-done.11.refs_3_ = bf16[48,2048]{1,0:T(8,128)(2,1)S(1)} collective-permute-done((bf16[48,2048]{1,0:T(8,128)(2,1)S(1)}, bf16[48,2048]{1,0:T(8,128)(2,1)S(1)}, u32[]{:S(2)}, u32[]{:S(2)}) %collective-permute-start.11) | collective-permute-done | bytes 196640 | tf_op jit(solution)/shard_map/ppermute | solution.py:286
  116.5 2.3 %collective-permute-start.29 = (bf16[48,2048]{1,0:T(8,128)(2,1)S(1)}, bf16[48,2048]{1,0:T(8,128)(2,1)S(1)}, u32[]{:S(2)}, u32[]{:S(2)}) collective-permute-start(bf16[48,2048]{1,0:T(8,128)(2,1)S(1)} %get-tuple-element.84), channel_id=1, source_target_pairs={{0,6},{1,7},{2,4},{3,5},{4,2},{5,3},{6,0},{7,1},{8,14},{9,15},{10,... | collective-permute-start | bytes 589832 | tf_op jit(solution)/shard_map/ppermute | solution.py:286
  118.7 3.9 %shard_map.121 = (bf16[48,2048]{1,0:T(8,128)(2,1)S(1)}, bf16[48,2048]{1,0:T(8,128)(2,1)S(1)}, bf16[48,2048]{1,0:T(8,128)(2,1)S(1)}, bf16[48,2048]{1,0:T(8,128)(2,1)S(1)}) custom-call(s32[5]{0:T(128)S(1)} %stack.23.where_ref, bf16[48,2048]{1,0:T(8,128)(2,1)S(1)} %get-tuple-element.65.refs_0_, bf16[48,2048]{1,0:T(8,128)(2,1)S(1)} %collective-permute-done.9.refs_1_, ...), custom_call_target="tpu_custom_call" | custom-call | flops 2415919104 | bytes 13369364 | tf_op jit(solution)/shard_map/pallas_call | solution.py:161
  125.5 3.2 %collective-permute-done.29.refs_3_ = bf16[48,2048]{1,0:T(8,128)(2,1)S(1)} collective-permute-done((bf16[48,2048]{1,0:T(8,128)(2,1)S(1)}, bf16[48,2048]{1,0:T(8,128)(2,1)S(1)}, u32[]{:S(2)}, u32[]{:S(2)}) %collective-permute-start.29) | collective-permute-done | bytes 196640 | tf_op jit(solution)/shard_map/ppermute | solution.py:286
  129.8 1.6 collective-permute-done.12.refs_1_
  132.4 6.5 %collective-permute-done.14.refs_3_ = bf16[48,2048]{1,0:T(8,128)(2,1)S(1)} collective-permute-done((bf16[48,2048]{1,0:T(8,128)(2,1)S(1)}, bf16[48,2048]{1,0:T(8,128)(2,1)S(1)}, u32[]{:S(2)}, u32[]{:S(2)}) %collective-permute-start.14) | collective-permute-done | bytes 196640 | tf_op jit(solution)/shard_map/ppermute | solution.py:286
  140.5 2.0 %collective-permute-start.53 = (bf16[64,2048]{1,0:T(8,128)(2,1)S(1)}, bf16[64,2048]{1,0:T(8,128)(2,1)S(1)}, u32[]{:S(2)}, u32[]{:S(2)}) collective-permute-start(bf16[64,2048]{1,0:T(8,128)(2,1)S(1)} %shard_map.136), channel_id=1, source_target_pairs={{0,8},{1,9},{2,10},{3,11},{4,12},{5,13},{6,14},{7,15},{8,24},{9,25... | collective-permute-start | bytes 786440 | tf_op jit(solution)/shard_map/ppermute | solution.py:286
  143.5 6.5 %collective-permute-done.53.refs_0_ = bf16[64,2048]{1,0:T(8,128)(2,1)S(1)} collective-permute-done((bf16[64,2048]{1,0:T(8,128)(2,1)S(1)}, bf16[64,2048]{1,0:T(8,128)(2,1)S(1)}, u32[]{:S(2)}, u32[]{:S(2)}) %collective-permute-start.53) | collective-permute-done | bytes 262176 | tf_op jit(solution)/shard_map/ppermute | solution.py:286
  150.6 1.8 %collective-permute-start.54 = (bf16[64,2048]{1,0:T(8,128)(2,1)S(1)}, bf16[64,2048]{1,0:T(8,128)(2,1)S(1)}, u32[]{:S(2)}, u32[]{:S(2)}) collective-permute-start(bf16[64,2048]{1,0:T(8,128)(2,1)S(1)} %shard_map.137), channel_id=1, source_target_pairs={{0,8},{1,9},{2,10},{3,11},{4,12},{5,13},{6,14},{7,15},{8,24},{9,25... | collective-permute-start | bytes 786440 | tf_op jit(solution)/shard_map/ppermute | solution.py:286
  152.4 3.2 %collective-permute-done.50.refs_0_ = bf16[64,2048]{1,0:T(8,128)(2,1)S(1)} collective-permute-done((bf16[64,2048]{1,0:T(8,128)(2,1)S(1)}, bf16[64,2048]{1,0:T(8,128)(2,1)S(1)}, u32[]{:S(2)}, u32[]{:S(2)}) %collective-permute-start.50) | collective-permute-done | bytes 262176 | tf_op jit(solution)/shard_map/ppermute | solution.py:286
  156.3 1.8 %collective-permute-start.51 = (bf16[64,2048]{1,0:T(8,128)(2,1)S(1)}, bf16[64,2048]{1,0:T(8,128)(2,1)S(1)}, u32[]{:S(2)}, u32[]{:S(2)}) collective-permute-start(bf16[64,2048]{1,0:T(8,128)(2,1)S(1)} %shard_map.134), channel_id=1, source_target_pairs={{0,8},{1,9},{2,10},{3,11},{4,12},{5,13},{6,14},{7,15},{8,24},{9,25... | collective-permute-start | bytes 786440 | tf_op jit(solution)/shard_map/ppermute | solution.py:286
  158.1 3.2 %collective-permute-done.54.refs_1_ = bf16[64,2048]{1,0:T(8,128)(2,1)S(1)} collective-permute-done((bf16[64,2048]{1,0:T(8,128)(2,1)S(1)}, bf16[64,2048]{1,0:T(8,128)(2,1)S(1)}, u32[]{:S(2)}, u32[]{:S(2)}) %collective-permute-start.54) | collective-permute-done | bytes 262176 | tf_op jit(solution)/shard_map/ppermute | solution.py:286
  161.2 4.2 %collective-permute-done.51.refs_0_ = bf16[64,2048]{1,0:T(8,128)(2,1)S(1)} collective-permute-done((bf16[64,2048]{1,0:T(8,128)(2,1)S(1)}, bf16[64,2048]{1,0:T(8,128)(2,1)S(1)}, u32[]{:S(2)}, u32[]{:S(2)}) %collective-permute-start.51) | collective-permute-done | bytes 262176 | tf_op jit(solution)/shard_map/ppermute | solution.py:286
  165.5 1.6 shard_map.138
  (111 shorter events, 27.2 us)
Async XLA Ops:
  2.8 14.5 %collective-permute-start = (bf16[144,512]{1,0:T(8,128)(2,1)S(1)}, bf16[144,512]{1,0:T(8,128)(2,1)S(1)}, u32[]{:S(2)}, u32[]{:S(2)}) collective-permute-start(bf16[144,512]{1,0:T(8,128)(2,1)S(1)} %get-tuple-element.58), channel_id=1, source_target_pairs={{0,1},{1,0},{2,3},{3,2},{4,5},{5,4},{6,7},{7,6},{8,9},{9,8},{10,11... | collective-permute-start | bytes 442376 | tf_op jit(solution)/shard_map/ppermute | solution.py:286
  3.4 14.0 %collective-permute-start.1 = (bf16[144,512]{1,0:T(8,128)(2,1)S(1)}, bf16[144,512]{1,0:T(8,128)(2,1)S(1)}, u32[]{:S(2)}, u32[]{:S(2)}) collective-permute-start(bf16[144,512]{1,0:T(8,128)(2,1)S(1)} %get-tuple-element.59), channel_id=1, source_target_pairs={{0,2},{1,3},{2,0},{3,1},{4,6},{5,7},{6,4},{7,5},{8,10},{9,11},{10,... | collective-permute-start | bytes 442376 | tf_op jit(solution)/shard_map/ppermute | solution.py:286
  6.0 11.4 %collective-permute-start.2 = (bf16[144,512]{1,0:T(8,128)(2,1)S(1)}, bf16[144,512]{1,0:T(8,128)(2,1)S(1)}, u32[]{:S(2)}, u32[]{:S(2)}) collective-permute-start(bf16[144,512]{1,0:T(8,128)(2,1)S(1)} %get-tuple-element.60), channel_id=1, source_target_pairs={{0,3},{1,2},{2,1},{3,0},{4,7},{5,6},{6,5},{7,4},{8,11},{9,10},{10,... | collective-permute-start | bytes 442376 | tf_op jit(solution)/shard_map/ppermute | solution.py:286
  20.2 10.8 %collective-permute-start.19 = (bf16[72,2048]{1,0:T(8,128)(2,1)S(1)}, bf16[72,2048]{1,0:T(8,128)(2,1)S(1)}, u32[]{:S(2)}, u32[]{:S(2)}) collective-permute-start(bf16[72,2048]{1,0:T(8,128)(2,1)S(1)} %get-tuple-element.63.refs_1_), channel_id=1, source_target_pairs={{0,8},{1,9},{2,10},{3,11},{4,12},{5,13},{6,14},{7,15},{8,24},{9,25... | collective-permute-start | bytes 884744 | tf_op jit(solution)/shard_map/ppermute | solution.py:286
  20.2 16.4 %collective-permute-start.16 = (bf16[64,2048]{1,0:T(8,128)(2,1)S(1)}, bf16[64,2048]{1,0:T(8,128)(2,1)S(1)}, u32[]{:S(2)}, u32[]{:S(2)}) collective-permute-start(bf16[64,2048]{1,0:T(8,128)(2,1)S(1)} %get-tuple-element.62.refs_0_), channel_id=1, source_target_pairs={{0,8},{1,9},{2,10},{3,11},{4,12},{5,13},{6,14},{7,15},{8,24},{9,25... | collective-permute-start | bytes 786440 | tf_op jit(solution)/shard_map/ppermute | solution.py:286
  31.0 11.9 %collective-permute-start.20 = (bf16[72,2048]{1,0:T(8,128)(2,1)S(1)}, bf16[72,2048]{1,0:T(8,128)(2,1)S(1)}, u32[]{:S(2)}, u32[]{:S(2)}) collective-permute-start(bf16[72,2048]{1,0:T(8,128)(2,1)S(1)} %collective-permute-done.19.refs_1_), channel_id=1, source_target_pairs={{0,8},{1,9},{2,10},{3,11},{4,12},{5,13},{6,14},{7,15},{8,24},{9,25... | collective-permute-start | bytes 884744 | tf_op jit(solution)/shard_map/ppermute | solution.py:286
  36.6 11.2 %collective-permute-start.17 = (bf16[64,2048]{1,0:T(8,128)(2,1)S(1)}, bf16[64,2048]{1,0:T(8,128)(2,1)S(1)}, u32[]{:S(2)}, u32[]{:S(2)}) collective-permute-start(bf16[64,2048]{1,0:T(8,128)(2,1)S(1)} %collective-permute-done.16.refs_0_), channel_id=1, source_target_pairs={{0,8},{1,9},{2,10},{3,11},{4,12},{5,13},{6,14},{7,15},{8,24},{9,25... | collective-permute-start | bytes 786440 | tf_op jit(solution)/shard_map/ppermute | solution.py:286
  36.6 11.2 %collective-permute-start.40 = (bf16[64,2048]{1,0:T(8,128)(2,1)S(1)}, bf16[64,2048]{1,0:T(8,128)(2,1)S(1)}, u32[]{:S(2)}, u32[]{:S(2)}) collective-permute-start(bf16[64,2048]{1,0:T(8,128)(2,1)S(1)} %collective-permute-done.16.refs_0_), channel_id=1, source_target_pairs={{0,1},{1,0},{2,3},{3,2},{4,5},{5,4},{6,7},{7,6},{8,9},{9,8},{10,11... | collective-permute-start | bytes 786440 | tf_op jit(solution)/shard_map/ppermute | solution.py:286
  36.6 13.6 %collective-permute-start.41 = (bf16[72,2048]{1,0:T(8,128)(2,1)S(1)}, bf16[72,2048]{1,0:T(8,128)(2,1)S(1)}, u32[]{:S(2)}, u32[]{:S(2)}) collective-permute-start(bf16[72,2048]{1,0:T(8,128)(2,1)S(1)} %collective-permute-done.19.refs_1_), channel_id=1, source_target_pairs={{0,1},{1,0},{2,3},{3,2},{4,5},{5,4},{6,7},{7,6},{8,9},{9,8},{10,11... | collective-permute-start | bytes 884744 | tf_op jit(solution)/shard_map/ppermute | solution.py:286
  42.9 10.2 %collective-permute-start.32 = (bf16[72,2048]{1,0:T(8,128)(2,1)S(1)}, bf16[72,2048]{1,0:T(8,128)(2,1)S(1)}, u32[]{:S(2)}, u32[]{:S(2)}) collective-permute-start(bf16[72,2048]{1,0:T(8,128)(2,1)S(1)} %collective-permute-done.20.refs_1_), channel_id=1, source_target_pairs={{0,1},{1,0},{2,3},{3,2},{4,5},{5,4},{6,7},{7,6},{8,9},{9,8},{10,11... | collective-permute-start | bytes 884744 | tf_op jit(solution)/shard_map/ppermute | solution.py:286
  47.8 17.4 %collective-permute-start.21 = (bf16[72,2048]{1,0:T(8,128)(2,1)S(1)}, bf16[72,2048]{1,0:T(8,128)(2,1)S(1)}, u32[]{:S(2)}, u32[]{:S(2)}) collective-permute-start(bf16[72,2048]{1,0:T(8,128)(2,1)S(1)} %collective-permute-done.20.refs_1_), channel_id=1, source_target_pairs={{0,8},{1,9},{2,10},{3,11},{4,12},{5,13},{6,14},{7,15},{8,24},{9,25... | collective-permute-start | bytes 884744 | tf_op jit(solution)/shard_map/ppermute | solution.py:286
  47.8 16.8 %collective-permute-start.18 = (bf16[64,2048]{1,0:T(8,128)(2,1)S(1)}, bf16[64,2048]{1,0:T(8,128)(2,1)S(1)}, u32[]{:S(2)}, u32[]{:S(2)}) collective-permute-start(bf16[64,2048]{1,0:T(8,128)(2,1)S(1)} %collective-permute-done.17.refs_0_), channel_id=1, source_target_pairs={{0,8},{1,9},{2,10},{3,11},{4,12},{5,13},{6,14},{7,15},{8,24},{9,25... | collective-permute-start | bytes 786440 | tf_op jit(solution)/shard_map/ppermute | solution.py:286
  52.5 7.8 %collective-permute-start.43 = (bf16[48,2048]{1,0:T(8,128)(2,1)S(1)}, bf16[48,2048]{1,0:T(8,128)(2,1)S(1)}, u32[]{:S(2)}, u32[]{:S(2)}) collective-permute-start(bf16[48,2048]{1,0:T(8,128)(2,1)S(1)} %get-tuple-element.101), channel_id=1, source_target_pairs={{0,4},{1,5},{2,6},{3,7},{4,0},{5,1},{6,2},{7,3},{8,12},{9,13},{10,... | collective-permute-start | bytes 589832 | tf_op jit(solution)/shard_map/ppermute | solution.py:286
  53.1 10.4 %collective-permute-start.44 = (bf16[48,2048]{1,0:T(8,128)(2,1)S(1)}, bf16[48,2048]{1,0:T(8,128)(2,1)S(1)}, u32[]{:S(2)}, u32[]{:S(2)}) collective-permute-start(bf16[48,2048]{1,0:T(8,128)(2,1)S(1)} %get-tuple-element.102), channel_id=1, source_target_pairs={{0,6},{1,7},{2,4},{3,5},{4,2},{5,3},{6,0},{7,1},{8,14},{9,15},{10,... | collective-permute-start | bytes 589832 | tf_op jit(solution)/shard_map/ppermute | solution.py:286
  58.3 20.7 %collective-permute-start.8 = (bf16[72,2048]{1,0:T(8,128)(2,1)S(1)}, bf16[72,2048]{1,0:T(8,128)(2,1)S(1)}, u32[]{:S(2)}, u32[]{:S(2)}) collective-permute-start(bf16[72,2048]{1,0:T(8,128)(2,1)S(1)} %get-tuple-element.63.refs_1_), channel_id=1, source_target_pairs={{0,1},{1,0},{2,3},{3,2},{4,5},{5,4},{6,7},{7,6},{8,9},{9,8},{10,11... | collective-permute-start | bytes 884744 | tf_op jit(solution)/shard_map/ppermute | solution.py:286
  60.3 18.4 %collective-permute-start.7 = (bf16[64,2048]{1,0:T(8,128)(2,1)S(1)}, bf16[64,2048]{1,0:T(8,128)(2,1)S(1)}, u32[]{:S(2)}, u32[]{:S(2)}) collective-permute-start(bf16[64,2048]{1,0:T(8,128)(2,1)S(1)} %get-tuple-element.62.refs_0_), channel_id=1, source_target_pairs={{0,1},{1,0},{2,3},{3,2},{4,5},{5,4},{6,7},{7,6},{8,9},{9,8},{10,11... | collective-permute-start | bytes 786440 | tf_op jit(solution)/shard_map/ppermute | solution.py:286
  64.7 7.7 %collective-permute-start.34 = (bf16[48,2048]{1,0:T(8,128)(2,1)S(1)}, bf16[48,2048]{1,0:T(8,128)(2,1)S(1)}, u32[]{:S(2)}, u32[]{:S(2)}) collective-permute-start(bf16[48,2048]{1,0:T(8,128)(2,1)S(1)} %get-tuple-element.90), channel_id=1, source_target_pairs={{0,4},{1,5},{2,6},{3,7},{4,0},{5,1},{6,2},{7,3},{8,12},{9,13},{10,... | collective-permute-start | bytes 589832 | tf_op jit(solution)/shard_map/ppermute | solution.py:286
  65.3 9.8 %collective-permute-start.35 = (bf16[48,2048]{1,0:T(8,128)(2,1)S(1)}, bf16[48,2048]{1,0:T(8,128)(2,1)S(1)}, u32[]{:S(2)}, u32[]{:S(2)}) collective-permute-start(bf16[48,2048]{1,0:T(8,128)(2,1)S(1)} %get-tuple-element.91), channel_id=1, source_target_pairs={{0,6},{1,7},{2,4},{3,5},{4,2},{5,3},{6,0},{7,1},{8,14},{9,15},{10,... | collective-permute-start | bytes 589832 | tf_op jit(solution)/shard_map/ppermute | solution.py:286
  70.7 10.4 %collective-permute-start.45 = (bf16[48,2048]{1,0:T(8,128)(2,1)S(1)}, bf16[48,2048]{1,0:T(8,128)(2,1)S(1)}, u32[]{:S(2)}, u32[]{:S(2)}) collective-permute-start(bf16[48,2048]{1,0:T(8,128)(2,1)S(1)} %get-tuple-element.104), channel_id=1, source_target_pairs={{0,2},{1,3},{2,0},{3,1},{4,6},{5,7},{6,4},{7,5},{8,10},{9,11},{10,... | collective-permute-start | bytes 589832 | tf_op jit(solution)/shard_map/ppermute | solution.py:286
  72.3 10.0 %collective-permute-start.22 = (bf16[64,2048]{1,0:T(8,128)(2,1)S(1)}, bf16[64,2048]{1,0:T(8,128)(2,1)S(1)}, u32[]{:S(2)}, u32[]{:S(2)}) collective-permute-start(bf16[64,2048]{1,0:T(8,128)(2,1)S(1)} %collective-permute-done.18.refs_0_), channel_id=1, source_target_pairs={{0,1},{1,0},{2,3},{3,2},{4,5},{5,4},{6,7},{7,6},{8,9},{9,8},{10,11... | collective-permute-start | bytes 786440 | tf_op jit(solution)/shard_map/ppermute | solution.py:286
  75.1 7.4 %collective-permute-start.23 = (bf16[72,2048]{1,0:T(8,128)(2,1)S(1)}, bf16[72,2048]{1,0:T(8,128)(2,1)S(1)}, u32[]{:S(2)}, u32[]{:S(2)}) collective-permute-start(bf16[72,2048]{1,0:T(8,128)(2,1)S(1)} %collective-permute-done.21.refs_1_), channel_id=1, source_target_pairs={{0,1},{1,0},{2,3},{3,2},{4,5},{5,4},{6,7},{7,6},{8,9},{9,8},{10,11... | collective-permute-start | bytes 884744 | tf_op jit(solution)/shard_map/ppermute | solution.py:286
  78.7 7.8 %collective-permute-start.46 = (bf16[48,2048]{1,0:T(8,128)(2,1)S(1)}, bf16[48,2048]{1,0:T(8,128)(2,1)S(1)}, u32[]{:S(2)}, u32[]{:S(2)}) collective-permute-start(bf16[48,2048]{1,0:T(8,128)(2,1)S(1)} %get-tuple-element.105), channel_id=1, source_target_pairs={{0,4},{1,5},{2,6},{3,7},{4,0},{5,1},{6,2},{7,3},{8,12},{9,13},{10,... | collective-permute-start | bytes 589832 | tf_op jit(solution)/shard_map/ppermute | solution.py:286
  79.0 12.1 %collective-permute-start.47 = (bf16[48,2048]{1,0:T(8,128)(2,1)S(1)}, bf16[48,2048]{1,0:T(8,128)(2,1)S(1)}, u32[]{:S(2)}, u32[]{:S(2)}) collective-permute-start(bf16[48,2048]{1,0:T(8,128)(2,1)S(1)} %get-tuple-element.106), channel_id=1, source_target_pairs={{0,6},{1,7},{2,4},{3,5},{4,2},{5,3},{6,0},{7,1},{8,14},{9,15},{10,... | collective-permute-start | bytes 589832 | tf_op jit(solution)/shard_map/ppermute | solution.py:286
  81.1 12.0 %collective-permute-start.36 = (bf16[48,2048]{1,0:T(8,128)(2,1)S(1)}, bf16[48,2048]{1,0:T(8,128)(2,1)S(1)}, u32[]{:S(2)}, u32[]{:S(2)}) collective-permute-start(bf16[48,2048]{1,0:T(8,128)(2,1)S(1)} %get-tuple-element.93), channel_id=1, source_target_pairs={{0,2},{1,3},{2,0},{3,1},{4,6},{5,7},{6,4},{7,5},{8,10},{9,11},{10,... | collective-permute-start | bytes 589832 | tf_op jit(solution)/shard_map/ppermute | solution.py:286
  82.3 12.7 %collective-permute-start.37 = (bf16[48,2048]{1,0:T(8,128)(2,1)S(1)}, bf16[48,2048]{1,0:T(8,128)(2,1)S(1)}, u32[]{:S(2)}, u32[]{:S(2)}) collective-permute-start(bf16[48,2048]{1,0:T(8,128)(2,1)S(1)} %get-tuple-element.94), channel_id=1, source_target_pairs={{0,4},{1,5},{2,6},{3,7},{4,0},{5,1},{6,2},{7,3},{8,12},{9,13},{10,... | collective-permute-start | bytes 589832 | tf_op jit(solution)/shard_map/ppermute | solution.py:286
  82.5 17.1 %collective-permute-start.38 = (bf16[48,2048]{1,0:T(8,128)(2,1)S(1)}, bf16[48,2048]{1,0:T(8,128)(2,1)S(1)}, u32[]{:S(2)}, u32[]{:S(2)}) collective-permute-start(bf16[48,2048]{1,0:T(8,128)(2,1)S(1)} %get-tuple-element.95), channel_id=1, source_target_pairs={{0,6},{1,7},{2,4},{3,5},{4,2},{5,3},{6,0},{7,1},{8,14},{9,15},{10,... | collective-permute-start | bytes 589832 | tf_op jit(solution)/shard_map/ppermute | solution.py:286
  86.6 14.4 %collective-permute-start.24 = (bf16[48,2048]{1,0:T(8,128)(2,1)S(1)}, bf16[48,2048]{1,0:T(8,128)(2,1)S(1)}, u32[]{:S(2)}, u32[]{:S(2)}) collective-permute-start(bf16[48,2048]{1,0:T(8,128)(2,1)S(1)} %get-tuple-element.78), channel_id=1, source_target_pairs={{0,2},{1,3},{2,0},{3,1},{4,6},{5,7},{6,4},{7,5},{8,10},{9,11},{10,... | collective-permute-start | bytes 589832 | tf_op jit(solution)/shard_map/ppermute | solution.py:286
  91.1 12.4 %collective-permute-start.25 = (bf16[48,2048]{1,0:T(8,128)(2,1)S(1)}, bf16[48,2048]{1,0:T(8,128)(2,1)S(1)}, u32[]{:S(2)}, u32[]{:S(2)}) collective-permute-start(bf16[48,2048]{1,0:T(8,128)(2,1)S(1)} %get-tuple-element.79), channel_id=1, source_target_pairs={{0,4},{1,5},{2,6},{3,7},{4,0},{5,1},{6,2},{7,3},{8,12},{9,13},{10,... | collective-permute-start | bytes 589832 | tf_op jit(solution)/shard_map/ppermute | solution.py:286
  93.1 14.9 %collective-permute-start.26 = (bf16[48,2048]{1,0:T(8,128)(2,1)S(1)}, bf16[48,2048]{1,0:T(8,128)(2,1)S(1)}, u32[]{:S(2)}, u32[]{:S(2)}) collective-permute-start(bf16[48,2048]{1,0:T(8,128)(2,1)S(1)} %get-tuple-element.80), channel_id=1, source_target_pairs={{0,6},{1,7},{2,4},{3,5},{4,2},{5,3},{6,0},{7,1},{8,14},{9,15},{10,... | collective-permute-start | bytes 589832 | tf_op jit(solution)/shard_map/ppermute | solution.py:286
  95.0 27.6 %collective-permute-start.48 = (bf16[128,2048]{1,0:T(8,128)(2,1)S(1)}, bf16[128,2048]{1,0:T(8,128)(2,1)S(1)}, u32[]{:S(2)}, u32[]{:S(2)}) collective-permute-start(bf16[128,2048]{1,0:T(8,128)(2,1)S(1)} %get-tuple-element.108), channel_id=1, source_target_pairs={{0,1},{1,0},{2,3},{3,2},{4,5},{5,4},{6,7},{7,6},{8,9},{9,8},{10,11... | collective-permute-start | bytes 1572872 | tf_op jit(solution)/shard_map/ppermute | solution.py:286
  99.5 12.4 %collective-permute-start.10 = (bf16[48,2048]{1,0:T(8,128)(2,1)S(1)}, bf16[48,2048]{1,0:T(8,128)(2,1)S(1)}, u32[]{:S(2)}, u32[]{:S(2)}) collective-permute-start(bf16[48,2048]{1,0:T(8,128)(2,1)S(1)} %get-tuple-element.67), channel_id=1, source_target_pairs={{0,4},{1,5},{2,6},{3,7},{4,0},{5,1},{6,2},{7,3},{8,12},{9,13},{10,... | collective-permute-start | bytes 589832 | tf_op jit(solution)/shard_map/ppermute | solution.py:286
  100.9 15.1 %collective-permute-start.11 = (bf16[48,2048]{1,0:T(8,128)(2,1)S(1)}, bf16[48,2048]{1,0:T(8,128)(2,1)S(1)}, u32[]{:S(2)}, u32[]{:S(2)}) collective-permute-start(bf16[48,2048]{1,0:T(8,128)(2,1)S(1)} %get-tuple-element.68), channel_id=1, source_target_pairs={{0,6},{1,7},{2,4},{3,5},{4,2},{5,3},{6,0},{7,1},{8,14},{9,15},{10,... | collective-permute-start | bytes 589832 | tf_op jit(solution)/shard_map/ppermute | solution.py:286
  103.5 12.9 %collective-permute-start.9 = (bf16[48,2048]{1,0:T(8,128)(2,1)S(1)}, bf16[48,2048]{1,0:T(8,128)(2,1)S(1)}, u32[]{:S(2)}, u32[]{:S(2)}) collective-permute-start(bf16[48,2048]{1,0:T(8,128)(2,1)S(1)} %get-tuple-element.66), channel_id=1, source_target_pairs={{0,2},{1,3},{2,0},{3,1},{4,6},{5,7},{6,4},{7,5},{8,10},{9,11},{10,... | collective-permute-start | bytes 589832 | tf_op jit(solution)/shard_map/ppermute | solution.py:286
  108.0 31.9 %collective-permute-start.39 = (bf16[128,2048]{1,0:T(8,128)(2,1)S(1)}, bf16[128,2048]{1,0:T(8,128)(2,1)S(1)}, u32[]{:S(2)}, u32[]{:S(2)}) collective-permute-start(bf16[128,2048]{1,0:T(8,128)(2,1)S(1)} %get-tuple-element.97), channel_id=1, source_target_pairs={{0,1},{1,0},{2,3},{3,2},{4,5},{5,4},{6,7},{7,6},{8,9},{9,8},{10,11... | collective-permute-start | bytes 1572872 | tf_op jit(solution)/shard_map/ppermute | solution.py:286
  112.0 11.5 %collective-permute-start.27 = (bf16[48,2048]{1,0:T(8,128)(2,1)S(1)}, bf16[48,2048]{1,0:T(8,128)(2,1)S(1)}, u32[]{:S(2)}, u32[]{:S(2)}) collective-permute-start(bf16[48,2048]{1,0:T(8,128)(2,1)S(1)} %get-tuple-element.82), channel_id=1, source_target_pairs={{0,2},{1,3},{2,0},{3,1},{4,6},{5,7},{6,4},{7,5},{8,10},{9,11},{10,... | collective-permute-start | bytes 589832 | tf_op jit(solution)/shard_map/ppermute | solution.py:286
  116.1 9.0 %collective-permute-start.28 = (bf16[48,2048]{1,0:T(8,128)(2,1)S(1)}, bf16[48,2048]{1,0:T(8,128)(2,1)S(1)}, u32[]{:S(2)}, u32[]{:S(2)}) collective-permute-start(bf16[48,2048]{1,0:T(8,128)(2,1)S(1)} %get-tuple-element.83), channel_id=1, source_target_pairs={{0,4},{1,5},{2,6},{3,7},{4,0},{5,1},{6,2},{7,3},{8,12},{9,13},{10,... | collective-permute-start | bytes 589832 | tf_op jit(solution)/shard_map/ppermute | solution.py:286
  116.5 12.3 %collective-permute-start.29 = (bf16[48,2048]{1,0:T(8,128)(2,1)S(1)}, bf16[48,2048]{1,0:T(8,128)(2,1)S(1)}, u32[]{:S(2)}, u32[]{:S(2)}) collective-permute-start(bf16[48,2048]{1,0:T(8,128)(2,1)S(1)} %get-tuple-element.84), channel_id=1, source_target_pairs={{0,6},{1,7},{2,4},{3,5},{4,2},{5,3},{6,0},{7,1},{8,14},{9,15},{10,... | collective-permute-start | bytes 589832 | tf_op jit(solution)/shard_map/ppermute | solution.py:286
  122.6 8.8 %collective-permute-start.12 = (bf16[48,2048]{1,0:T(8,128)(2,1)S(1)}, bf16[48,2048]{1,0:T(8,128)(2,1)S(1)}, u32[]{:S(2)}, u32[]{:S(2)}) collective-permute-start(bf16[48,2048]{1,0:T(8,128)(2,1)S(1)} %get-tuple-element.70), channel_id=1, source_target_pairs={{0,2},{1,3},{2,0},{3,1},{4,6},{5,7},{6,4},{7,5},{8,10},{9,11},{10,... | collective-permute-start | bytes 589832 | tf_op jit(solution)/shard_map/ppermute | solution.py:286
  123.5 7.9 %collective-permute-start.13 = (bf16[48,2048]{1,0:T(8,128)(2,1)S(1)}, bf16[48,2048]{1,0:T(8,128)(2,1)S(1)}, u32[]{:S(2)}, u32[]{:S(2)}) collective-permute-start(bf16[48,2048]{1,0:T(8,128)(2,1)S(1)} %get-tuple-element.71), channel_id=1, source_target_pairs={{0,4},{1,5},{2,6},{3,7},{4,0},{5,1},{6,2},{7,3},{8,12},{9,13},{10,... | collective-permute-start | bytes 589832 | tf_op jit(solution)/shard_map/ppermute | solution.py:286
  125.1 14.8 %collective-permute-start.52 = (bf16[64,2048]{1,0:T(8,128)(2,1)S(1)}, bf16[64,2048]{1,0:T(8,128)(2,1)S(1)}, u32[]{:S(2)}, u32[]{:S(2)}) collective-permute-start(bf16[64,2048]{1,0:T(8,128)(2,1)S(1)} %shard_map.135), channel_id=1, source_target_pairs={{0,8},{1,9},{2,10},{3,11},{4,12},{5,13},{6,14},{7,15},{8,24},{9,25... | collective-permute-start | bytes 786440 | tf_op jit(solution)/shard_map/ppermute | solution.py:286
  129.8 20.3 %collective-permute-start.30 = (bf16[128,2048]{1,0:T(8,128)(2,1)S(1)}, bf16[128,2048]{1,0:T(8,128)(2,1)S(1)}, u32[]{:S(2)}, u32[]{:S(2)}) collective-permute-start(bf16[128,2048]{1,0:T(8,128)(2,1)S(1)} %get-tuple-element.86), channel_id=1, source_target_pairs={{0,1},{1,0},{2,3},{3,2},{4,5},{5,4},{6,7},{7,6},{8,9},{9,8},{10,11... | collective-permute-start | bytes 1572872 | tf_op jit(solution)/shard_map/ppermute | solution.py:286
  131.4 11.2 %collective-permute-start.49 = (bf16[64,2048]{1,0:T(8,128)(2,1)S(1)}, bf16[64,2048]{1,0:T(8,128)(2,1)S(1)}, u32[]{:S(2)}, u32[]{:S(2)}) collective-permute-start(bf16[64,2048]{1,0:T(8,128)(2,1)S(1)} %shard_map.132), channel_id=1, source_target_pairs={{0,8},{1,9},{2,10},{3,11},{4,12},{5,13},{6,14},{7,15},{8,24},{9,25... | collective-permute-start | bytes 786440 | tf_op jit(solution)/shard_map/ppermute | solution.py:286
  131.4 7.5 %collective-permute-start.14 = (bf16[48,2048]{1,0:T(8,128)(2,1)S(1)}, bf16[48,2048]{1,0:T(8,128)(2,1)S(1)}, u32[]{:S(2)}, u32[]{:S(2)}) collective-permute-start(bf16[48,2048]{1,0:T(8,128)(2,1)S(1)} %get-tuple-element.72), channel_id=1, source_target_pairs={{0,6},{1,7},{2,4},{3,5},{4,2},{5,3},{6,0},{7,1},{8,14},{9,15},{10,... | collective-permute-start | bytes 589832 | tf_op jit(solution)/shard_map/ppermute | solution.py:286
  140.5 9.5 %collective-permute-start.53 = (bf16[64,2048]{1,0:T(8,128)(2,1)S(1)}, bf16[64,2048]{1,0:T(8,128)(2,1)S(1)}, u32[]{:S(2)}, u32[]{:S(2)}) collective-permute-start(bf16[64,2048]{1,0:T(8,128)(2,1)S(1)} %shard_map.136), channel_id=1, source_target_pairs={{0,8},{1,9},{2,10},{3,11},{4,12},{5,13},{6,14},{7,15},{8,24},{9,25... | collective-permute-start | bytes 786440 | tf_op jit(solution)/shard_map/ppermute | solution.py:286
  142.6 15.5 %collective-permute-start.15 = (bf16[128,2048]{1,0:T(8,128)(2,1)S(1)}, bf16[128,2048]{1,0:T(8,128)(2,1)S(1)}, u32[]{:S(2)}, u32[]{:S(2)}) collective-permute-start(bf16[128,2048]{1,0:T(8,128)(2,1)S(1)} %get-tuple-element.74), channel_id=1, source_target_pairs={{0,1},{1,0},{2,3},{3,2},{4,5},{5,4},{6,7},{7,6},{8,9},{9,8},{10,11... | collective-permute-start | bytes 1572872 | tf_op jit(solution)/shard_map/ppermute | solution.py:286
  143.2 12.4 %collective-permute-start.50 = (bf16[64,2048]{1,0:T(8,128)(2,1)S(1)}, bf16[64,2048]{1,0:T(8,128)(2,1)S(1)}, u32[]{:S(2)}, u32[]{:S(2)}) collective-permute-start(bf16[64,2048]{1,0:T(8,128)(2,1)S(1)} %shard_map.133), channel_id=1, source_target_pairs={{0,8},{1,9},{2,10},{3,11},{4,12},{5,13},{6,14},{7,15},{8,24},{9,25... | collective-permute-start | bytes 786440 | tf_op jit(solution)/shard_map/ppermute | solution.py:286
  150.6 10.6 %collective-permute-start.54 = (bf16[64,2048]{1,0:T(8,128)(2,1)S(1)}, bf16[64,2048]{1,0:T(8,128)(2,1)S(1)}, u32[]{:S(2)}, u32[]{:S(2)}) collective-permute-start(bf16[64,2048]{1,0:T(8,128)(2,1)S(1)} %shard_map.137), channel_id=1, source_target_pairs={{0,8},{1,9},{2,10},{3,11},{4,12},{5,13},{6,14},{7,15},{8,24},{9,25... | collective-permute-start | bytes 786440 | tf_op jit(solution)/shard_map/ppermute | solution.py:286
  156.3 9.2 %collective-permute-start.51 = (bf16[64,2048]{1,0:T(8,128)(2,1)S(1)}, bf16[64,2048]{1,0:T(8,128)(2,1)S(1)}, u32[]{:S(2)}, u32[]{:S(2)}) collective-permute-start(bf16[64,2048]{1,0:T(8,128)(2,1)S(1)} %shard_map.134), channel_id=1, source_target_pairs={{0,8},{1,9},{2,10},{3,11},{4,12},{5,13},{6,14},{7,15},{8,24},{9,25... | collective-permute-start | bytes 786440 | tf_op jit(solution)/shard_map/ppermute | solution.py:286
  (20 other events, 308.7 us)

commit v6 on v5

--- a/solution.py
+++ b/solution.py
@@ -10,6 +10,8 @@
 
 GROUPS = 4
 CORES = 2
+HIDDEN_CUT = 256
+DOWN_CUT = 2048
 COVER_FLOPS = 40_000_000_000
 
 norm_eps = 1e-05
@@ -201,44 +203,75 @@
 
 
 def share_kernel(where_ref, factor_ref, *refs, capacity):
-    back_refs, (given_ref, kept_ref) = refs[:-2], refs[-2:]
-    given_ref[...] = weighted_sum(factor_ref, back_refs, 1, capacity).astype(jnp.bfloat16)
+    back_refs, given_refs, kept_ref = refs[:-3], refs[-3:-1], refs[-1]
+    given = weighted_sum(factor_ref, back_refs, 1, capacity).astype(jnp.bfloat16)
+    half = given_refs[0].shape[0]
+    given_refs[0][...] = given[:half]
+    given_refs[1][...] = given[half:]
     kept_ref[...] = weighted_sum(factor_ref, back_refs, 0, capacity)
 
 
 def sum_kernel(where_ref, kept_ref, got_ref, *refs, start):
     size = refs[-1].shape[0]
     rows = slice(start, start + size)
-    total = kept_ref[rows, :] + got_ref[rows, :].astype(jnp.float32)
+    total = kept_ref[rows, :] + got_ref[...].astype(jnp.float32)
     for ref in refs[:-1]:
         total = total + ref[...].astype(jnp.float32)
     refs[-1][...] = total.astype(jnp.bfloat16)
 
 
-def final_kernel(where_ref, kept_ref, got_ref, resid_ref, *refs):
-    total = kept_ref[...] + got_ref[...].astype(jnp.float32) + resid_ref[...].astype(jnp.float32)
-    if len(refs) > 1:
-        total = total + jnp.concatenate([ref[...] for ref in refs[:-1]], 0).astype(jnp.float32)
+def final_kernel(where_ref, kept_ref, resid_ref, *refs, count):
+    total = kept_ref[...] + resid_ref[...].astype(jnp.float32)
+    for ref in refs[:count]:
+        total = total + ref[...].astype(jnp.float32)
     refs[-1][...] = total.astype(jnp.bfloat16)
+
+
+def final_half(where, h, kept, resid, pieces, so_far):
+    size, width = pieces[0].shape
+    part = pl.BlockSpec((size, width), lambda i: (h, 0))
+    whole = pl.BlockSpec((size, width), lambda i: (0, 0))
+    args = [where, kept, resid, *pieces] + ([] if so_far is None else [so_far])
+    rest = [] if so_far is None else [pl.BlockSpec(memory_space=pl.ANY)]
+    return pl.pallas_call(
+        functools.partial(final_kernel, count=len(pieces)),
+        grid=(1,),
+        out_shape=jax.ShapeDtypeStruct(resid.shape, jnp.bfloat16),
+        in_specs=[pl.BlockSpec(memory_space=pltpu.SMEM), part, part] + [whole] * len(pieces) + rest,
+        out_specs=part,
+        input_output_aliases={} if so_far is None else {len(args) - 1: 0},
+        compiler_params=pltpu.CompilerParams(vmem_limit_bytes=VMEM_BYTES),
+        cost_estimate=pl.CostEstimate(
+            flops=resid.size, transcendentals=0, bytes_accessed=4 * resid.size
+        ),
+        name="final",
+    )(*args)
 
 
 def expert_kernel(where_ref, *refs):
     chips = (len(refs) - 3) // 2
-    row_refs, (gate_ref, up_ref, down_ref), out_refs = refs[:chips], refs[chips : chips + 3], refs[chips + 3 :]
+    row_refs, matrices, out_refs = refs[:chips], refs[chips : chips + 3], refs[chips + 3 :]
+    gate_ref, up_ref, down_ref = matrices
     rows = jnp.concatenate([ref[...] for ref in row_refs], 0)
     hidden = gate_ref.shape[1]
-    cut = min(hidden, 256)
-    total = None
+    cut = min(hidden, HIDDEN_CUT)
+    parts = []
     for start in range(0, hidden, cut):
         lanes = slice(start, start + cut)
         gated = jnp.minimum(dot32(rows, gate_ref[:, lanes]), clamp_limit)
         linear = jnp.clip(dot32(rows, up_ref[:, lanes]), -clamp_limit, clamp_limit)
-        activated = (gated * jax.nn.sigmoid(sigmoid_alpha * gated) * (linear + 1.0)).astype(
-            jnp.bfloat16
-        )
-        part = dot32(activated, down_ref[lanes, :])
-        total = part if total is None else total + part
-    result = total.astype(jnp.bfloat16)
+        activated = gated * jax.nn.sigmoid(sigmoid_alpha * gated) * (linear + 1.0)
+        parts.append(activated.astype(jnp.bfloat16))
+    activated = jnp.concatenate(parts, 1)
+    width = down_ref.shape[1]
+    cut = min(width, DOWN_CUT)
+    result = jnp.concatenate(
+        [
+            dot32(activated, down_ref[:, start : start + cut]).astype(jnp.bfloat16)
+            for start in range(0, width, cut)
+        ],
+        1,
+    )
     length = row_refs[0].shape[0]
     for d in range(chips):
         out_refs[d][...] = result[d * length : (d + 1) * length]
@@ -353,12 +386,12 @@
         return in_plane(results)
 
     def share(factors, back):
-        given, kept = call(
+        *given, kept = call(
             functools.partial(share_kernel, capacity=capacity),
-            [shape, jax.ShapeDtypeStruct(shape.shape, jnp.float32)],
+            [piece, piece, jax.ShapeDtypeStruct(shape.shape, jnp.float32)],
             [where, factors, *back], 2 * small,
         )
-        return kept, swap(given)
+        return kept, [swap(given[h]) for h in range(2)]
 
     chunks = [chunk]
     for _ in range(1, planes):
@@ -370,18 +403,17 @@
     returned = [experts(arrived[s][0]) for s in range(planes)]
     carried = [[], []]
     for s in range(1, planes):
-        shares = share(arrived[s][1], returned[s])
+        kept, got = share(arrived[s][1], returned[s])
         for h in range(2):
             (total,) = call(
                 functools.partial(sum_kernel, start=h * half), [piece],
-                [where, *shares, *carried[h]], tokens * width,
+                [where, kept, got[h], *carried[h]], tokens * width,
             )
             carried[h] = [hop(total)]
-    shares = share(arrived[0][1], returned[0])
-    (out,) = call(
-        final_kernel, [shape], [where, *shares, resid, *carried[0], *carried[1]],
-        tokens * width,
-    )
+    kept, got = share(arrived[0][1], returned[0])
+    out = None
+    for h in range(2):
+        out = final_half(where, h, kept, resid, [got[h], *carried[h]], out)
     return out
 
 

time: 167 us -> 158 us (0.946)
  waiting for transfers between devices: 87.8 us -> 70.9 us
  starting transfers between devices: 44.8 us -> 52.8 us
    ppermute x55 -> x59, waiting for transfers between devices: 87.8 us -> 70.9 us  [move(): return lax.ppermute(value, every, [(i, to(i)) for i in range(devices)])]
    ppermute x55 -> x59, starting transfers between devices: 44.8 us -> 52.8 us  [move(): return lax.ppermute(value, every, [(i, to(i)) for i in range(devices)])]
    pallas_call x21 -> x20, Pallas kernels: 31.8 us -> 28.8 us  [call(): pl.pallas_call(kernel, out_shape=tuple(shapes), in_specs=specs, out_specs...]
    pallas_call x0 -> x2, Pallas kernels: none -> 2.75 us  [final_half(): pl.pallas_call(functools.partial(final_kernel, count=len(pieces)), grid=(...]
  transfers between devices with their start and end apart: 55 -> 59, of which waited for: 28 -> 21; matrix products, arithmetic and copies ran while one was open for 0% -> 0% of each run, Pallas kernels for 16% -> 17%
where the time goes in v6:
time: 158 us
  waiting for transfers between devices  70.9 us (45%)
  starting transfers between devices  52.8 us (33%)
  Pallas kernels  31.5 us (20%)
  local copies, waits for them, and re-layouts  2.19 us (1%)
    ppermute x59, waiting for transfers between devices, move(): return lax.ppermute(value, every, [(i, to(i)) for i in range(devices)])  70.9 us
    ppermute x59, starting transfers between devices, move(): return lax.ppermute(value, every, [(i, to(i)) for i in range(devices)])  52.8 us
    pallas_call x20, Pallas kernels, call(): pl.pallas_call(kernel, out_shape=tuple(shapes), in_specs=specs, out_specs...  28.8 us
  transfers between devices with their start and end apart: 59, of which 21 were waited for; matrix products, arithmetic and copies ran while one was open for 0% of the time, Pallas kernels for 17%

profile of v6, /device:TPU:0, one launch (start us, length us, event | category | flops | bytes accessed | tf_op | source)
XLA Modules:
  0.0 157.9 jit_solution(804465867734555098)
XLA Ops:
  0.9 1.2 copy-done.10
  3.4 2.6 %collective-permute-start.1 = (bf16[144,512]{1,0:T(8,128)(2,1)S(1)}, bf16[144,512]{1,0:T(8,128)(2,1)S(1)}, u32[]{:S(2)}, u32[]{:S(2)}) collective-permute-start(bf16[144,512]{1,0:T(8,128)(2,1)S(1)} %get-tuple-element.63), channel_id=1, source_target_pairs={{0,2},{1,3},{2,0},{3,1},{4,6},{5,7},{6,4},{7,5},{8,10},{9,11},{10,... | collective-permute-start | bytes 442376 | tf_op jit(solution)/shard_map/ppermute | solution.py:319
  6.0 1.7 %collective-permute-start.3 = (bf16[16,512]{1,0:T(8,128)(2,1)S(1)}, bf16[16,512]{1,0:T(8,128)(2,1)S(1)}, u32[]{:S(2)}, u32[]{:S(2)}) collective-permute-start(bf16[16,512]{1,0:T(8,128)(2,1)S(1)} %get-tuple-element.65), channel_id=1, source_target_pairs={{0,4},{1,5},{2,6},{3,7},{4,8},{5,9},{6,10},{7,11},{8,12},{9,13},{1... | collective-permute-start | bytes 49160 | tf_op jit(solution)/shard_map/ppermute | solution.py:319
  7.7 4.8 %collective-permute-done.3.refs_4_ = bf16[16,512]{1,0:T(8,128)(2,1)S(1)} collective-permute-done((bf16[16,512]{1,0:T(8,128)(2,1)S(1)}, bf16[16,512]{1,0:T(8,128)(2,1)S(1)}, u32[]{:S(2)}, u32[]{:S(2)}) %collective-permute-start.3) | collective-permute-done | bytes 16416 | tf_op jit(solution)/shard_map/ppermute | solution.py:319
  12.5 1.7 %collective-permute-start.5 = (bf16[16,512]{1,0:T(8,128)(2,1)S(1)}, bf16[16,512]{1,0:T(8,128)(2,1)S(1)}, u32[]{:S(2)}, u32[]{:S(2)}) collective-permute-start(bf16[16,512]{1,0:T(8,128)(2,1)S(1)} %collective-permute-done.3.refs_4_), channel_id=1, source_target_pairs={{0,2},{1,3},{2,0},{3,1},{4,6},{5,7},{6,4},{7,5},{8,10},{9,11},{10,... | collective-permute-start | bytes 49160 | tf_op jit(solution)/shard_map/ppermute | solution.py:319
  16.2 1.1 collective-permute-done.6.refs_7_
  17.5 2.7 %shard_map.119 = (bf16[128,2048]{1,0:T(8,128)(2,1)S(1)}, bf16[64,2048]{1,0:T(8,128)(2,1)S(1)}, bf16[72,2048]{1,0:T(8,128)(2,1)S(1)}) custom-call(s32[5]{0:T(128)S(1)} %stack.23.where_ref, s32[4,128]{1,0:T(4,128)S(1)} %bitcast.29, f32[4,128]{1,0:T(4,128)S(1)} %bitcast.30, s32[4,128]{1,0:T(4,128)S(1)} %bitcast.32, f32[1,2048]{1,0:T(1,128)S(1)} %bitcast.27, ...), custom_call_target="tpu_custom_call" | custom-call | flops 1342177280 | bytes 11687956 | tf_op jit(solution)/shard_map/pallas_call | solution.py:163
  20.2 2.4 %collective-permute-start.16 = (bf16[64,2048]{1,0:T(8,128)(2,1)S(1)}, bf16[64,2048]{1,0:T(8,128)(2,1)S(1)}, u32[]{:S(2)}, u32[]{:S(2)}) collective-permute-start(bf16[64,2048]{1,0:T(8,128)(2,1)S(1)} %get-tuple-element.66.refs_0_), channel_id=1, source_target_pairs={{0,8},{1,9},{2,10},{3,11},{4,12},{5,13},{6,14},{7,15},{8,24},{9,25... | collective-permute-start | bytes 786440 | tf_op jit(solution)/shard_map/ppermute | solution.py:319
  22.6 8.4 %collective-permute-done.19.refs_1_ = bf16[72,2048]{1,0:T(8,128)(2,1)S(1)} collective-permute-done((bf16[72,2048]{1,0:T(8,128)(2,1)S(1)}, bf16[72,2048]{1,0:T(8,128)(2,1)S(1)}, u32[]{:S(2)}, u32[]{:S(2)}) %collective-permute-start.19) | collective-permute-done | bytes 294944 | tf_op jit(solution)/shard_map/ppermute | solution.py:319
  31.0 4.9 %collective-permute-done.16.refs_0_ = bf16[64,2048]{1,0:T(8,128)(2,1)S(1)} collective-permute-done((bf16[64,2048]{1,0:T(8,128)(2,1)S(1)}, bf16[64,2048]{1,0:T(8,128)(2,1)S(1)}, u32[]{:S(2)}, u32[]{:S(2)}) %collective-permute-start.16) | collective-permute-done | bytes 262176 | tf_op jit(solution)/shard_map/ppermute | solution.py:319
  35.9 2.4 %collective-permute-start.17 = (bf16[64,2048]{1,0:T(8,128)(2,1)S(1)}, bf16[64,2048]{1,0:T(8,128)(2,1)S(1)}, u32[]{:S(2)}, u32[]{:S(2)}) collective-permute-start(bf16[64,2048]{1,0:T(8,128)(2,1)S(1)} %collective-permute-done.16.refs_0_), channel_id=1, source_target_pairs={{0,8},{1,9},{2,10},{3,11},{4,12},{5,13},{6,14},{7,15},{8,24},{9,25... | collective-permute-start | bytes 786440 | tf_op jit(solution)/shard_map/ppermute | solution.py:319
  39.4 1.2 collective-permute-start.42
  41.2 1.8 %collective-permute-start.44 = (bf16[48,2048]{1,0:T(8,128)(2,1)S(1)}, bf16[48,2048]{1,0:T(8,128)(2,1)S(1)}, u32[]{:S(2)}, u32[]{:S(2)}) collective-permute-start(bf16[48,2048]{1,0:T(8,128)(2,1)S(1)} %get-tuple-element.106), channel_id=1, source_target_pairs={{0,6},{1,7},{2,4},{3,5},{4,2},{5,3},{6,0},{7,1},{8,14},{9,15},{10,... | collective-permute-start | bytes 589832 | tf_op jit(solution)/shard_map/ppermute | solution.py:319
  42.9 8.9 %collective-permute-done.17.refs_0_ = bf16[64,2048]{1,0:T(8,128)(2,1)S(1)} collective-permute-done((bf16[64,2048]{1,0:T(8,128)(2,1)S(1)}, bf16[64,2048]{1,0:T(8,128)(2,1)S(1)}, u32[]{:S(2)}, u32[]{:S(2)}) %collective-permute-start.17) | collective-permute-done | bytes 262176 | tf_op jit(solution)/shard_map/ppermute | solution.py:319
  52.4 2.0 %collective-permute-start.21 = (bf16[72,2048]{1,0:T(8,128)(2,1)S(1)}, bf16[72,2048]{1,0:T(8,128)(2,1)S(1)}, u32[]{:S(2)}, u32[]{:S(2)}) collective-permute-start(bf16[72,2048]{1,0:T(8,128)(2,1)S(1)} %collective-permute-done.20.refs_1_), channel_id=1, source_target_pairs={{0,8},{1,9},{2,10},{3,11},{4,12},{5,13},{6,14},{7,15},{8,24},{9,25... | collective-permute-start | bytes 884744 | tf_op jit(solution)/shard_map/ppermute | solution.py:319
  54.5 3.3 %shard_map.130 = (bf16[48,2048]{1,0:T(8,128)(2,1)S(1)}, bf16[48,2048]{1,0:T(8,128)(2,1)S(1)}, bf16[48,2048]{1,0:T(8,128)(2,1)S(1)}, bf16[48,2048]{1,0:T(8,128)(2,1)S(1)}) custom-call(s32[5]{0:T(128)S(1)} %stack.23.where_ref, bf16[48,2048]{1,0:T(8,128)(2,1)S(1)} %get-tuple-element.103.refs_0_, bf16[48,2048]{1,0:T(8,128)(2,1)S(1)} %collective-permute-done.42.refs_1_, ...), custom_call_target="tpu_custom_call" | custom-call | flops 2415919104 | bytes 13369364 | tf_op jit(solution)/shard_map/pallas_call | solution.py:163
  57.8 1.2 collective-permute-start.45
  59.6 1.8 %collective-permute-start.47 = (bf16[48,2048]{1,0:T(8,128)(2,1)S(1)}, bf16[48,2048]{1,0:T(8,128)(2,1)S(1)}, u32[]{:S(2)}, u32[]{:S(2)}) collective-permute-start(bf16[48,2048]{1,0:T(8,128)(2,1)S(1)} %get-tuple-element.110), channel_id=1, source_target_pairs={{0,6},{1,7},{2,4},{3,5},{4,2},{5,3},{6,0},{7,1},{8,14},{9,15},{10,... | collective-permute-start | bytes 589832 | tf_op jit(solution)/shard_map/ppermute | solution.py:319
  61.3 1.1 shard_map.126
  62.5 1.2 collective-permute-start.33
  63.7 4.1 %collective-permute-done.21.refs_1_ = bf16[72,2048]{1,0:T(8,128)(2,1)S(1)} collective-permute-done((bf16[72,2048]{1,0:T(8,128)(2,1)S(1)}, bf16[72,2048]{1,0:T(8,128)(2,1)S(1)}, u32[]{:S(2)}, u32[]{:S(2)}) %collective-permute-start.21) | collective-permute-done | bytes 294944 | tf_op jit(solution)/shard_map/ppermute | solution.py:319
  67.8 2.6 %collective-permute-start.35 = (bf16[48,2048]{1,0:T(8,128)(2,1)S(1)}, bf16[48,2048]{1,0:T(8,128)(2,1)S(1)}, u32[]{:S(2)}, u32[]{:S(2)}) collective-permute-start(bf16[48,2048]{1,0:T(8,128)(2,1)S(1)} %get-tuple-element.95), channel_id=1, source_target_pairs={{0,6},{1,7},{2,4},{3,5},{4,2},{5,3},{6,0},{7,1},{8,14},{9,15},{10,... | collective-permute-start | bytes 589832 | tf_op jit(solution)/shard_map/ppermute | solution.py:319
  70.9 2.2 %collective-permute-done.33.refs_1_ = bf16[48,2048]{1,0:T(8,128)(2,1)S(1)} collective-permute-done((bf16[48,2048]{1,0:T(8,128)(2,1)S(1)}, bf16[48,2048]{1,0:T(8,128)(2,1)S(1)}, u32[]{:S(2)}, u32[]{:S(2)}) %collective-permute-start.33) | collective-permute-done | bytes 196640 | tf_op jit(solution)/shard_map/ppermute | solution.py:319
  74.1 1.4 collective-permute-done.34.refs_2_
  75.5 3.4 %collective-permute-done.35.refs_3_ = bf16[48,2048]{1,0:T(8,128)(2,1)S(1)} collective-permute-done((bf16[48,2048]{1,0:T(8,128)(2,1)S(1)}, bf16[48,2048]{1,0:T(8,128)(2,1)S(1)}, u32[]{:S(2)}, u32[]{:S(2)}) %collective-permute-start.35) | collective-permute-done | bytes 196640 | tf_op jit(solution)/shard_map/ppermute | solution.py:319
  79.0 3.3 %shard_map.127 = (bf16[48,2048]{1,0:T(8,128)(2,1)S(1)}, bf16[48,2048]{1,0:T(8,128)(2,1)S(1)}, bf16[48,2048]{1,0:T(8,128)(2,1)S(1)}, bf16[48,2048]{1,0:T(8,128)(2,1)S(1)}) custom-call(s32[5]{0:T(128)S(1)} %stack.23.where_ref, bf16[48,2048]{1,0:T(8,128)(2,1)S(1)} %get-tuple-element.92.refs_0_, bf16[48,2048]{1,0:T(8,128)(2,1)S(1)} %collective-permute-done.33.refs_1_, ...), custom_call_target="tpu_custom_call" | custom-call | flops 2415919104 | bytes 13369364 | tf_op jit(solution)/shard_map/pallas_call | solution.py:163
  83.6 2.2 %collective-permute-start.38 = (bf16[48,2048]{1,0:T(8,128)(2,1)S(1)}, bf16[48,2048]{1,0:T(8,128)(2,1)S(1)}, u32[]{:S(2)}, u32[]{:S(2)}) collective-permute-start(bf16[48,2048]{1,0:T(8,128)(2,1)S(1)} %get-tuple-element.99), channel_id=1, source_target_pairs={{0,6},{1,7},{2,4},{3,5},{4,2},{5,3},{6,0},{7,1},{8,14},{9,15},{10,... | collective-permute-start | bytes 589832 | tf_op jit(solution)/shard_map/ppermute | solution.py:319
  87.5 1.9 %collective-permute-done.36.refs_1_ = bf16[48,2048]{1,0:T(8,128)(2,1)S(1)} collective-permute-done((bf16[48,2048]{1,0:T(8,128)(2,1)S(1)}, bf16[48,2048]{1,0:T(8,128)(2,1)S(1)}, u32[]{:S(2)}, u32[]{:S(2)}) %collective-permute-start.36) | collective-permute-done | bytes 196640 | tf_op jit(solution)/shard_map/ppermute | solution.py:319
  91.4 3.9 %collective-permute-done.38.refs_3_ = bf16[48,2048]{1,0:T(8,128)(2,1)S(1)} collective-permute-done((bf16[48,2048]{1,0:T(8,128)(2,1)S(1)}, bf16[48,2048]{1,0:T(8,128)(2,1)S(1)}, u32[]{:S(2)}, u32[]{:S(2)}) %collective-permute-start.38) | collective-permute-done | bytes 196640 | tf_op jit(solution)/shard_map/ppermute | solution.py:319
  95.3 1.2 collective-permute-start.26
  100.3 1.5 collective-permute-start.10
  103.8 3.3 %shard_map.124 = (bf16[48,2048]{1,0:T(8,128)(2,1)S(1)}, bf16[48,2048]{1,0:T(8,128)(2,1)S(1)}, bf16[48,2048]{1,0:T(8,128)(2,1)S(1)}, bf16[48,2048]{1,0:T(8,128)(2,1)S(1)}) custom-call(s32[5]{0:T(128)S(1)} %stack.23.where_ref, bf16[48,2048]{1,0:T(8,128)(2,1)S(1)} %get-tuple-element.81.refs_0_, bf16[48,2048]{1,0:T(8,128)(2,1)S(1)} %collective-permute-done.24.refs_1_, ...), custom_call_target="tpu_custom_call" | custom-call | flops 2415919104 | bytes 13369364 | tf_op jit(solution)/shard_map/pallas_call | solution.py:163
  108.1 1.8 %collective-permute-start.49 = (bf16[64,2048]{1,0:T(8,128)(2,1)S(1)}, bf16[64,2048]{1,0:T(8,128)(2,1)S(1)}, u32[]{:S(2)}, u32[]{:S(2)}) collective-permute-start(bf16[64,2048]{1,0:T(8,128)(2,1)S(1)} %shard_map.132), channel_id=1, source_target_pairs={{0,8},{1,9},{2,10},{3,11},{4,12},{5,13},{6,14},{7,15},{8,24},{9,25... | collective-permute-start | bytes 786440 | tf_op jit(solution)/shard_map/ppermute | solution.py:319
  109.9 2.5 %collective-permute-done.11.refs_3_ = bf16[48,2048]{1,0:T(8,128)(2,1)S(1)} collective-permute-done((bf16[48,2048]{1,0:T(8,128)(2,1)S(1)}, bf16[48,2048]{1,0:T(8,128)(2,1)S(1)}, u32[]{:S(2)}, u32[]{:S(2)}) %collective-permute-start.11) | collective-permute-done | bytes 196640 | tf_op jit(solution)/shard_map/ppermute | solution.py:319
  112.3 1.4 collective-permute-done.9.refs_1_
  114.8 1.4 collective-permute-start.28
  117.2 3.3 %shard_map.121 = (bf16[48,2048]{1,0:T(8,128)(2,1)S(1)}, bf16[48,2048]{1,0:T(8,128)(2,1)S(1)}, bf16[48,2048]{1,0:T(8,128)(2,1)S(1)}, bf16[48,2048]{1,0:T(8,128)(2,1)S(1)}) custom-call(s32[5]{0:T(128)S(1)} %stack.23.where_ref, bf16[48,2048]{1,0:T(8,128)(2,1)S(1)} %get-tuple-element.69.refs_0_, bf16[48,2048]{1,0:T(8,128)(2,1)S(1)} %collective-permute-done.9.refs_1_, ...), custom_call_target="tpu_custom_call" | custom-call | flops 2415919104 | bytes 13369364 | tf_op jit(solution)/shard_map/pallas_call | solution.py:163
  120.5 1.1 collective-permute-start.12
  122.6 1.4 collective-permute-start.13
  124.6 2.6 %collective-permute-done.29.refs_3_ = bf16[48,2048]{1,0:T(8,128)(2,1)S(1)} collective-permute-done((bf16[48,2048]{1,0:T(8,128)(2,1)S(1)}, bf16[48,2048]{1,0:T(8,128)(2,1)S(1)}, u32[]{:S(2)}, u32[]{:S(2)}) %collective-permute-start.29) | collective-permute-done | bytes 196640 | tf_op jit(solution)/shard_map/ppermute | solution.py:319
  127.1 2.0 %collective-permute-start.57 = (bf16[64,2048]{1,0:T(8,128)(2,1)S(1)}, bf16[64,2048]{1,0:T(8,128)(2,1)S(1)}, u32[]{:S(2)}, u32[]{:S(2)}) collective-permute-start(bf16[64,2048]{1,0:T(8,128)(2,1)S(1)} %shard_map.136), channel_id=1, source_target_pairs={{0,8},{1,9},{2,10},{3,11},{4,12},{5,13},{6,14},{7,15},{8,24},{9,25... | collective-permute-start | bytes 786440 | tf_op jit(solution)/shard_map/ppermute | solution.py:319
  131.5 2.2 %collective-permute-start.14 = (bf16[48,2048]{1,0:T(8,128)(2,1)S(1)}, bf16[48,2048]{1,0:T(8,128)(2,1)S(1)}, u32[]{:S(2)}, u32[]{:S(2)}) collective-permute-start(bf16[48,2048]{1,0:T(8,128)(2,1)S(1)} %get-tuple-element.76), channel_id=1, source_target_pairs={{0,6},{1,7},{2,4},{3,5},{4,2},{5,3},{6,0},{7,1},{8,14},{9,15},{10,... | collective-permute-start | bytes 589832 | tf_op jit(solution)/shard_map/ppermute | solution.py:319
  133.7 5.8 %collective-permute-done.14.refs_3_ = bf16[48,2048]{1,0:T(8,128)(2,1)S(1)} collective-permute-done((bf16[48,2048]{1,0:T(8,128)(2,1)S(1)}, bf16[48,2048]{1,0:T(8,128)(2,1)S(1)}, u32[]{:S(2)}, u32[]{:S(2)}) %collective-permute-start.14) | collective-permute-done | bytes 196640 | tf_op jit(solution)/shard_map/ppermute | solution.py:319
  141.3 2.4 %collective-permute-start.58 = (bf16[64,2048]{1,0:T(8,128)(2,1)S(1)}, bf16[64,2048]{1,0:T(8,128)(2,1)S(1)}, u32[]{:S(2)}, u32[]{:S(2)}) collective-permute-start(bf16[64,2048]{1,0:T(8,128)(2,1)S(1)} %shard_map.137), channel_id=1, source_target_pairs={{0,8},{1,9},{2,10},{3,11},{4,12},{5,13},{6,14},{7,15},{8,24},{9,25... | collective-permute-start | bytes 786440 | tf_op jit(solution)/shard_map/ppermute | solution.py:319
  144.9 6.4 %collective-permute-done.58.refs_1_ = bf16[64,2048]{1,0:T(8,128)(2,1)S(1)} collective-permute-done((bf16[64,2048]{1,0:T(8,128)(2,1)S(1)}, bf16[64,2048]{1,0:T(8,128)(2,1)S(1)}, u32[]{:S(2)}, u32[]{:S(2)}) %collective-permute-start.58) | collective-permute-done | bytes 262176 | tf_op jit(solution)/shard_map/ppermute | solution.py:319
  151.4 1.4 final.2.refs_2_
  152.8 3.8 %collective-permute-done.51.refs_1_ = bf16[64,2048]{1,0:T(8,128)(2,1)S(1)} collective-permute-done((bf16[64,2048]{1,0:T(8,128)(2,1)S(1)}, bf16[64,2048]{1,0:T(8,128)(2,1)S(1)}, u32[]{:S(2)}, u32[]{:S(2)}) %collective-permute-start.51) | collective-permute-done | bytes 262176 | tf_op jit(solution)/shard_map/ppermute | solution.py:319
  156.5 1.4 final.3
  (120 shorter events, 29.5 us)
Async XLA Ops:
  2.8 14.5 %collective-permute-start = (bf16[144,512]{1,0:T(8,128)(2,1)S(1)}, bf16[144,512]{1,0:T(8,128)(2,1)S(1)}, u32[]{:S(2)}, u32[]{:S(2)}) collective-permute-start(bf16[144,512]{1,0:T(8,128)(2,1)S(1)} %get-tuple-element.62), channel_id=1, source_target_pairs={{0,1},{1,0},{2,3},{3,2},{4,5},{5,4},{6,7},{7,6},{8,9},{9,8},{10,11... | collective-permute-start | bytes 442376 | tf_op jit(solution)/shard_map/ppermute | solution.py:319
  3.4 14.0 %collective-permute-start.1 = (bf16[144,512]{1,0:T(8,128)(2,1)S(1)}, bf16[144,512]{1,0:T(8,128)(2,1)S(1)}, u32[]{:S(2)}, u32[]{:S(2)}) collective-permute-start(bf16[144,512]{1,0:T(8,128)(2,1)S(1)} %get-tuple-element.63), channel_id=1, source_target_pairs={{0,2},{1,3},{2,0},{3,1},{4,6},{5,7},{6,4},{7,5},{8,10},{9,11},{10,... | collective-permute-start | bytes 442376 | tf_op jit(solution)/shard_map/ppermute | solution.py:319
  6.0 11.4 %collective-permute-start.2 = (bf16[144,512]{1,0:T(8,128)(2,1)S(1)}, bf16[144,512]{1,0:T(8,128)(2,1)S(1)}, u32[]{:S(2)}, u32[]{:S(2)}) collective-permute-start(bf16[144,512]{1,0:T(8,128)(2,1)S(1)} %get-tuple-element.64), channel_id=1, source_target_pairs={{0,3},{1,2},{2,1},{3,0},{4,7},{5,6},{6,5},{7,4},{8,11},{9,10},{10,... | collective-permute-start | bytes 442376 | tf_op jit(solution)/shard_map/ppermute | solution.py:319
  20.2 10.8 %collective-permute-start.19 = (bf16[72,2048]{1,0:T(8,128)(2,1)S(1)}, bf16[72,2048]{1,0:T(8,128)(2,1)S(1)}, u32[]{:S(2)}, u32[]{:S(2)}) collective-permute-start(bf16[72,2048]{1,0:T(8,128)(2,1)S(1)} %get-tuple-element.67.refs_1_), channel_id=1, source_target_pairs={{0,8},{1,9},{2,10},{3,11},{4,12},{5,13},{6,14},{7,15},{8,24},{9,25... | collective-permute-start | bytes 884744 | tf_op jit(solution)/shard_map/ppermute | solution.py:319
  20.2 15.6 %collective-permute-start.16 = (bf16[64,2048]{1,0:T(8,128)(2,1)S(1)}, bf16[64,2048]{1,0:T(8,128)(2,1)S(1)}, u32[]{:S(2)}, u32[]{:S(2)}) collective-permute-start(bf16[64,2048]{1,0:T(8,128)(2,1)S(1)} %get-tuple-element.66.refs_0_), channel_id=1, source_target_pairs={{0,8},{1,9},{2,10},{3,11},{4,12},{5,13},{6,14},{7,15},{8,24},{9,25... | collective-permute-start | bytes 786440 | tf_op jit(solution)/shard_map/ppermute | solution.py:319
  35.9 15.9 %collective-permute-start.20 = (bf16[72,2048]{1,0:T(8,128)(2,1)S(1)}, bf16[72,2048]{1,0:T(8,128)(2,1)S(1)}, u32[]{:S(2)}, u32[]{:S(2)}) collective-permute-start(bf16[72,2048]{1,0:T(8,128)(2,1)S(1)} %collective-permute-done.19.refs_1_), channel_id=1, source_target_pairs={{0,8},{1,9},{2,10},{3,11},{4,12},{5,13},{6,14},{7,15},{8,24},{9,25... | collective-permute-start | bytes 884744 | tf_op jit(solution)/shard_map/ppermute | solution.py:319
  35.9 15.9 %collective-permute-start.17 = (bf16[64,2048]{1,0:T(8,128)(2,1)S(1)}, bf16[64,2048]{1,0:T(8,128)(2,1)S(1)}, u32[]{:S(2)}, u32[]{:S(2)}) collective-permute-start(bf16[64,2048]{1,0:T(8,128)(2,1)S(1)} %collective-permute-done.16.refs_0_), channel_id=1, source_target_pairs={{0,8},{1,9},{2,10},{3,11},{4,12},{5,13},{6,14},{7,15},{8,24},{9,25... | collective-permute-start | bytes 786440 | tf_op jit(solution)/shard_map/ppermute | solution.py:319
  39.4 12.5 %collective-permute-start.42 = (bf16[48,2048]{1,0:T(8,128)(2,1)S(1)}, bf16[48,2048]{1,0:T(8,128)(2,1)S(1)}, u32[]{:S(2)}, u32[]{:S(2)}) collective-permute-start(bf16[48,2048]{1,0:T(8,128)(2,1)S(1)} %get-tuple-element.104), channel_id=1, source_target_pairs={{0,2},{1,3},{2,0},{3,1},{4,6},{5,7},{6,4},{7,5},{8,10},{9,11},{10,... | collective-permute-start | bytes 589832 | tf_op jit(solution)/shard_map/ppermute | solution.py:319
  40.6 11.8 %collective-permute-start.43 = (bf16[48,2048]{1,0:T(8,128)(2,1)S(1)}, bf16[48,2048]{1,0:T(8,128)(2,1)S(1)}, u32[]{:S(2)}, u32[]{:S(2)}) collective-permute-start(bf16[48,2048]{1,0:T(8,128)(2,1)S(1)} %get-tuple-element.105), channel_id=1, source_target_pairs={{0,4},{1,5},{2,6},{3,7},{4,0},{5,1},{6,2},{7,3},{8,12},{9,13},{10,... | collective-permute-start | bytes 589832 | tf_op jit(solution)/shard_map/ppermute | solution.py:319
  41.2 13.3 %collective-permute-start.44 = (bf16[48,2048]{1,0:T(8,128)(2,1)S(1)}, bf16[48,2048]{1,0:T(8,128)(2,1)S(1)}, u32[]{:S(2)}, u32[]{:S(2)}) collective-permute-start(bf16[48,2048]{1,0:T(8,128)(2,1)S(1)} %get-tuple-element.106), channel_id=1, source_target_pairs={{0,6},{1,7},{2,4},{3,5},{4,2},{5,3},{6,0},{7,1},{8,14},{9,15},{10,... | collective-permute-start | bytes 589832 | tf_op jit(solution)/shard_map/ppermute | solution.py:319
  51.8 10.7 %collective-permute-start.18 = (bf16[64,2048]{1,0:T(8,128)(2,1)S(1)}, bf16[64,2048]{1,0:T(8,128)(2,1)S(1)}, u32[]{:S(2)}, u32[]{:S(2)}) collective-permute-start(bf16[64,2048]{1,0:T(8,128)(2,1)S(1)} %collective-permute-done.17.refs_0_), channel_id=1, source_target_pairs={{0,8},{1,9},{2,10},{3,11},{4,12},{5,13},{6,14},{7,15},{8,24},{9,25... | collective-permute-start | bytes 786440 | tf_op jit(solution)/shard_map/ppermute | solution.py:319
  51.8 7.7 %collective-permute-start.32 = (bf16[72,2048]{1,0:T(8,128)(2,1)S(1)}, bf16[72,2048]{1,0:T(8,128)(2,1)S(1)}, u32[]{:S(2)}, u32[]{:S(2)}) collective-permute-start(bf16[72,2048]{1,0:T(8,128)(2,1)S(1)} %collective-permute-done.20.refs_1_), channel_id=1, source_target_pairs={{0,1},{1,0},{2,3},{3,2},{4,5},{5,4},{6,7},{7,6},{8,9},{9,8},{10,11... | collective-permute-start | bytes 884744 | tf_op jit(solution)/shard_map/ppermute | solution.py:319
  52.4 15.4 %collective-permute-start.21 = (bf16[72,2048]{1,0:T(8,128)(2,1)S(1)}, bf16[72,2048]{1,0:T(8,128)(2,1)S(1)}, u32[]{:S(2)}, u32[]{:S(2)}) collective-permute-start(bf16[72,2048]{1,0:T(8,128)(2,1)S(1)} %collective-permute-done.20.refs_1_), channel_id=1, source_target_pairs={{0,8},{1,9},{2,10},{3,11},{4,12},{5,13},{6,14},{7,15},{8,24},{9,25... | collective-permute-start | bytes 884744 | tf_op jit(solution)/shard_map/ppermute | solution.py:319
  57.8 10.0 %collective-permute-start.45 = (bf16[48,2048]{1,0:T(8,128)(2,1)S(1)}, bf16[48,2048]{1,0:T(8,128)(2,1)S(1)}, u32[]{:S(2)}, u32[]{:S(2)}) collective-permute-start(bf16[48,2048]{1,0:T(8,128)(2,1)S(1)} %get-tuple-element.108), channel_id=1, source_target_pairs={{0,2},{1,3},{2,0},{3,1},{4,6},{5,7},{6,4},{7,5},{8,10},{9,11},{10,... | collective-permute-start | bytes 589832 | tf_op jit(solution)/shard_map/ppermute | solution.py:319
  59.0 11.4 %collective-permute-start.46 = (bf16[48,2048]{1,0:T(8,128)(2,1)S(1)}, bf16[48,2048]{1,0:T(8,128)(2,1)S(1)}, u32[]{:S(2)}, u32[]{:S(2)}) collective-permute-start(bf16[48,2048]{1,0:T(8,128)(2,1)S(1)} %get-tuple-element.109), channel_id=1, source_target_pairs={{0,4},{1,5},{2,6},{3,7},{4,0},{5,1},{6,2},{7,3},{8,12},{9,13},{10,... | collective-permute-start | bytes 589832 | tf_op jit(solution)/shard_map/ppermute | solution.py:319
  59.6 10.8 %collective-permute-start.47 = (bf16[48,2048]{1,0:T(8,128)(2,1)S(1)}, bf16[48,2048]{1,0:T(8,128)(2,1)S(1)}, u32[]{:S(2)}, u32[]{:S(2)}) collective-permute-start(bf16[48,2048]{1,0:T(8,128)(2,1)S(1)} %get-tuple-element.110), channel_id=1, source_target_pairs={{0,6},{1,7},{2,4},{3,5},{4,2},{5,3},{6,0},{7,1},{8,14},{9,15},{10,... | collective-permute-start | bytes 589832 | tf_op jit(solution)/shard_map/ppermute | solution.py:319
  62.5 10.6 %collective-permute-start.33 = (bf16[48,2048]{1,0:T(8,128)(2,1)S(1)}, bf16[48,2048]{1,0:T(8,128)(2,1)S(1)}, u32[]{:S(2)}, u32[]{:S(2)}) collective-permute-start(bf16[48,2048]{1,0:T(8,128)(2,1)S(1)} %get-tuple-element.93), channel_id=1, source_target_pairs={{0,2},{1,3},{2,0},{3,1},{4,6},{5,7},{6,4},{7,5},{8,10},{9,11},{10,... | collective-permute-start | bytes 589832 | tf_op jit(solution)/shard_map/ppermute | solution.py:319
  67.8 7.8 %collective-permute-start.34 = (bf16[48,2048]{1,0:T(8,128)(2,1)S(1)}, bf16[48,2048]{1,0:T(8,128)(2,1)S(1)}, u32[]{:S(2)}, u32[]{:S(2)}) collective-permute-start(bf16[48,2048]{1,0:T(8,128)(2,1)S(1)} %get-tuple-element.94), channel_id=1, source_target_pairs={{0,4},{1,5},{2,6},{3,7},{4,0},{5,1},{6,2},{7,3},{8,12},{9,13},{10,... | collective-permute-start | bytes 589832 | tf_op jit(solution)/shard_map/ppermute | solution.py:319
  67.8 11.2 %collective-permute-start.35 = (bf16[48,2048]{1,0:T(8,128)(2,1)S(1)}, bf16[48,2048]{1,0:T(8,128)(2,1)S(1)}, u32[]{:S(2)}, u32[]{:S(2)}) collective-permute-start(bf16[48,2048]{1,0:T(8,128)(2,1)S(1)} %get-tuple-element.95), channel_id=1, source_target_pairs={{0,6},{1,7},{2,4},{3,5},{4,2},{5,3},{6,0},{7,1},{8,14},{9,15},{10,... | collective-permute-start | bytes 589832 | tf_op jit(solution)/shard_map/ppermute | solution.py:319
  70.3 12.9 %collective-permute-start.7 = (bf16[64,2048]{1,0:T(8,128)(2,1)S(1)}, bf16[64,2048]{1,0:T(8,128)(2,1)S(1)}, u32[]{:S(2)}, u32[]{:S(2)}) collective-permute-start(bf16[64,2048]{1,0:T(8,128)(2,1)S(1)} %get-tuple-element.66.refs_0_), channel_id=1, source_target_pairs={{0,1},{1,0},{2,3},{3,2},{4,5},{5,4},{6,7},{7,6},{8,9},{9,8},{10,11... | collective-permute-start | bytes 786440 | tf_op jit(solution)/shard_map/ppermute | solution.py:319
  70.3 13.3 %collective-permute-start.22 = (bf16[64,2048]{1,0:T(8,128)(2,1)S(1)}, bf16[64,2048]{1,0:T(8,128)(2,1)S(1)}, u32[]{:S(2)}, u32[]{:S(2)}) collective-permute-start(bf16[64,2048]{1,0:T(8,128)(2,1)S(1)} %collective-permute-done.18.refs_0_), channel_id=1, source_target_pairs={{0,1},{1,0},{2,3},{3,2},{4,5},{5,4},{6,7},{7,6},{8,9},{9,8},{10,11... | collective-permute-start | bytes 786440 | tf_op jit(solution)/shard_map/ppermute | solution.py:319
  73.1 12.8 %collective-permute-start.23 = (bf16[72,2048]{1,0:T(8,128)(2,1)S(1)}, bf16[72,2048]{1,0:T(8,128)(2,1)S(1)}, u32[]{:S(2)}, u32[]{:S(2)}) collective-permute-start(bf16[72,2048]{1,0:T(8,128)(2,1)S(1)} %collective-permute-done.21.refs_1_), channel_id=1, source_target_pairs={{0,1},{1,0},{2,3},{3,2},{4,5},{5,4},{6,7},{7,6},{8,9},{9,8},{10,11... | collective-permute-start | bytes 884744 | tf_op jit(solution)/shard_map/ppermute | solution.py:319
  75.5 10.3 %collective-permute-start.55 = (bf16[64,2048]{1,0:T(8,128)(2,1)S(1)}, bf16[64,2048]{1,0:T(8,128)(2,1)S(1)}, u32[]{:S(2)}, u32[]{:S(2)}) collective-permute-start(bf16[64,2048]{1,0:T(8,128)(2,1)S(1)} %get-tuple-element.116), channel_id=1, source_target_pairs={{0,1},{1,0},{2,3},{3,2},{4,5},{5,4},{6,7},{7,6},{8,9},{9,8},{10,11... | collective-permute-start | bytes 786440 | tf_op jit(solution)/shard_map/ppermute | solution.py:319
  83.3 7.4 %collective-permute-start.37 = (bf16[48,2048]{1,0:T(8,128)(2,1)S(1)}, bf16[48,2048]{1,0:T(8,128)(2,1)S(1)}, u32[]{:S(2)}, u32[]{:S(2)}) collective-permute-start(bf16[48,2048]{1,0:T(8,128)(2,1)S(1)} %get-tuple-element.98), channel_id=1, source_target_pairs={{0,4},{1,5},{2,6},{3,7},{4,0},{5,1},{6,2},{7,3},{8,12},{9,13},{10,... | collective-permute-start | bytes 589832 | tf_op jit(solution)/shard_map/ppermute | solution.py:319
  83.6 11.7 %collective-permute-start.38 = (bf16[48,2048]{1,0:T(8,128)(2,1)S(1)}, bf16[48,2048]{1,0:T(8,128)(2,1)S(1)}, u32[]{:S(2)}, u32[]{:S(2)}) collective-permute-start(bf16[48,2048]{1,0:T(8,128)(2,1)S(1)} %get-tuple-element.99), channel_id=1, source_target_pairs={{0,6},{1,7},{2,4},{3,5},{4,2},{5,3},{6,0},{7,1},{8,14},{9,15},{10,... | collective-permute-start | bytes 589832 | tf_op jit(solution)/shard_map/ppermute | solution.py:319
  85.9 12.2 %collective-permute-start.8 = (bf16[72,2048]{1,0:T(8,128)(2,1)S(1)}, bf16[72,2048]{1,0:T(8,128)(2,1)S(1)}, u32[]{:S(2)}, u32[]{:S(2)}) collective-permute-start(bf16[72,2048]{1,0:T(8,128)(2,1)S(1)} %get-tuple-element.67.refs_1_), channel_id=1, source_target_pairs={{0,1},{1,0},{2,3},{3,2},{4,5},{5,4},{6,7},{7,6},{8,9},{9,8},{10,11... | collective-permute-start | bytes 884744 | tf_op jit(solution)/shard_map/ppermute | solution.py:319
  85.9 12.6 %collective-permute-start.48 = (bf16[64,2048]{1,0:T(8,128)(2,1)S(1)}, bf16[64,2048]{1,0:T(8,128)(2,1)S(1)}, u32[]{:S(2)}, u32[]{:S(2)}) collective-permute-start(bf16[64,2048]{1,0:T(8,128)(2,1)S(1)} %get-tuple-element.112), channel_id=1, source_target_pairs={{0,1},{1,0},{2,3},{3,2},{4,5},{5,4},{6,7},{7,6},{8,9},{9,8},{10,11... | collective-permute-start | bytes 786440 | tf_op jit(solution)/shard_map/ppermute | solution.py:319
  89.4 10.9 %collective-permute-start.24 = (bf16[48,2048]{1,0:T(8,128)(2,1)S(1)}, bf16[48,2048]{1,0:T(8,128)(2,1)S(1)}, u32[]{:S(2)}, u32[]{:S(2)}) collective-permute-start(bf16[48,2048]{1,0:T(8,128)(2,1)S(1)} %get-tuple-element.82), channel_id=1, source_target_pairs={{0,2},{1,3},{2,0},{3,1},{4,6},{5,7},{6,4},{7,5},{8,10},{9,11},{10,... | collective-permute-start | bytes 589832 | tf_op jit(solution)/shard_map/ppermute | solution.py:319
  90.7 11.0 %collective-permute-start.25 = (bf16[48,2048]{1,0:T(8,128)(2,1)S(1)}, bf16[48,2048]{1,0:T(8,128)(2,1)S(1)}, u32[]{:S(2)}, u32[]{:S(2)}) collective-permute-start(bf16[48,2048]{1,0:T(8,128)(2,1)S(1)} %get-tuple-element.83), channel_id=1, source_target_pairs={{0,4},{1,5},{2,6},{3,7},{4,0},{5,1},{6,2},{7,3},{8,12},{9,13},{10,... | collective-permute-start | bytes 589832 | tf_op jit(solution)/shard_map/ppermute | solution.py:319
  98.1 16.7 %collective-permute-start.56 = (bf16[64,2048]{1,0:T(8,128)(2,1)S(1)}, bf16[64,2048]{1,0:T(8,128)(2,1)S(1)}, u32[]{:S(2)}, u32[]{:S(2)}) collective-permute-start(bf16[64,2048]{1,0:T(8,128)(2,1)S(1)} %shard_map.135), channel_id=1, source_target_pairs={{0,8},{1,9},{2,10},{3,11},{4,12},{5,13},{6,14},{7,15},{8,24},{9,25... | collective-permute-start | bytes 786440 | tf_op jit(solution)/shard_map/ppermute | solution.py:319
  98.5 17.7 %collective-permute-start.54 = (bf16[64,2048]{1,0:T(8,128)(2,1)S(1)}, bf16[64,2048]{1,0:T(8,128)(2,1)S(1)}, u32[]{:S(2)}, u32[]{:S(2)}) collective-permute-start(bf16[64,2048]{1,0:T(8,128)(2,1)S(1)} %get-tuple-element.115), channel_id=1, source_target_pairs={{0,1},{1,0},{2,3},{3,2},{4,5},{5,4},{6,7},{7,6},{8,9},{9,8},{10,11... | collective-permute-start | bytes 786440 | tf_op jit(solution)/shard_map/ppermute | solution.py:319
  100.3 7.8 %collective-permute-start.10 = (bf16[48,2048]{1,0:T(8,128)(2,1)S(1)}, bf16[48,2048]{1,0:T(8,128)(2,1)S(1)}, u32[]{:S(2)}, u32[]{:S(2)}) collective-permute-start(bf16[48,2048]{1,0:T(8,128)(2,1)S(1)} %get-tuple-element.71), channel_id=1, source_target_pairs={{0,4},{1,5},{2,6},{3,7},{4,0},{5,1},{6,2},{7,3},{8,12},{9,13},{10,... | collective-permute-start | bytes 589832 | tf_op jit(solution)/shard_map/ppermute | solution.py:319
  101.7 10.6 %collective-permute-start.11 = (bf16[48,2048]{1,0:T(8,128)(2,1)S(1)}, bf16[48,2048]{1,0:T(8,128)(2,1)S(1)}, u32[]{:S(2)}, u32[]{:S(2)}) collective-permute-start(bf16[48,2048]{1,0:T(8,128)(2,1)S(1)} %get-tuple-element.72), channel_id=1, source_target_pairs={{0,6},{1,7},{2,4},{3,5},{4,2},{5,3},{6,0},{7,1},{8,14},{9,15},{10,... | collective-permute-start | bytes 589832 | tf_op jit(solution)/shard_map/ppermute | solution.py:319
  102.7 11.0 %collective-permute-start.9 = (bf16[48,2048]{1,0:T(8,128)(2,1)S(1)}, bf16[48,2048]{1,0:T(8,128)(2,1)S(1)}, u32[]{:S(2)}, u32[]{:S(2)}) collective-permute-start(bf16[48,2048]{1,0:T(8,128)(2,1)S(1)} %get-tuple-element.70), channel_id=1, source_target_pairs={{0,2},{1,3},{2,0},{3,1},{4,6},{5,7},{6,4},{7,5},{8,10},{9,11},{10,... | collective-permute-start | bytes 589832 | tf_op jit(solution)/shard_map/ppermute | solution.py:319
  108.1 22.0 %collective-permute-start.49 = (bf16[64,2048]{1,0:T(8,128)(2,1)S(1)}, bf16[64,2048]{1,0:T(8,128)(2,1)S(1)}, u32[]{:S(2)}, u32[]{:S(2)}) collective-permute-start(bf16[64,2048]{1,0:T(8,128)(2,1)S(1)} %shard_map.132), channel_id=1, source_target_pairs={{0,8},{1,9},{2,10},{3,11},{4,12},{5,13},{6,14},{7,15},{8,24},{9,25... | collective-permute-start | bytes 786440 | tf_op jit(solution)/shard_map/ppermute | solution.py:319
  112.3 17.9 %collective-permute-start.39 = (bf16[64,2048]{1,0:T(8,128)(2,1)S(1)}, bf16[64,2048]{1,0:T(8,128)(2,1)S(1)}, u32[]{:S(2)}, u32[]{:S(2)}) collective-permute-start(bf16[64,2048]{1,0:T(8,128)(2,1)S(1)} %get-tuple-element.101), channel_id=1, source_target_pairs={{0,1},{1,0},{2,3},{3,2},{4,5},{5,4},{6,7},{7,6},{8,9},{9,8},{10,11... | collective-permute-start | bytes 786440 | tf_op jit(solution)/shard_map/ppermute | solution.py:319
  114.8 7.8 %collective-permute-start.28 = (bf16[48,2048]{1,0:T(8,128)(2,1)S(1)}, bf16[48,2048]{1,0:T(8,128)(2,1)S(1)}, u32[]{:S(2)}, u32[]{:S(2)}) collective-permute-start(bf16[48,2048]{1,0:T(8,128)(2,1)S(1)} %get-tuple-element.87), channel_id=1, source_target_pairs={{0,4},{1,5},{2,6},{3,7},{4,0},{5,1},{6,2},{7,3},{8,12},{9,13},{10,... | collective-permute-start | bytes 589832 | tf_op jit(solution)/shard_map/ppermute | solution.py:319
  116.2 11.0 %collective-permute-start.29 = (bf16[48,2048]{1,0:T(8,128)(2,1)S(1)}, bf16[48,2048]{1,0:T(8,128)(2,1)S(1)}, u32[]{:S(2)}, u32[]{:S(2)}) collective-permute-start(bf16[48,2048]{1,0:T(8,128)(2,1)S(1)} %get-tuple-element.88), channel_id=1, source_target_pairs={{0,6},{1,7},{2,4},{3,5},{4,2},{5,3},{6,0},{7,1},{8,14},{9,15},{10,... | collective-permute-start | bytes 589832 | tf_op jit(solution)/shard_map/ppermute | solution.py:319
  120.5 10.7 %collective-permute-start.12 = (bf16[48,2048]{1,0:T(8,128)(2,1)S(1)}, bf16[48,2048]{1,0:T(8,128)(2,1)S(1)}, u32[]{:S(2)}, u32[]{:S(2)}) collective-permute-start(bf16[48,2048]{1,0:T(8,128)(2,1)S(1)} %get-tuple-element.74), channel_id=1, source_target_pairs={{0,2},{1,3},{2,0},{3,1},{4,6},{5,7},{6,4},{7,5},{8,10},{9,11},{10,... | collective-permute-start | bytes 589832 | tf_op jit(solution)/shard_map/ppermute | solution.py:319
  122.6 8.9 %collective-permute-start.13 = (bf16[48,2048]{1,0:T(8,128)(2,1)S(1)}, bf16[48,2048]{1,0:T(8,128)(2,1)S(1)}, u32[]{:S(2)}, u32[]{:S(2)}) collective-permute-start(bf16[48,2048]{1,0:T(8,128)(2,1)S(1)} %get-tuple-element.75), channel_id=1, source_target_pairs={{0,4},{1,5},{2,6},{3,7},{4,0},{5,1},{6,2},{7,3},{8,12},{9,13},{10,... | collective-permute-start | bytes 589832 | tf_op jit(solution)/shard_map/ppermute | solution.py:319
  127.1 13.5 %collective-permute-start.57 = (bf16[64,2048]{1,0:T(8,128)(2,1)S(1)}, bf16[64,2048]{1,0:T(8,128)(2,1)S(1)}, u32[]{:S(2)}, u32[]{:S(2)}) collective-permute-start(bf16[64,2048]{1,0:T(8,128)(2,1)S(1)} %shard_map.136), channel_id=1, source_target_pairs={{0,8},{1,9},{2,10},{3,11},{4,12},{5,13},{6,14},{7,15},{8,24},{9,25... | collective-permute-start | bytes 786440 | tf_op jit(solution)/shard_map/ppermute | solution.py:319
  130.1 10.5 %collective-permute-start.53 = (bf16[64,2048]{1,0:T(8,128)(2,1)S(1)}, bf16[64,2048]{1,0:T(8,128)(2,1)S(1)}, u32[]{:S(2)}, u32[]{:S(2)}) collective-permute-start(bf16[64,2048]{1,0:T(8,128)(2,1)S(1)} %get-tuple-element.114), channel_id=1, source_target_pairs={{0,1},{1,0},{2,3},{3,2},{4,5},{5,4},{6,7},{7,6},{8,9},{9,8},{10,11... | collective-permute-start | bytes 786440 | tf_op jit(solution)/shard_map/ppermute | solution.py:319
  130.8 13.1 %collective-permute-start.50 = (bf16[64,2048]{1,0:T(8,128)(2,1)S(1)}, bf16[64,2048]{1,0:T(8,128)(2,1)S(1)}, u32[]{:S(2)}, u32[]{:S(2)}) collective-permute-start(bf16[64,2048]{1,0:T(8,128)(2,1)S(1)} %shard_map.133), channel_id=1, source_target_pairs={{0,8},{1,9},{2,10},{3,11},{4,12},{5,13},{6,14},{7,15},{8,24},{9,25... | collective-permute-start | bytes 786440 | tf_op jit(solution)/shard_map/ppermute | solution.py:319
  131.3 12.6 %collective-permute-start.30 = (bf16[64,2048]{1,0:T(8,128)(2,1)S(1)}, bf16[64,2048]{1,0:T(8,128)(2,1)S(1)}, u32[]{:S(2)}, u32[]{:S(2)}) collective-permute-start(bf16[64,2048]{1,0:T(8,128)(2,1)S(1)} %get-tuple-element.90), channel_id=1, source_target_pairs={{0,1},{1,0},{2,3},{3,2},{4,5},{5,4},{6,7},{7,6},{8,9},{9,8},{10,11... | collective-permute-start | bytes 786440 | tf_op jit(solution)/shard_map/ppermute | solution.py:319
  131.5 8.0 %collective-permute-start.14 = (bf16[48,2048]{1,0:T(8,128)(2,1)S(1)}, bf16[48,2048]{1,0:T(8,128)(2,1)S(1)}, u32[]{:S(2)}, u32[]{:S(2)}) collective-permute-start(bf16[48,2048]{1,0:T(8,128)(2,1)S(1)} %get-tuple-element.76), channel_id=1, source_target_pairs={{0,6},{1,7},{2,4},{3,5},{4,2},{5,3},{6,0},{7,1},{8,14},{9,15},{10,... | collective-permute-start | bytes 589832 | tf_op jit(solution)/shard_map/ppermute | solution.py:319
  141.3 10.1 %collective-permute-start.58 = (bf16[64,2048]{1,0:T(8,128)(2,1)S(1)}, bf16[64,2048]{1,0:T(8,128)(2,1)S(1)}, u32[]{:S(2)}, u32[]{:S(2)}) collective-permute-start(bf16[64,2048]{1,0:T(8,128)(2,1)S(1)} %shard_map.137), channel_id=1, source_target_pairs={{0,8},{1,9},{2,10},{3,11},{4,12},{5,13},{6,14},{7,15},{8,24},{9,25... | collective-permute-start | bytes 786440 | tf_op jit(solution)/shard_map/ppermute | solution.py:319
  143.7 9.1 %collective-permute-start.15 = (bf16[64,2048]{1,0:T(8,128)(2,1)S(1)}, bf16[64,2048]{1,0:T(8,128)(2,1)S(1)}, u32[]{:S(2)}, u32[]{:S(2)}) collective-permute-start(bf16[64,2048]{1,0:T(8,128)(2,1)S(1)} %get-tuple-element.79), channel_id=1, source_target_pairs={{0,1},{1,0},{2,3},{3,2},{4,5},{5,4},{6,7},{7,6},{8,9},{9,8},{10,11... | collective-permute-start | bytes 786440 | tf_op jit(solution)/shard_map/ppermute | solution.py:319
  144.5 12.0 %collective-permute-start.51 = (bf16[64,2048]{1,0:T(8,128)(2,1)S(1)}, bf16[64,2048]{1,0:T(8,128)(2,1)S(1)}, u32[]{:S(2)}, u32[]{:S(2)}) collective-permute-start(bf16[64,2048]{1,0:T(8,128)(2,1)S(1)} %shard_map.134), channel_id=1, source_target_pairs={{0,8},{1,9},{2,10},{3,11},{4,12},{5,13},{6,14},{7,15},{8,24},{9,25... | collective-permute-start | bytes 786440 | tf_op jit(solution)/shard_map/ppermute | solution.py:319
  (24 other events, 294.7 us)
